TPU v7x, 32 devices: a whole 2x2x4 slice. The times are simulated.
32 devices in a mesh: sp: 16 (over z, y, x), tp: 2 (over core).
Axes of the slice: x: 2, y: 2, z: 4, core: 2. Of those that a mesh axis runs over, the one named last changes fastest.
Arguments:
- moe_input: bfloat16 [4096, 2048], P('sp'), may hold values from -6 to 6
- cotangent: bfloat16 [4096, 2048], P('sp'), may hold values from -6 to 6
- expert_ids: int32 [4096, 2], P('sp'), may hold values from 0 to 15, all different within a row; in each aligned block of 256 rows (0 to 255, 256 to 511, ...) at most 64 rows name the same one
- route_weight: float32 [4096, 2], P('sp'), may hold values from 0.05 to 0.6
- gate_proj: bfloat16 [16, 2048, 1024], P('sp', None, 'tp'), may hold values from -0.125 to 0.125
- up_proj: bfloat16 [16, 2048, 1024], P('sp', None, 'tp'), may hold values from -0.125 to 0.125
- down_proj: bfloat16 [16, 1024, 2048], P('sp', 'tp'), may hold values from -0.1875 to 0.1875
- out_weight: bfloat16 [2048, 2048], P(None, 'tp'), may hold values from -0.125 to 0.125
- recur_input: bfloat16 [4096, 2048], P('sp', 'tp'), may hold values from -6 to 6
- gate_input: bfloat16 [4096, 2048], P('sp', 'tp'), may hold values from -6 to 6
- states: float32 [4096, 2048], P('sp', 'tp'), may hold values from -6 to 6
- conv_taps: bfloat16 [4, 2048], P(None, 'tp'), may hold values from -3 to 3
- decay_gate_w: bfloat16 [16, 128, 128], P('tp'), may hold values from -0.5 to 0.5
- input_gate_w: bfloat16 [16, 128, 128], P('tp'), may hold values from -0.5 to 0.5
- decay_rate: float32 [2048], P('tp'), may hold values from 7.3242187e-06 to 0.008
- decay_extra: float32 [4096, 2048], P('sp', 'tp'), may hold values from -0.77 to 0
Outputs:
- gate_proj_grad: bfloat16 [16, 2048, 1024], P('sp', None, 'tp')
- up_proj_grad: bfloat16 [16, 2048, 1024], P('sp', None, 'tp')
- down_proj_grad: bfloat16 [16, 1024, 2048], P('sp', 'tp')
- out_weight_grad: float32 [2048, 2048], P('sp', 'tp')
- input_grad: bfloat16 [4096, 2048], P('sp')
- recur_grad: bfloat16 [4096, 2048], P('sp', 'tp')
- gate_grad: bfloat16 [4096, 2048], P('sp', 'tp')
Inputs may be any that keep to these rules, and one draw needn't show every extreme that they name: `expert_ids`: within each aligned block of 256 tokens a token names 2 different experts, and no expert is named more than 64 times.
All inputs are finite; a program needn't handle non-finite values.
Results may differ from a plain program's by a relative error of at most 0.012.
Values may be sent and summed in bfloat16 or wider, within the bound.
No kernel may reach another device: no remote copies, remote signals or barrier semaphores. Data moves between devices by JAX's collectives and lax.ppermute only.
A program may use at most 128 MiB of HBM per device.

v0:
```python
import jax
import jax.numpy as jnp
from jax import lax
from jax.experimental import pallas as pl
from jax.experimental.pallas import tpu as pltpu
from jax.sharding import PartitionSpec as P


decay_scale = 8.0
f32 = jnp.float32
bf16 = jnp.bfloat16


def dot(left, right, contract):
    return lax.dot_general(left, right, (contract, ((), ())), preferred_element_type=f32)


def rows_of(left, right):
    return dot(left, right, ((0,), (0,)))


def cols_of(left, right):
    return dot(left, right, ((1,), (1,)))


def times(left, right):
    return dot(left, right, ((1,), (0,)))


def shifted(value, axis, steps):
    count = lax.axis_size(axis)
    pairs = [(s, s + steps) for s in range(max(0, -steps), min(count, count - steps))]
    return lax.ppermute(value, axis, pairs)


def swapped(value, axis, mask):
    count = lax.axis_size(axis)
    return lax.ppermute(value, axis, [(s, s ^ mask) for s in range(count)])


def back_scan(decays, values):
    rows = values.shape[0]
    inner = lax.broadcasted_iota(jnp.int32, values.shape, 0) % 8
    step = 1
    while step < rows:
        if step < 8:
            keep = inner < 8 - step
            later_a = jnp.where(keep, pltpu.roll(decays, rows - step, 0), 1.0)
            later_b = jnp.where(keep, pltpu.roll(values, rows - step, 0), 0.0)
            values = values + decays * later_b
            decays = decays * later_a
            step *= 2
        else:
            break
    tiles = rows // 8
    decay_out = [None] * tiles
    value_out = [None] * tiles
    carry_a = jnp.ones_like(values[:1])
    carry_b = jnp.zeros_like(values[:1])
    for tile in reversed(range(tiles)):
        part_a = decays[tile * 8 : tile * 8 + 8]
        part_b = values[tile * 8 : tile * 8 + 8]
        value_out[tile] = part_b + part_a * carry_b
        decay_out[tile] = part_a * carry_a
        carry_b = value_out[tile][:1]
        carry_a = decay_out[tile][:1]
    return decay_out, value_out


def mixer_kernel(grad_ref, weight_ref, gelu_ref, slope_ref, next_ref, first_ref,
                 gate_ref, local_ref, cumul_ref, ends_ref):
    mixer = jnp.dot(grad_ref[...], weight_ref[...], preferred_element_type=f32)
    gate_ref[...] = (mixer * slope_ref[...]).astype(bf16)
    decays, values = back_scan(next_ref[...], mixer * gelu_ref[...])
    for tile, (part_a, part_b) in enumerate(zip(decays, values)):
        cumul_ref[tile * 8 : tile * 8 + 8] = part_a
        local_ref[tile * 8 : tile * 8 + 8] = part_b
    first = first_ref[...]
    end_a = first * decays[0][:1]
    end_b = first * values[0][:1]
    for peer in range(ends_ref.shape[0]):
        ends_ref[peer] = jnp.concatenate([end_a, end_b], axis=0)


def mixer_call(input_grad, out_weight, gelu, slope, next_decay, first, peers):
    rows, width = input_grad.shape
    channels = out_weight.shape[1]
    block = 256
    wide = pl.BlockSpec((rows, block), lambda i: (0, i))
    return pl.pallas_call(
        mixer_kernel,
        grid=(channels // block,),
        in_specs=[
            pl.BlockSpec((rows, width), lambda i: (0, 0)),
            pl.BlockSpec((width, block), lambda i: (0, i)),
            wide, wide, wide,
            pl.BlockSpec((1, block), lambda i: (0, i)),
        ],
        out_specs=[wide, wide, wide, pl.BlockSpec((peers, 2, block), lambda i: (0, 0, i))],
        out_shape=[
            jax.ShapeDtypeStruct((rows, channels), bf16),
            jax.ShapeDtypeStruct((rows, channels), f32),
            jax.ShapeDtypeStruct((rows, channels), f32),
            jax.ShapeDtypeStruct((peers, 2, channels), f32),
        ],
        cost_estimate=pl.CostEstimate(
            flops=2 * rows * width * channels, bytes_accessed=8 << 20, transcendentals=0
        ),
        name="mixer",
    )(input_grad, out_weight, gelu, slope, next_decay, first)


def tail_kernel(where_ref, ends_ref, local_ref, cumul_ref, to_decay_ref, to_input_ref, direct_ref,
                head_ref, head_coef_ref, taps_ref, decay_w_ref, input_w_ref, out_ref):
    mine = where_ref[0]
    count = ends_ref.shape[0]
    carry = jnp.zeros_like(local_ref[:1])
    head_carry = carry
    for place in reversed(range(1, count)):
        ends = ends_ref[place]
        longer = ends[1:2] + ends[0:1] * carry
        head_carry = jnp.where(place > mine + 1, longer, head_carry)
        carry = jnp.where(place > mine, longer, carry)
    decay_w = decay_w_ref[0]
    input_w = input_w_ref[0]

    def conv_grad(carried, to_decay, to_input, direct):
        decay_pre = (carried * to_decay).astype(bf16)
        input_pre = (carried * to_input).astype(bf16)
        return carried * direct + cols_of(decay_pre, decay_w) + cols_of(input_pre, input_w)

    main = conv_grad(
        local_ref[...] + cumul_ref[...] * carry, to_decay_ref[...], to_input_ref[...], direct_ref[...]
    )
    halo = conv_grad(
        head_ref[...] + head_coef_ref[0] * head_carry,
        head_coef_ref[1], head_coef_ref[2], head_coef_ref[3],
    )
    rows = main.shape[0]
    whole = jnp.concatenate([main, halo], axis=0)
    taps = taps_ref[...].astype(f32)
    total = taps[0:1] * pltpu.roll(whole, whole.shape[0] - 3, 0)
    for tap in range(1, 3):
        total = total + taps[tap : tap + 1] * pltpu.roll(whole, whole.shape[0] - 3 + tap, 0)
    total = total + taps[3:4] * whole
    out_ref[...] = total[:rows].astype(bf16)


def tail_call(mine, ends, local, cumul, to_decay, to_input, direct, head, head_coef, taps, decay_w, input_w):
    rows, channels = local.shape
    count = ends.shape[0]
    block = decay_w.shape[1]
    wide = pl.BlockSpec((rows, block), lambda i, s: (0, i))
    return pl.pallas_call(
        tail_kernel,
        grid_spec=pltpu.PrefetchScalarGridSpec(
            num_scalar_prefetch=1,
            grid=(channels // block,),
            in_specs=[
                pl.BlockSpec((count, 2, block), lambda i, s: (0, 0, i)),
                wide, wide, wide, wide, wide,
                pl.BlockSpec((8, block), lambda i, s: (0, i)),
                pl.BlockSpec((4, 8, block), lambda i, s: (0, 0, i)),
                pl.BlockSpec((4, block), lambda i, s: (0, i)),
                pl.BlockSpec((1, block, block), lambda i, s: (i, 0, 0)),
                pl.BlockSpec((1, block, block), lambda i, s: (i, 0, 0)),
            ],
            out_specs=wide,
        ),
        out_shape=jax.ShapeDtypeStruct((rows, channels), bf16),
        cost_estimate=pl.CostEstimate(
            flops=8 * rows * block * channels, bytes_accessed=7 << 20, transcendentals=0
        ),
        name="tail",
    )(mine, ends, local, cumul, to_decay, to_input, direct, head, head_coef, taps, decay_w, input_w)


def combine_kernel(where_ref, mine_ref, other_ref, cot_ref, grad_ref, *piece_refs):
    total = mine_ref[...].astype(f32) + other_ref[...].astype(f32) + cot_ref[...].astype(f32)
    grad_ref[...] = total.astype(bf16)
    group = len(piece_refs)
    inner = lax.rem(where_ref[0], group)
    wide = grad_ref.shape[1] // group
    cut = piece_refs[0].shape[1]
    lanes = 128
    outer = cut // lanes
    assert wide == cut
    for k, piece_ref in enumerate(piece_refs):
        for level in range(outer):
            column = pl.multiple_of((level * group + (inner ^ k)) * lanes, lanes)
            piece_ref[:, level * lanes : (level + 1) * lanes] = grad_ref[:, pl.ds(column, lanes)]


def combine_call(where, mine, other, cotangent, group):
    rows, width = mine.shape
    block = rows // 4
    cut = width // group
    wide = pl.BlockSpec((block, width), lambda i, s: (i, 0))
    return pl.pallas_call(
        combine_kernel,
        grid_spec=pltpu.PrefetchScalarGridSpec(
            num_scalar_prefetch=1,
            grid=(4,),
            in_specs=[wide, wide, wide],
            out_specs=[wide] + [pl.BlockSpec((block, cut), lambda i, s: (i, 0))] * group,
        ),
        out_shape=[jax.ShapeDtypeStruct((rows, width), bf16)]
        + [jax.ShapeDtypeStruct((rows, cut), bf16)] * group,
        cost_estimate=pl.CostEstimate(flops=1 << 28, bytes_accessed=5 << 20, transcendentals=0),
        name="combine",
    )(where, mine, other, cotangent)


def on_device(
    moe_input,
    cotangent,
    expert_ids,
    route_weight,
    gate_proj,
    up_proj,
    down_proj,
    out_weight,
    recur_input,
    gate_input,
    states,
    conv_taps,
    decay_gate_w,
    input_gate_w,
    decay_rate,
    decay_extra,
):
    experts = lax.axis_size("sp")
    cores = lax.axis_size("tp")
    place = lax.axis_index("sp")
    core = lax.axis_index("tp")
    group = 8 if experts % 8 == 0 else experts
    outer = experts // group
    tok_rows, width = moe_input.shape
    channels = recur_input.shape[1]
    top_count = expert_ids.shape[1]
    capacity = max(2, 4 * tok_rows // experts)
    share = capacity // cores
    own_slots = experts * share

    flat_ids = expert_ids.reshape(-1)
    onehot = (flat_ids[:, None] == jnp.arange(experts, dtype=jnp.int32)[None, :]).astype(jnp.int32)
    slot_rank = jnp.sum((jnp.cumsum(onehot, axis=0) - onehot) * onehot, axis=1)
    pair_slots = (flat_ids * capacity + slot_rank).reshape(tok_rows, top_count)
    slot_iota = jnp.arange(own_slots, dtype=jnp.int32)
    slot_ids = (slot_iota // share) * capacity + core * share + slot_iota % share
    hits = slot_ids[:, None, None] == pair_slots[None, :, :]
    placing = jnp.any(hits, axis=2).astype(bf16)
    slot_weight = jnp.sum(jnp.where(hits, route_weight[None, :, :], 0.0), axis=(1, 2))
    send_rows = times(placing, moe_input).astype(bf16).reshape(experts, share, width)
    edge = jnp.concatenate([recur_input[-3:].astype(f32), states[-1:]], axis=0)
    edge = shifted(edge, "sp", 1)
    edge, send_rows, late = lax.optimization_barrier((edge, send_rows, (gate_input, states, cotangent)))
    gate_input, states, cotangent_late = late
    got_rows = lax.all_to_all(send_rows, "sp", split_axis=0, concat_axis=0, tiled=True)

    send_grads = times(placing, cotangent_late) * slot_weight[:, None]
    send_grads = send_grads.astype(bf16).reshape(experts, share, width)

    gate_float = gate_input.astype(f32)
    gelu_value, gelu_back = jax.vjp(jax.nn.gelu, gate_float)
    slope = states * gelu_back(jnp.ones_like(gate_float))[0]
    mixer_out = (states * gelu_value).astype(bf16)
    extended = jnp.concatenate([edge[:3], recur_input.astype(f32)], axis=0)
    prev_state = edge[3:]
    taps = conv_taps.astype(f32)
    conv = taps[0] * extended[0:tok_rows]
    for tap in range(1, 4):
        conv = conv + taps[tap] * extended[tap : tap + tok_rows]
    blocks, block_width = decay_gate_w.shape[:2]
    conv_low = conv.astype(bf16)

    def by_block(value, weights):
        parts = [
            times(value[:, b * block_width : (b + 1) * block_width], weights[b]) for b in range(blocks)
        ]
        return jnp.concatenate(parts, axis=1)

    recur_gate = jax.nn.sigmoid(by_block(conv_low, decay_gate_w))
    input_gate = jax.nn.sigmoid(by_block(conv_low, input_gate_w))
    first_row = (place * tok_rows + jnp.arange(tok_rows, dtype=jnp.int32) == 0)[:, None]
    log_decay = -decay_scale * recur_gate * decay_rate[None, :] + decay_extra
    decay_value = jnp.exp(log_decay)
    mult = jnp.where(first_row, 1.0, jnp.sqrt(-jnp.expm1(2.0 * log_decay)))
    prev_states = jnp.concatenate([prev_state, states[:-1]], axis=0)
    next_decay = jnp.concatenate([decay_value[1:], jnp.ones((1, channels), f32)], axis=0)
    to_log = prev_states * decay_value - jnp.where(
        first_row, 0.0, input_gate * conv * decay_value * decay_value / mult
    )
    to_decay = to_log * (-decay_scale * decay_rate[None, :]) * recur_gate * (1.0 - recur_gate)
    to_input = mult * conv * input_gate * (1.0 - input_gate)
    direct = mult * input_gate

    statics = (gelu_value, slope, mixer_out, next_decay, decay_value[:1], to_decay, to_input, direct)
    statics, send_grads = lax.optimization_barrier((statics, send_grads))
    gelu_value, slope, mixer_out, next_decay, first_decay, to_decay, to_input, direct = statics

    got_grads = lax.all_to_all(send_grads, "sp", split_axis=0, concat_axis=0, tiled=True)
    rows_here = got_rows.reshape(own_slots, width)
    rows_there = swapped(rows_here, "tp", 1)
    head_coef = shifted(jnp.stack([to_decay[:8], to_input[:8], direct[:8]]), "sp", -1)
    mixers = {0: mixer_out}
    half = group // 2
    mixers[half] = swapped(mixer_out, "sp", half)
    weight_gate = gate_proj[0]
    weight_up = up_proj[0]
    weight_down = down_proj[0]
    pres = tuple(
        (times(rows, weight_gate), times(rows, weight_up)) for rows in (rows_here, rows_there)
    )
    got_grads, mixers[half], pres, rows_there = lax.optimization_barrier(
        (got_grads, mixers[half], pres, rows_there)
    )
    for k in range(1, half):
        mixers[k] = swapped(mixer_out, "sp", k)
        mixers[k ^ half] = swapped(mixers[half], "sp", k)
    grads_here = got_grads.reshape(own_slots, width)
    grads_there = swapped(grads_here, "tp", 1)

    def expert(pre, grads_in):
        gate_pre, up_pre = pre
        sigmoid_gate = jax.nn.sigmoid(gate_pre)
        silu_gate = gate_pre * sigmoid_gate
        hidden = (silu_gate * up_pre).astype(bf16)
        hidden_grad = cols_of(grads_in, weight_down)
        gate_pre_grad = (
            hidden_grad * up_pre * sigmoid_gate * (1.0 + gate_pre * (1.0 - sigmoid_gate))
        ).astype(bf16)
        up_pre_grad = (hidden_grad * silu_gate).astype(bf16)
        return hidden, gate_pre_grad, up_pre_grad

    hidden_h, gate_h, up_h = expert(pres[0], grads_here)
    grads_there, hidden_h, gate_h, up_h = lax.optimization_barrier((grads_there, hidden_h, gate_h, up_h))
    hidden_t, gate_t, up_t = expert(pres[1], grads_there)
    partial_t = cols_of(gate_t, weight_gate) + cols_of(up_t, weight_up)
    from_there = swapped(partial_t.astype(bf16), "tp", 1)
    partial_h = cols_of(gate_h, weight_gate) + cols_of(up_h, weight_up)
    shared = (partial_h + from_there.astype(f32)).astype(bf16).reshape(experts, share, width)
    back = lax.all_to_all(shared, "sp", split_axis=0, concat_axis=0, tiled=True)
    down_grad = rows_of(hidden_h, grads_here) + rows_of(hidden_t, grads_there)
    gate_weight_grad = rows_of(rows_here, gate_h) + rows_of(rows_there, gate_t)
    up_weight_grad = rows_of(rows_here, up_h) + rows_of(rows_there, up_t)
    weight_grads = (gate_weight_grad.astype(bf16), up_weight_grad.astype(bf16), down_grad.astype(bf16))
    back, weight_grads, mixers, head_coef = lax.optimization_barrier(
        (back, weight_grads, mixers, head_coef)
    )

    mine_back = rows_of(placing, back.reshape(own_slots, width)).astype(bf16)
    other_back = swapped(mine_back, "tp", 1)
    out_rows = width // experts
    where = place[None].astype(jnp.int32)
    if out_rows % 128 == 0:
        input_grad, *pieces = combine_call(where, mine_back, other_back, cotangent, group)
    else:
        input_grad = (
            mine_back.astype(f32) + other_back.astype(f32) + cotangent.astype(f32)
        ).astype(bf16)
        split_grad = input_grad.reshape(tok_rows, outer, group, out_rows)
        pieces = [
            lax.dynamic_slice_in_dim(split_grad, place % group ^ k, 1, 2).reshape(tok_rows, -1)
            for k in range(group)
        ]

    grads = [pieces[0]]
    for k in range(1, group):
        grads.append(swapped(pieces[k], "sp", k))
    gate_grad, local, cumul, ends = mixer_call(
        input_grad, out_weight, gelu_value, slope, next_decay, first_decay, experts
    )
    head = shifted(jnp.stack([local[:8], cumul[:8]]), "sp", -1)
    ends = lax.all_to_all(ends, "sp", split_axis=0, concat_axis=0, tiled=True)
    grads, ends, head = lax.optimization_barrier((grads, ends, head))
    product = rows_of(grads[0], mixers[0])
    for k in range(1, group):
        product = product + rows_of(grads[k], mixers[k])
    product = product.reshape(outer, out_rows, channels)
    level = place // group

    def block_for(index):
        return lax.dynamic_slice_in_dim(product, index, 1, 0)[0]

    out_weight_grad = block_for(level)
    for k in range(1, outer):
        received = swapped(block_for(level ^ k).astype(bf16), "sp", k * group)
        out_weight_grad = out_weight_grad + received.astype(f32)

    head_coef = jnp.concatenate([head[1:], head_coef], axis=0)
    recur_grad = tail_call(
        where, ends, local, cumul, to_decay, to_input, direct,
        head[0], head_coef, conv_taps, decay_gate_w, input_gate_w,
    )
    return (
        weight_grads[0][None],
        weight_grads[1][None],
        weight_grads[2][None],
        out_weight_grad,
        input_grad,
        recur_grad,
        gate_grad,
    )


def solution(mesh):
    return jax.shard_map(
        on_device,
        mesh=mesh,
        in_specs=(
            P("sp", None),
            P("sp", None),
            P("sp", None),
            P("sp", None),
            P("sp", None, "tp"),
            P("sp", None, "tp"),
            P("sp", "tp", None),
            P(None, "tp"),
            P("sp", "tp"),
            P("sp", "tp"),
            P("sp", "tp"),
            P(None, "tp"),
            P("tp", None, None),
            P("tp", None, None),
            P("tp"),
            P("sp", "tp"),
        ),
        out_specs=(
            P("sp", None, "tp"),
            P("sp", None, "tp"),
            P("sp", "tp", None),
            P("sp", "tp"),
            P("sp", None),
            P("sp", "tp"),
            P("sp", "tp"),
        ),
        check_vma=False,
    )
```

profile of v0, /device:TPU:0, one launch (start us, length us, event | category | flops | bytes accessed | tf_op | source)
XLA Modules:
  0.0 297.5 jit_solution(6932563781595241071)
XLA Ops:
  2.3 4.9 %collective-permute-start = (f32[4,1024]{1,0:T(4,128)S(1)}, f32[4,1024]{1,0:T(4,128)S(1)}, u32[]{:S(2)}, u32[]{:S(2)}) collective-permute-start(f32[4,1024]{1,0:T(4,128)S(1)} %pad_maximum_fusion.4), channel_id=1, source_target_pairs={{0,2},{2,4},{4,6},{6,8},{8,10},{10,12},{12,14},{14,16},{16,18},{18... | collective-permute-start | bytes 49160 | tf_op jit(solution)/shard_map/ppermute | solution.py:33
  8.3 1.2 reduce-window.6
  13.4 3.3 %convolution_convert_fusion = bf16[512,2048]{1,0:T(8,128)(2,1)} fusion(pred[512,256]{1,0:T(8,128)(4,1)S(1)} %compare_reduce_fusion, bf16[256,2048]{1,0:T(8,128)(2,1)} %param.16), kind=kOutput, calls=%fused_computation.6 | convolution fusion | flops 537919488 | bytes 3276800 | tf_op jit(solution)/shard_map/dot_general | solution.py:15
  16.7 1.2 convert_element_type.87
  17.9 1.4 fusion.117
  22.5 6.1 %all-to-all-start.1 = ((bf16[16,32,2048]{2,1,0:T(8,128)(2,1)}), bf16[16,32,2048]{2,1,0:T(8,128)(2,1)}, u32[]{:S(2)}, u32[]{:S(2)}) async-start(bf16[16,32,2048]{2,1,0:T(8,128)(2,1)} %bitcast.170), calls=%async_computation.1 | async-start | bytes 4194304 | tf_op jit(solution)/shard_map/all_to_all | solution.py:259
  33.1 4.7 %subtract_multiply_fusion = (f32[256,1024]{1,0:T(8,128)S(1)}, f32[256,1024]{1,0:T(8,128)}, f32[256,1024]{1,0:T(8,128)}, f32[256,1024]{1,0:T(8,128)S(1)}) fusion(f32[256,1024]{1,0:T(8,128)S(1)} %copy-done.10, f32[256,1024]{1,0:T(8,128)S(1)} %convolution_dynamic-update-slice_fusion, f32[256,1024]{1,0:T(8,128)} %param.31, f32[1024]{0:T(1024)S(1)} %broadcast_multiply_fusion, ...), kind=kLoop, calls=%fused_computation.94 | loop fusion | flops 7340032 | bytes 9441536 | tf_op jit(solution)/shard_map/mul | solution.py:295
  38.6 1.1 concatenate.24.next_ref
  39.7 2.0 multiply_convert_fusion
  41.7 2.0 multiply_convert_fusion.7
  43.7 27.9 %all-to-all-done.1 = bf16[16,32,2048]{2,1,0:T(8,128)(2,1)} async-done(((bf16[16,32,2048]{2,1,0:T(8,128)(2,1)}), bf16[16,32,2048]{2,1,0:T(8,128)(2,1)}, u32[]{:S(2)}, u32[]{:S(2)}) %all-to-all-start.1) | async-done | bytes 2097184 | tf_op jit(solution)/shard_map/all_to_all | solution.py:259
  71.6 10.0 %all-to-all-start = ((bf16[16,32,2048]{2,1,0:T(8,128)(2,1)}), bf16[16,32,2048]{2,1,0:T(8,128)(2,1)}, u32[]{:S(2)}, u32[]{:S(2)}) async-start(bf16[16,32,2048]{2,1,0:T(8,128)(2,1)} %bitcast.171), calls=%async_computation | async-start | bytes 4194304 | tf_op jit(solution)/shard_map/all_to_all | solution.py:302
  81.6 1.9 collective-permute-start.1
  83.6 4.4 %fusion.16 = f32[512,512]{1,0:T(8,128)} fusion(bf16[512,2048]{1,0:T(8,128)(2,1)} %bitcast.23, bf16[1,2048,512]{2,1,0:T(8,128)(2,1)} %param.20), kind=kOutput, calls=%fused_computation.24 | convolution fusion | flops 1073741824 | bytes 5242880 | tf_op jit(solution)/shard_map/dot_general | solution.py:15
  88.0 4.0 %fusion.9 = f32[512,512]{1,0:T(8,128)} fusion(bf16[512,2048]{1,0:T(8,128)(2,1)} %bitcast.23, bf16[1,2048,512]{2,1,0:T(8,128)(2,1)S(1)} %copy-done), kind=kOutput, calls=%fused_computation.17 | convolution fusion | flops 1073741824 | bytes 5242880 | tf_op jit(solution)/shard_map/dot_general | solution.py:15
  92.0 2.2 fusion.14
  94.2 2.3 fusion.7
  96.5 31.6 %collective-permute-done.1 = bf16[256,1024]{1,0:T(8,128)(2,1)} collective-permute-done((bf16[256,1024]{1,0:T(8,128)(2,1)}, bf16[256,1024]{1,0:T(8,128)(2,1)}, u32[]{:S(2)}, u32[]{:S(2)}) %collective-permute-start.1) | collective-permute-done | bytes 524320 | tf_op jit(solution)/shard_map/ppermute | solution.py:38
  128.2 5.4 %multiply_convert_fusion.4 = (bf16[512,512]{1,0:T(8,128)(2,1)S(1)}, bf16[512,512]{1,0:T(8,128)(2,1)S(1)}, bf16[512,512]{1,0:T(8,128)(2,1)}) fusion(f32[512,512]{1,0:T(8,128)} %fusion.16, f32[512,512]{1,0:T(8,128)} %fusion.9, bf16[512,2048]{1,0:T(8,128)(2,1)} %bitcast.26, bf16[1,512,2048]{2,1,0:T(8,128)(2,1)} %param.22), kind=kOutput, calls=%fused_computation.89 | convolution fusion | flops 1077673984 | bytes 7864320 | tf_op jit(solution)/shard_map/dot_general | solution.py:15
  133.6 1.7 multiply_convert_fusion.2
  136.3 1.3 fusion.11
  137.6 1.3 add_convert_fusion.4
  139.3 1.3 fusion.5
  140.6 2.5 collective-permute-done.4
  143.1 2.7 add_convert_fusion.3
  145.8 6.6 %all-to-all-start.2 = ((bf16[16,32,2048]{2,1,0:T(8,128)(2,1)}), bf16[16,32,2048]{2,1,0:T(8,128)(2,1)}, u32[]{:S(2)}, u32[]{:S(2)}) async-start(bf16[16,32,2048]{2,1,0:T(8,128)(2,1)} %bitcast.172), calls=%async_computation.2 | async-start | bytes 4194304 | tf_op jit(solution)/shard_map/all_to_all | solution.py:343
  152.4 1.9 collective-permute-start.5
  154.3 1.5 collective-permute-start.6
  157.6 1.6 collective-permute-start.11
  159.2 4.0 %collective-permute-start.10 = (bf16[256,1024]{1,0:T(8,128)(2,1)}, bf16[256,1024]{1,0:T(8,128)(2,1)S(1)}, u32[]{:S(2)}, u32[]{:S(2)}) collective-permute-start(bf16[256,1024]{1,0:T(8,128)(2,1)} %collective-permute-done.1), channel_id=1, source_target_pairs={{0,6},{2,4},{4,2},{6,0},{8,14},{10,12},{12,10},{14,8},{16,22},{18,... | collective-permute-start | bytes 1572872 | tf_op jit(solution)/shard_map/ppermute | solution.py:38
  163.2 2.3 fusion.122
  165.5 4.4 %add_convert_fusion.1 = bf16[2048,512]{1,0:T(8,128)(2,1)} fusion(f32[2048,512]{1,0:T(8,128)S(1)} %fusion.122, bf16[512,2048]{1,0:T(8,128)(2,1)} %bitcast.23, bf16[512,512]{1,0:T(8,128)(2,1)S(1)} %copy-done.12), kind=kOutput, calls=%fused_computation.1 | convolution fusion | flops 1075838976 | bytes 8912896 | tf_op jit(solution)/shard_map/dot_general | solution.py:15
  169.9 1.3 fusion.121
  171.3 4.5 %add_convert_fusion.2 = bf16[2048,512]{1,0:T(8,128)(2,1)} fusion(f32[2048,512]{1,0:T(8,128)S(1)} %fusion.121, bf16[512,2048]{1,0:T(8,128)(2,1)} %bitcast.23, bf16[512,512]{1,0:T(8,128)(2,1)S(1)} %copy-done.20), kind=kOutput, calls=%fused_computation.2 | convolution fusion | flops 1075838976 | bytes 8912896 | tf_op jit(solution)/shard_map/dot_general | solution.py:15
  175.7 27.6 %collective-permute-done.11 = f32[3,8,1024]{2,1,0:T(8,128)} collective-permute-done((f32[3,8,1024]{2,1,0:T(8,128)S(1)}, f32[3,8,1024]{2,1,0:T(8,128)}, u32[]{:S(2)}, u32[]{:S(2)}) %collective-permute-start.11) | collective-permute-done | bytes 98336 | tf_op jit(solution)/shard_map/ppermute | solution.py:33
  203.3 4.3 %collective-permute-start.8 = (bf16[256,1024]{1,0:T(8,128)(2,1)}, bf16[256,1024]{1,0:T(8,128)(2,1)S(1)}, u32[]{:S(2)}, u32[]{:S(2)}) collective-permute-start(bf16[256,1024]{1,0:T(8,128)(2,1)} %collective-permute-done.1), channel_id=1, source_target_pairs={{0,2},{2,0},{4,6},{6,4},{8,10},{10,8},{12,14},{14,12},{16,18},{18,... | collective-permute-start | bytes 1572872 | tf_op jit(solution)/shard_map/ppermute | solution.py:38
  207.6 1.2 collective-permute-start.9
  208.8 1.4 fusion.49
  210.2 4.3 %add_convert_fusion = bf16[512,2048]{1,0:T(8,128)(2,1)} fusion(f32[512,2048]{1,0:T(8,128)S(1)} %fusion.49, bf16[512,512]{1,0:T(8,128)(2,1)S(1)} %copy-done.21, bf16[512,2048]{1,0:T(8,128)(2,1)} %bitcast.26), kind=kOutput, calls=%fused_computation | convolution fusion | flops 1075838976 | bytes 8912896 | tf_op jit(solution)/shard_map/dot_general | solution.py:15
  214.5 4.8 %collective-permute-done.10 = bf16[256,1024]{1,0:T(8,128)(2,1)S(1)} collective-permute-done((bf16[256,1024]{1,0:T(8,128)(2,1)}, bf16[256,1024]{1,0:T(8,128)(2,1)S(1)}, u32[]{:S(2)}, u32[]{:S(2)}) %collective-permute-start.10) | collective-permute-done | bytes 524320 | tf_op jit(solution)/shard_map/ppermute | solution.py:38
  219.3 5.5 %collective-permute-done.8 = bf16[256,1024]{1,0:T(8,128)(2,1)S(1)} collective-permute-done((bf16[256,1024]{1,0:T(8,128)(2,1)}, bf16[256,1024]{1,0:T(8,128)(2,1)S(1)}, u32[]{:S(2)}, u32[]{:S(2)}) %collective-permute-start.8) | collective-permute-done | bytes 524320 | tf_op jit(solution)/shard_map/ppermute | solution.py:38
  224.8 4.9 %collective-permute-done.9 = bf16[256,1024]{1,0:T(8,128)(2,1)} collective-permute-done((bf16[256,1024]{1,0:T(8,128)(2,1)}, bf16[256,1024]{1,0:T(8,128)(2,1)}, u32[]{:S(2)}, u32[]{:S(2)}) %collective-permute-start.9) | collective-permute-done | bytes 524320 | tf_op jit(solution)/shard_map/ppermute | solution.py:38
  229.7 2.3 convolution_convert_fusion.1.mine_ref
  232.2 2.6 collective-permute-done.12.other_ref
  235.8 4.1 %combine.1 = (bf16[256,2048]{1,0:T(8,128)(2,1)}, bf16[256,256]{1,0:T(8,128)(2,1)}, bf16[256,256]{1,0:T(8,128)(2,1)}, bf16[256,256]{1,0:T(8,128)(2,1)}, bf16[256,...) custom-call(s32[1]{0:T(128)} %bitcast.35.where_ref, ...), custom_call_target="tpu_custom_call" | custom-call | flops 268435456 | bytes 5242880 | tf_op jit(solution)/shard_map/combine/pallas_call | solution.py:199
  240.0 7.4 %mixer.1 = (bf16[256,1024]{1,0:T(8,128)(2,1)}, f32[256,1024]{1,0:T(8,128)}, f32[256,1024]{1,0:T(8,128)}, f32[16,2,1024]{2,1,0:T(2,128)}) custom-call(bf16[256,2048]{1,0:T(8,128)(2,1)} %get-tuple-element.65.grad_ref, bf16[2048,1024]{1,0:T(8,128)(2,1)} %weight_ref.1, f32[256,1024]{1,0:T(8,128)} %get-tuple-element.102.gelu_ref, ...), custom_call_target="tpu_custom_call" | custom-call | flops 1073741824 | bytes 8388608 | tf_op jit(solution)/shard_map/mixer/pallas_call | solution.py:90
  249.0 3.5 %all-to-all-start.3 = ((f32[16,2,1024]{2,1,0:T(2,128)}), f32[16,2,1024]{2,1,0:T(2,128)S(1)}, u32[]{:S(2)}, u32[]{:S(2)}) async-start(f32[16,2,1024]{2,1,0:T(2,128)} %get-tuple-element.106), calls=%async_computation.3 | async-start | bytes 262144 | tf_op jit(solution)/shard_map/all_to_all | solution.py:375
  252.5 1.9 collective-permute-start.13
  254.4 1.5 collective-permute-start.14
  255.8 1.5 collective-permute-start.20
  257.4 2.7 collective-permute-start.15
  260.1 1.5 collective-permute-start.16
  261.6 1.1 collective-permute-done.20
  262.7 2.4 collective-permute-start.17
  265.7 2.3 collective-permute-start.19
  268.0 2.1 collective-permute-done.17
  270.2 3.2 %collective-permute-done.18 = bf16[256,256]{1,0:T(8,128)(2,1)S(1)} collective-permute-done((bf16[256,256]{1,0:T(8,128)(2,1)S(1)}, bf16[256,256]{1,0:T(8,128)(2,1)S(1)}, u32[]{:S(2)}, u32[]{:S(2)}) %collective-permute-start.18) | collective-permute-done | bytes 131104 | tf_op jit(solution)/shard_map/ppermute | solution.py:38
  275.0 1.4 fusion.124
  276.4 1.4 fusion.125
  277.8 1.4 fusion.126
  279.6 1.4 fusion.128
  282.8 3.1 %collective-permute-start.21 = (bf16[128,1024]{1,0:T(8,128)(2,1)}, bf16[128,1024]{1,0:T(8,128)(2,1)S(1)}, u32[]{:S(2)}, u32[]{:S(2)}) collective-permute-start(bf16[128,1024]{1,0:T(8,128)(2,1)} %fusion.51), channel_id=1, source_target_pairs={{0,16},{2,18},{4,20},{6,22},{8,24},{10,26},{12,28},{14,30},{16,0},... | collective-permute-start | bytes 786440 | tf_op jit(solution)/shard_map/ppermute | solution.py:38
  286.5 1.6 pad_maximum_fusion.1.head_coef_ref
  288.1 7.5 %tail.1 = bf16[256,1024]{1,0:T(8,128)(2,1)} custom-call(s32[1]{0:T(128)} %bitcast.35.where_ref, f32[16,2,1024]{2,1,0:T(2,128)} %copy-done.32, f32[256,1024]{1,0:T(8,128)} %get-tuple-element.107.local_ref, f32[256,1024]{1,0:T(8,128)} %get-tuple-element.108.cumul_ref, f32[256,1024]{1,0:T(8,128)} %get-tuple-element.86.to_decay_ref, f32[256,1024]{1,0:T(8,128)} %copy-done.6, ...), custom_call_target="tpu_custom_call" | custom-call | flops 268435456 | bytes 7340032 | tf_op jit(solution)/shard_map/tail/pallas_call | solution.py:154
  (177 shorter events, 27.8 us)
Async XLA Ops:
  0.6 87.4 %copy-start = (bf16[1,2048,512]{2,1,0:T(8,128)(2,1)S(1)}, bf16[1,2048,512]{2,1,0:T(8,128)(2,1)}, u32[]{:S(2)}) copy-start(bf16[1,2048,512]{2,1,0:T(8,128)(2,1)} %param.21) | copy-start | bytes 6291460
  2.3 15.6 %collective-permute-start = (f32[4,1024]{1,0:T(4,128)S(1)}, f32[4,1024]{1,0:T(4,128)S(1)}, u32[]{:S(2)}, u32[]{:S(2)}) collective-permute-start(f32[4,1024]{1,0:T(4,128)S(1)} %pad_maximum_fusion.4), channel_id=1, source_target_pairs={{0,2},{2,4},{4,6},{6,8},{8,10},{10,12},{12,14},{14,16},{16,18},{18... | collective-permute-start | bytes 49160 | tf_op jit(solution)/shard_map/ppermute | solution.py:33
  16.7 2.7 copy-start.28
  22.5 9.4 %copy-start.27 = (bf16[8,128,128]{2,1,0:T(8,128)(2,1)S(1)}, bf16[8,128,128]{2,1,0:T(8,128)(2,1)}, u32[]{:S(2)}) copy-start(bf16[8,128,128]{2,1,0:T(8,128)(2,1)} %input_w_ref.1) | copy-start | bytes 786436
  22.5 49.1 %all-to-all-start.1 = ((bf16[16,32,2048]{2,1,0:T(8,128)(2,1)}), bf16[16,32,2048]{2,1,0:T(8,128)(2,1)}, u32[]{:S(2)}, u32[]{:S(2)}) async-start(bf16[16,32,2048]{2,1,0:T(8,128)(2,1)} %bitcast.170), calls=%async_computation.1 | async-start | bytes 4194304 | tf_op jit(solution)/shard_map/all_to_all | solution.py:259
  28.7 4.4 %copy-start.7 = (f32[256,1024]{1,0:T(8,128)S(1)}, f32[256,1024]{1,0:T(8,128)}, u32[]{:S(2)}) copy-start(f32[256,1024]{1,0:T(8,128)} %param.26) | copy-start | bytes 3145732
  28.7 4.4 %copy-start.10 = (f32[256,1024]{1,0:T(8,128)S(1)}, f32[256,1024]{1,0:T(8,128)}, u32[]{:S(2)}) copy-start(f32[256,1024]{1,0:T(8,128)} %get-tuple-element.130) | copy-start | bytes 3145732
  37.9 118.9 %copy-start.6 = (f32[256,1024]{1,0:T(8,128)}, f32[256,1024]{1,0:T(8,128)S(1)}, u32[]{:S(2)}) copy-start(f32[256,1024]{1,0:T(8,128)S(1)} %get-tuple-element.87.to_input_ref) | copy-start | bytes 3145732
  71.6 56.5 %all-to-all-start = ((bf16[16,32,2048]{2,1,0:T(8,128)(2,1)}), bf16[16,32,2048]{2,1,0:T(8,128)(2,1)}, u32[]{:S(2)}, u32[]{:S(2)}) async-start(bf16[16,32,2048]{2,1,0:T(8,128)(2,1)} %bitcast.171), calls=%async_computation | async-start | bytes 4194304 | tf_op jit(solution)/shard_map/all_to_all | solution.py:302
  81.6 10.4 %collective-permute-start.2 = (bf16[512,2048]{1,0:T(8,128)(2,1)}, bf16[512,2048]{1,0:T(8,128)(2,1)S(1)}, u32[]{:S(2)}, u32[]{:S(2)}) collective-permute-start(bf16[512,2048]{1,0:T(8,128)(2,1)} %bitcast.23), channel_id=1, source_target_pairs={{0,1},{1,0},{2,3},{3,2},{4,5},{5,4},{6,7},{7,6},{8,9},{9,8},{10,11... | collective-permute-start | bytes 6291464 | tf_op jit(solution)/shard_map/ppermute | solution.py:38
  81.6 46.4 %collective-permute-start.1 = (bf16[256,1024]{1,0:T(8,128)(2,1)}, bf16[256,1024]{1,0:T(8,128)(2,1)}, u32[]{:S(2)}, u32[]{:S(2)}) collective-permute-start(bf16[256,1024]{1,0:T(8,128)(2,1)} %get-tuple-element.110), channel_id=1, source_target_pairs={{0,8},{2,10},{4,12},{6,14},{8,0},{10,2},{12,4},{14,6},{16,24},{18,... | collective-permute-start | bytes 1572872 | tf_op jit(solution)/shard_map/ppermute | solution.py:38
  88.0 4.0 %copy-start.4 = (bf16[1,2048,512]{2,1,0:T(8,128)(2,1)S(1)}, bf16[1,2048,512]{2,1,0:T(8,128)(2,1)}, u32[]{:S(2)}) copy-start(bf16[1,2048,512]{2,1,0:T(8,128)(2,1)} %param.20) | copy-start | bytes 6291460
  128.1 5.5 %copy-start.23 = (f32[512,512]{1,0:T(8,128)S(1)}, f32[512,512]{1,0:T(8,128)}, u32[]{:S(2)}) copy-start(f32[512,512]{1,0:T(8,128)} %fusion.14) | copy-start | bytes 3145732
  128.1 5.5 %copy-start.25 = (f32[512,512]{1,0:T(8,128)S(1)}, f32[512,512]{1,0:T(8,128)}, u32[]{:S(2)}) copy-start(f32[512,512]{1,0:T(8,128)} %fusion.7) | copy-start | bytes 3145732
  128.1 5.5 %copy-start.44 = (bf16[1,512,2048]{2,1,0:T(8,128)(2,1)S(1)}, bf16[1,512,2048]{2,1,0:T(8,128)(2,1)}, u32[]{:S(2)}) copy-start(bf16[1,512,2048]{2,1,0:T(8,128)(2,1)} %param.22) | copy-start | bytes 6291460
  128.1 5.5 %collective-permute-start.3 = (bf16[512,2048]{1,0:T(8,128)(2,1)}, bf16[512,2048]{1,0:T(8,128)(2,1)S(1)}, u32[]{:S(2)}, u32[]{:S(2)}) collective-permute-start(bf16[512,2048]{1,0:T(8,128)(2,1)} %bitcast.26), channel_id=1, source_target_pairs={{0,1},{1,0},{2,3},{3,2},{4,5},{5,4},{6,7},{7,6},{8,9},{9,8},{10,11... | collective-permute-start | bytes 6291464 | tf_op jit(solution)/shard_map/ppermute | solution.py:38
  133.5 5.8 %copy-start.11 = (bf16[512,512]{1,0:T(8,128)(2,1)}, bf16[512,512]{1,0:T(8,128)(2,1)S(1)}, u32[]{:S(2)}) copy-start(bf16[512,512]{1,0:T(8,128)(2,1)S(1)} %get-tuple-element.79) | copy-start | bytes 1572868
  133.6 9.6 %copy-start.19 = (bf16[512,512]{1,0:T(8,128)(2,1)}, bf16[512,512]{1,0:T(8,128)(2,1)S(1)}, u32[]{:S(2)}) copy-start(bf16[512,512]{1,0:T(8,128)(2,1)S(1)} %get-tuple-element.78) | copy-start | bytes 1572868
  133.6 2.7 copy-start.5
  138.9 4.2 %collective-permute-start.4 = (bf16[512,2048]{1,0:T(8,128)(2,1)S(1)}, bf16[512,2048]{1,0:T(8,128)(2,1)S(1)}, u32[]{:S(2)}, u32[]{:S(2)}) collective-permute-start(bf16[512,2048]{1,0:T(8,128)(2,1)S(1)} %add_convert_fusion.4), channel_id=1, source_target_pairs={{0,1},{1,0},{2,3},{3,2},{4,5},{5,4},{6,7},{7,6},{8,9},{9,8},{10,11... | collective-permute-start | bytes 6291464 | tf_op jit(solution)/shard_map/ppermute | solution.py:38
  145.8 17.3 %copy-start.3 = (bf16[512,2048]{1,0:T(8,128)(2,1)S(1)}, bf16[512,2048]{1,0:T(8,128)(2,1)}, u32[]{:S(2)}) copy-start(bf16[512,2048]{1,0:T(8,128)(2,1)} %copy-done.2) | copy-start | bytes 6291460
  145.8 83.9 %all-to-all-start.2 = ((bf16[16,32,2048]{2,1,0:T(8,128)(2,1)}), bf16[16,32,2048]{2,1,0:T(8,128)(2,1)}, u32[]{:S(2)}, u32[]{:S(2)}) async-start(bf16[16,32,2048]{2,1,0:T(8,128)(2,1)} %bitcast.172), calls=%async_computation.2 | async-start | bytes 4194304 | tf_op jit(solution)/shard_map/all_to_all | solution.py:343
  152.4 55.1 %collective-permute-start.5 = (bf16[256,1024]{1,0:T(8,128)(2,1)}, bf16[256,1024]{1,0:T(8,128)(2,1)S(1)}, u32[]{:S(2)}, u32[]{:S(2)}) collective-permute-start(bf16[256,1024]{1,0:T(8,128)(2,1)} %get-tuple-element.110), channel_id=1, source_target_pairs={{0,2},{2,0},{4,6},{6,4},{8,10},{10,8},{12,14},{14,12},{16,18},{18,... | collective-permute-start | bytes 1572872 | tf_op jit(solution)/shard_map/ppermute | solution.py:38
  154.3 60.2 %collective-permute-start.6 = (bf16[256,1024]{1,0:T(8,128)(2,1)}, bf16[256,1024]{1,0:T(8,128)(2,1)}, u32[]{:S(2)}, u32[]{:S(2)}) collective-permute-start(bf16[256,1024]{1,0:T(8,128)(2,1)} %get-tuple-element.110), channel_id=1, source_target_pairs={{0,4},{2,6},{4,0},{6,2},{8,12},{10,14},{12,8},{14,10},{16,20},{18,... | collective-permute-start | bytes 1572872 | tf_op jit(solution)/shard_map/ppermute | solution.py:38
  155.8 58.7 %collective-permute-start.7 = (bf16[256,1024]{1,0:T(8,128)(2,1)}, bf16[256,1024]{1,0:T(8,128)(2,1)}, u32[]{:S(2)}, u32[]{:S(2)}) collective-permute-start(bf16[256,1024]{1,0:T(8,128)(2,1)} %get-tuple-element.110), channel_id=1, source_target_pairs={{0,6},{2,4},{4,2},{6,0},{8,14},{10,12},{12,10},{14,8},{16,22},{18,... | collective-permute-start | bytes 1572872 | tf_op jit(solution)/shard_map/ppermute | solution.py:38
  157.5 8.0 %copy-start.12 = (bf16[512,512]{1,0:T(8,128)(2,1)S(1)}, bf16[512,512]{1,0:T(8,128)(2,1)}, u32[]{:S(2)}) copy-start(bf16[512,512]{1,0:T(8,128)(2,1)} %copy-done.11) | copy-start | bytes 1572868
  157.6 45.7 %collective-permute-start.11 = (f32[3,8,1024]{2,1,0:T(8,128)S(1)}, f32[3,8,1024]{2,1,0:T(8,128)}, u32[]{:S(2)}, u32[]{:S(2)}) collective-permute-start(f32[3,8,1024]{2,1,0:T(8,128)S(1)} %pad_maximum_fusion.2), channel_id=1, source_target_pairs={{2,0},{4,2},{6,4},{8,6},{10,8},{12,10},{14,12},{16,14},{18,16},{20... | collective-permute-start | bytes 294920 | tf_op jit(solution)/shard_map/ppermute | solution.py:33
  159.2 60.1 %collective-permute-start.10 = (bf16[256,1024]{1,0:T(8,128)(2,1)}, bf16[256,1024]{1,0:T(8,128)(2,1)S(1)}, u32[]{:S(2)}, u32[]{:S(2)}) collective-permute-start(bf16[256,1024]{1,0:T(8,128)(2,1)} %collective-permute-done.1), channel_id=1, source_target_pairs={{0,6},{2,4},{4,2},{6,0},{8,14},{10,12},{12,10},{14,8},{16,22},{18,... | collective-permute-start | bytes 1572872 | tf_op jit(solution)/shard_map/ppermute | solution.py:38
  165.5 4.4 %copy-start.14 = (bf16[512,512]{1,0:T(8,128)(2,1)S(1)}, bf16[512,512]{1,0:T(8,128)(2,1)}, u32[]{:S(2)}) copy-start(bf16[512,512]{1,0:T(8,128)(2,1)} %copy-done.13) | copy-start | bytes 1572868
  171.2 37.6 %copy-start.17 = (bf16[512,2048]{1,0:T(8,128)(2,1)S(1)}, bf16[512,2048]{1,0:T(8,128)(2,1)}, u32[]{:S(2)}) copy-start(bf16[512,2048]{1,0:T(8,128)(2,1)} %copy-done.16) | copy-start | bytes 6291460
  171.2 37.5 %copy-start.24 = (f32[512,512]{1,0:T(8,128)S(1)}, f32[512,512]{1,0:T(8,128)}, u32[]{:S(2)}) copy-start(f32[512,512]{1,0:T(8,128)} %fusion.14) | copy-start | bytes 3145732
  171.3 37.5 %copy-start.26 = (f32[512,512]{1,0:T(8,128)S(1)}, f32[512,512]{1,0:T(8,128)}, u32[]{:S(2)}) copy-start(f32[512,512]{1,0:T(8,128)} %fusion.7) | copy-start | bytes 3145732
  175.7 34.5 %copy-start.21 = (bf16[512,512]{1,0:T(8,128)(2,1)S(1)}, bf16[512,512]{1,0:T(8,128)(2,1)}, u32[]{:S(2)}) copy-start(bf16[512,512]{1,0:T(8,128)(2,1)} %get-tuple-element.84) | copy-start | bytes 1572868
  203.3 21.5 %collective-permute-start.8 = (bf16[256,1024]{1,0:T(8,128)(2,1)}, bf16[256,1024]{1,0:T(8,128)(2,1)S(1)}, u32[]{:S(2)}, u32[]{:S(2)}) collective-permute-start(bf16[256,1024]{1,0:T(8,128)(2,1)} %collective-permute-done.1), channel_id=1, source_target_pairs={{0,2},{2,0},{4,6},{6,4},{8,10},{10,8},{12,14},{14,12},{16,18},{18,... | collective-permute-start | bytes 1572872 | tf_op jit(solution)/shard_map/ppermute | solution.py:38
  207.6 2.6 copy-start.29
  207.6 22.2 %collective-permute-start.9 = (bf16[256,1024]{1,0:T(8,128)(2,1)}, bf16[256,1024]{1,0:T(8,128)(2,1)}, u32[]{:S(2)}, u32[]{:S(2)}) collective-permute-start(bf16[256,1024]{1,0:T(8,128)(2,1)} %collective-permute-done.1), channel_id=1, source_target_pairs={{0,4},{2,6},{4,0},{6,2},{8,12},{10,14},{12,8},{14,10},{16,20},{18,... | collective-permute-start | bytes 1572872 | tf_op jit(solution)/shard_map/ppermute | solution.py:38
  232.1 2.7 copy-start.8
  232.1 2.7 collective-permute-start.12
  240.0 12.5 %copy-start.51 = (bf16[256,256]{1,0:T(8,128)(2,1)S(1)}, bf16[256,256]{1,0:T(8,128)(2,1)}, u32[]{:S(2)}) copy-start(bf16[256,256]{1,0:T(8,128)(2,1)} %get-tuple-element.94) | copy-start | bytes 393220
  240.0 14.4 %copy-start.50 = (bf16[256,256]{1,0:T(8,128)(2,1)S(1)}, bf16[256,256]{1,0:T(8,128)(2,1)}, u32[]{:S(2)}) copy-start(bf16[256,256]{1,0:T(8,128)(2,1)} %get-tuple-element.95) | copy-start | bytes 393220
  240.0 17.4 %copy-start.49 = (bf16[256,256]{1,0:T(8,128)(2,1)S(1)}, bf16[256,256]{1,0:T(8,128)(2,1)}, u32[]{:S(2)}) copy-start(bf16[256,256]{1,0:T(8,128)(2,1)} %get-tuple-element.96) | copy-start | bytes 393220
  240.0 20.1 %copy-start.48 = (bf16[256,256]{1,0:T(8,128)(2,1)S(1)}, bf16[256,256]{1,0:T(8,128)(2,1)}, u32[]{:S(2)}) copy-start(bf16[256,256]{1,0:T(8,128)(2,1)} %get-tuple-element.97) | copy-start | bytes 393220
  240.0 22.7 %copy-start.47 = (bf16[256,256]{1,0:T(8,128)(2,1)S(1)}, bf16[256,256]{1,0:T(8,128)(2,1)}, u32[]{:S(2)}) copy-start(bf16[256,256]{1,0:T(8,128)(2,1)} %get-tuple-element.98) | copy-start | bytes 393220
  240.0 25.1 %copy-start.46 = (bf16[256,256]{1,0:T(8,128)(2,1)S(1)}, bf16[256,256]{1,0:T(8,128)(2,1)}, u32[]{:S(2)}) copy-start(bf16[256,256]{1,0:T(8,128)(2,1)} %get-tuple-element.99) | copy-start | bytes 393220
  240.0 25.7 %copy-start.45 = (bf16[256,256]{1,0:T(8,128)(2,1)S(1)}, bf16[256,256]{1,0:T(8,128)(2,1)}, u32[]{:S(2)}) copy-start(bf16[256,256]{1,0:T(8,128)(2,1)} %get-tuple-element.100) | copy-start | bytes 393220
  240.0 34.6 %copy-start.30 = (bf16[256,1024]{1,0:T(8,128)(2,1)S(1)}, bf16[256,1024]{1,0:T(8,128)(2,1)}, u32[]{:S(2)}) copy-start(bf16[256,1024]{1,0:T(8,128)(2,1)} %copy-done.29) | copy-start | bytes 1572868
  249.0 25.0 %all-to-all-start.3 = ((f32[16,2,1024]{2,1,0:T(2,128)}), f32[16,2,1024]{2,1,0:T(2,128)S(1)}, u32[]{:S(2)}, u32[]{:S(2)}) async-start(f32[16,2,1024]{2,1,0:T(2,128)} %get-tuple-element.106), calls=%async_computation.3 | async-start | bytes 262144 | tf_op jit(solution)/shard_map/all_to_all | solution.py:375
  252.5 12.6 %collective-permute-start.13 = (bf16[256,256]{1,0:T(8,128)(2,1)S(1)}, bf16[256,256]{1,0:T(8,128)(2,1)S(1)}, u32[]{:S(2)}, u32[]{:S(2)}) collective-permute-start(bf16[256,256]{1,0:T(8,128)(2,1)S(1)} %copy-done.51), channel_id=1, source_target_pairs={{0,2},{2,0},{4,6},{6,4},{8,10},{10,8},{12,14},{14,12},{16,18},{18,... | collective-permute-start | bytes 393224 | tf_op jit(solution)/shard_map/ppermute | solution.py:38
  254.4 11.3 %collective-permute-start.14 = (bf16[256,256]{1,0:T(8,128)(2,1)S(1)}, bf16[256,256]{1,0:T(8,128)(2,1)S(1)}, u32[]{:S(2)}, u32[]{:S(2)}) collective-permute-start(bf16[256,256]{1,0:T(8,128)(2,1)S(1)} %copy-done.50), channel_id=1, source_target_pairs={{0,4},{2,6},{4,0},{6,2},{8,12},{10,14},{12,8},{14,10},{16,20},{18,... | collective-permute-start | bytes 393224 | tf_op jit(solution)/shard_map/ppermute | solution.py:38
  255.8 6.8 %collective-permute-start.20 = (f32[2,8,1024]{2,1,0:T(8,128)S(1)}, f32[2,8,1024]{2,1,0:T(8,128)S(1)}, u32[]{:S(2)}, u32[]{:S(2)}) collective-permute-start(f32[2,8,1024]{2,1,0:T(8,128)S(1)} %pad_maximum_fusion.3), channel_id=1, source_target_pairs={{2,0},{4,2},{6,4},{8,6},{10,8},{12,10},{14,12},{16,14},{18,16},{20... | collective-permute-start | bytes 196616 | tf_op jit(solution)/shard_map/ppermute | solution.py:33
  257.4 10.6 %collective-permute-start.15 = (bf16[256,256]{1,0:T(8,128)(2,1)S(1)}, bf16[256,256]{1,0:T(8,128)(2,1)S(1)}, u32[]{:S(2)}, u32[]{:S(2)}) collective-permute-start(bf16[256,256]{1,0:T(8,128)(2,1)S(1)} %copy-done.49), channel_id=1, source_target_pairs={{0,6},{2,4},{4,2},{6,0},{8,14},{10,12},{12,10},{14,8},{16,22},{18,... | collective-permute-start | bytes 393224 | tf_op jit(solution)/shard_map/ppermute | solution.py:38
  260.1 7.9 %collective-permute-start.16 = (bf16[256,256]{1,0:T(8,128)(2,1)S(1)}, bf16[256,256]{1,0:T(8,128)(2,1)S(1)}, u32[]{:S(2)}, u32[]{:S(2)}) collective-permute-start(bf16[256,256]{1,0:T(8,128)(2,1)S(1)} %copy-done.48), channel_id=1, source_target_pairs={{0,8},{2,10},{4,12},{6,14},{8,0},{10,2},{12,4},{14,6},{16,24},{18,... | collective-permute-start | bytes 393224 | tf_op jit(solution)/shard_map/ppermute | solution.py:38
  262.7 11.9 %copy-start.42 = (f32[2,8,1024]{2,1,0:T(8,128)}, f32[2,8,1024]{2,1,0:T(8,128)S(1)}, u32[]{:S(2)}) copy-start(f32[2,8,1024]{2,1,0:T(8,128)S(1)} %collective-permute-done.20) | copy-start | bytes 196612
  262.7 7.5 %collective-permute-start.17 = (bf16[256,256]{1,0:T(8,128)(2,1)S(1)}, bf16[256,256]{1,0:T(8,128)(2,1)S(1)}, u32[]{:S(2)}, u32[]{:S(2)}) collective-permute-start(bf16[256,256]{1,0:T(8,128)(2,1)S(1)} %copy-done.47), channel_id=1, source_target_pairs={{0,10},{2,8},{4,14},{6,12},{8,2},{10,0},{12,6},{14,4},{16,26},{18,... | collective-permute-start | bytes 393224 | tf_op jit(solution)/shard_map/ppermute | solution.py:38
  265.1 8.3 %collective-permute-start.18 = (bf16[256,256]{1,0:T(8,128)(2,1)S(1)}, bf16[256,256]{1,0:T(8,128)(2,1)S(1)}, u32[]{:S(2)}, u32[]{:S(2)}) collective-permute-start(bf16[256,256]{1,0:T(8,128)(2,1)S(1)} %copy-done.46), channel_id=1, source_target_pairs={{0,12},{2,14},{4,8},{6,10},{8,4},{10,6},{12,0},{14,2},{16,28},{18,... | collective-permute-start | bytes 393224 | tf_op jit(solution)/shard_map/ppermute | solution.py:38
  265.7 8.3 %collective-permute-start.19 = (bf16[256,256]{1,0:T(8,128)(2,1)S(1)}, bf16[256,256]{1,0:T(8,128)(2,1)S(1)}, u32[]{:S(2)}, u32[]{:S(2)}) collective-permute-start(bf16[256,256]{1,0:T(8,128)(2,1)S(1)} %copy-done.45), channel_id=1, source_target_pairs={{0,14},{2,12},{4,10},{6,8},{8,6},{10,4},{12,2},{14,0},{16,30},{18,... | collective-permute-start | bytes 393224 | tf_op jit(solution)/shard_map/ppermute | solution.py:38
  268.0 6.6 %copy-start.34 = (bf16[256,256]{1,0:T(8,128)(2,1)}, bf16[256,256]{1,0:T(8,128)(2,1)S(1)}, u32[]{:S(2)}) copy-start(bf16[256,256]{1,0:T(8,128)(2,1)S(1)} %collective-permute-done.16) | copy-start | bytes 393220
  270.2 4.4 %copy-start.36 = (bf16[256,256]{1,0:T(8,128)(2,1)}, bf16[256,256]{1,0:T(8,128)(2,1)S(1)}, u32[]{:S(2)}) copy-start(bf16[256,256]{1,0:T(8,128)(2,1)S(1)} %collective-permute-done.17) | copy-start | bytes 393220
  274.6 3.2 %copy-start.32 = (f32[16,2,1024]{2,1,0:T(2,128)}, f32[16,2,1024]{2,1,0:T(2,128)S(1)}, u32[]{:S(2)}) copy-start(f32[16,2,1024]{2,1,0:T(2,128)S(1)} %all-to-all-done.3.ends_ref) | copy-start | bytes 393220
  275.0 2.8 copy-start.35
  276.4 2.8 copy-start.37
  281.4 4.5 %copy-start.43 = (f32[2,8,1024]{2,1,0:T(8,128)S(1)}, f32[2,8,1024]{2,1,0:T(8,128)}, u32[]{:S(2)}) copy-start(f32[2,8,1024]{2,1,0:T(8,128)} %copy-done.42) | copy-start | bytes 196612
  282.8 13.9 %collective-permute-start.21 = (bf16[128,1024]{1,0:T(8,128)(2,1)}, bf16[128,1024]{1,0:T(8,128)(2,1)S(1)}, u32[]{:S(2)}, u32[]{:S(2)}) collective-permute-start(bf16[128,1024]{1,0:T(8,128)(2,1)} %fusion.51), channel_id=1, source_target_pairs={{0,16},{2,18},{4,20},{6,22},{8,24},{10,26},{12,28},{14,30},{16,0},... | collective-permute-start | bytes 786440 | tf_op jit(solution)/shard_map/ppermute | solution.py:38
  288.1 9.5 %copy-start.1 = (bf16[1,2048,512]{2,1,0:T(8,128)(2,1)S(1)}, bf16[1,2048,512]{2,1,0:T(8,128)(2,1)}, u32[]{:S(2)}) copy-start(bf16[1,2048,512]{2,1,0:T(8,128)(2,1)} %param.21) | copy-start | bytes 6291460
  (14 other events, 23.1 us)
where the time goes:
time: 299 us; the launch traced here: 298 us
  waiting for transfers between devices  116 us (39%)
  matrix products  67.1 us (22%)
  starting transfers between devices  65.8 us (22%)
  Pallas kernels  19 us (6%)
  other arithmetic  16.4 us (5%)
  local copies, waits for them, and re-layouts  12.2 us (4%)
    dot_general x43, matrix products, dot(): lax.dot_general(left, right, (contract, ((), ())), preferred_element_type...  67.1 us
    ppermute x19, waiting for transfers between devices, swapped(): return lax.ppermute(value, axis, [(s, s ^ mask) for s in range(count)])  59 us
    ppermute x19, starting transfers between devices, swapped(): return lax.ppermute(value, axis, [(s, s ^ mask) for s in range(count)])  31.5 us
    ppermute x3, waiting for transfers between devices, shifted(): return lax.ppermute(value, axis, pairs)  28.7 us
    all_to_all x1, waiting for transfers between devices, on_device(): lax.all_to_all(send_rows, 'sp', split_axis=0, concat_axis=0, tiled=True)  27.9 us
    all_to_all x1, starting transfers between devices, on_device(): lax.all_to_all(send_grads, 'sp', split_axis=0, concat_axis=0, tiled=True)  9.96 us
    ppermute x3, starting transfers between devices, shifted(): return lax.ppermute(value, axis, pairs)  8.06 us
    pallas_call x1, Pallas kernels, tail_call(): pl.pallas_call(tail_kernel, grid_spec=pltpu.PrefetchScalarGridSpec(num_sc...  7.51 us
  transfers between devices with their start and end apart: 26, of which 13 were waited for; matrix products, arithmetic and copies ran while one was open for 23% of the time, Pallas kernels for 3%

commit v1 on v0

--- a/solution.py
+++ b/solution.py
@@ -1,3 +1,5 @@
+import functools
+
 import jax
 import jax.numpy as jnp
 from jax import lax
@@ -175,40 +177,69 @@
     )(mine, ends, local, cumul, to_decay, to_input, direct, head, head_coef, taps, decay_w, input_w)
 
 
-def combine_kernel(where_ref, mine_ref, other_ref, cot_ref, grad_ref, *piece_refs):
+def combine_kernel(lanes, mine_ref, other_ref, cot_ref, grad_ref, piece_ref):
     total = mine_ref[...].astype(f32) + other_ref[...].astype(f32) + cot_ref[...].astype(f32)
-    grad_ref[...] = total.astype(bf16)
-    group = len(piece_refs)
-    inner = lax.rem(where_ref[0], group)
-    wide = grad_ref.shape[1] // group
-    cut = piece_refs[0].shape[1]
-    lanes = 128
-    outer = cut // lanes
-    assert wide == cut
-    for k, piece_ref in enumerate(piece_refs):
-        for level in range(outer):
-            column = pl.multiple_of((level * group + (inner ^ k)) * lanes, lanes)
-            piece_ref[:, level * lanes : (level + 1) * lanes] = grad_ref[:, pl.ds(column, lanes)]
-
-
-def combine_call(where, mine, other, cotangent, group):
+    total = total.astype(bf16)
+    grad_ref[...] = total
+    group, _, cut = piece_ref.shape
+    for peer in range(group):
+        for level in range(cut // lanes):
+            column = (level * group + peer) * lanes
+            piece_ref[peer, :, level * lanes : (level + 1) * lanes] = total[:, column : column + lanes]
+
+
+def combine_call(mine, other, cotangent, group, lanes):
     rows, width = mine.shape
     block = rows // 4
     cut = width // group
-    wide = pl.BlockSpec((block, width), lambda i, s: (i, 0))
+    wide = pl.BlockSpec((block, width), lambda i: (i, 0))
     return pl.pallas_call(
-        combine_kernel,
+        functools.partial(combine_kernel, lanes),
+        grid=(4,),
+        in_specs=[wide, wide, wide],
+        out_specs=[wide, pl.BlockSpec((group, block, cut), lambda i: (0, i, 0))],
+        out_shape=[
+            jax.ShapeDtypeStruct((rows, width), bf16),
+            jax.ShapeDtypeStruct((group, rows, cut), bf16),
+        ],
+        cost_estimate=pl.CostEstimate(flops=1 << 28, bytes_accessed=5 << 20, transcendentals=0),
+        name="combine",
+    )(mine, other, cotangent)
+
+
+def product_kernel(level_ref, *refs):
+    count = len(refs) // 2
+    out_refs = refs[2 * count :]
+    total = rows_of(refs[0][0], refs[count][...])
+    for k in range(1, count):
+        total = total + rows_of(refs[k][0], refs[count + k][...])
+    full_ref = out_refs[0]
+    full_ref[...] = total
+
+
+def product_call(where, grads, mixers):
+    group, rows, cut = grads.shape
+    channels = mixers[0].shape[1]
+    block = channels // 4
+
+    def grad_spec(k):
+        return pl.BlockSpec((1, rows, cut), lambda i, s: (jnp.bitwise_xor(lax.rem(s[0], group), k), 0, 0))
+
+    return pl.pallas_call(
+        product_kernel,
         grid_spec=pltpu.PrefetchScalarGridSpec(
             num_scalar_prefetch=1,
-            grid=(4,),
-            in_specs=[wide, wide, wide],
-            out_specs=[wide] + [pl.BlockSpec((block, cut), lambda i, s: (i, 0))] * group,
-        ),
-        out_shape=[jax.ShapeDtypeStruct((rows, width), bf16)]
-        + [jax.ShapeDtypeStruct((rows, cut), bf16)] * group,
-        cost_estimate=pl.CostEstimate(flops=1 << 28, bytes_accessed=5 << 20, transcendentals=0),
-        name="combine",
-    )(where, mine, other, cotangent)
+            grid=(channels // block,),
+            in_specs=[grad_spec(k) for k in range(group)]
+            + [pl.BlockSpec((rows, block), lambda i, s: (0, i))] * group,
+            out_specs=[pl.BlockSpec((cut, block), lambda i, s: (0, i))],
+        ),
+        out_shape=[jax.ShapeDtypeStruct((cut, channels), f32)],
+        cost_estimate=pl.CostEstimate(
+            flops=2 * group * rows * cut * channels, bytes_accessed=6 << 20, transcendentals=0
+        ),
+        name="product",
+    )(where, *([grads] * group), *mixers)[0]
 
 
 def on_device(
@@ -250,14 +281,14 @@
     slot_ids = (slot_iota // share) * capacity + core * share + slot_iota % share
     hits = slot_ids[:, None, None] == pair_slots[None, :, :]
     placing = jnp.any(hits, axis=2).astype(bf16)
-    slot_weight = jnp.sum(jnp.where(hits, route_weight[None, :, :], 0.0), axis=(1, 2))
     send_rows = times(placing, moe_input).astype(bf16).reshape(experts, share, width)
+    late = (gate_input, states, recur_input, cotangent, route_weight)
+    send_rows, late = lax.optimization_barrier((send_rows, late))
+    gate_input, states, recur_input, cotangent_late, route_weight = late
+    got_rows = lax.all_to_all(send_rows, "sp", split_axis=0, concat_axis=0, tiled=True)
     edge = jnp.concatenate([recur_input[-3:].astype(f32), states[-1:]], axis=0)
     edge = shifted(edge, "sp", 1)
-    edge, send_rows, late = lax.optimization_barrier((edge, send_rows, (gate_input, states, cotangent)))
-    gate_input, states, cotangent_late = late
-    got_rows = lax.all_to_all(send_rows, "sp", split_axis=0, concat_axis=0, tiled=True)
-
+    slot_weight = jnp.sum(jnp.where(hits, route_weight[None, :, :], 0.0), axis=(1, 2))
     send_grads = times(placing, cotangent_late) * slot_weight[:, None]
     send_grads = send_grads.astype(bf16).reshape(experts, share, width)
 
@@ -265,6 +296,17 @@
     gelu_value, gelu_back = jax.vjp(jax.nn.gelu, gate_float)
     slope = states * gelu_back(jnp.ones_like(gate_float))[0]
     mixer_out = (states * gelu_value).astype(bf16)
+    half = group // 2
+    mixers = {0: mixer_out}
+    mixers[half] = swapped(mixer_out, "sp", half)
+    for k in range(1, half):
+        mixers[k] = swapped(mixer_out, "sp", k)
+    send_grads, mixers[half], gelu_value, slope, edge, got_rows = lax.optimization_barrier(
+        (send_grads, mixers[half], gelu_value, slope, edge, got_rows)
+    )
+    got_grads = lax.all_to_all(send_grads, "sp", split_axis=0, concat_axis=0, tiled=True)
+    for k in range(1, half):
+        mixers[k ^ half] = swapped(mixers[half], "sp", k)
     extended = jnp.concatenate([edge[:3], recur_input.astype(f32)], axis=0)
     prev_state = edge[3:]
     taps = conv_taps.astype(f32)
@@ -295,29 +337,19 @@
     to_input = mult * conv * input_gate * (1.0 - input_gate)
     direct = mult * input_gate
 
-    statics = (gelu_value, slope, mixer_out, next_decay, decay_value[:1], to_decay, to_input, direct)
-    statics, send_grads = lax.optimization_barrier((statics, send_grads))
-    gelu_value, slope, mixer_out, next_decay, first_decay, to_decay, to_input, direct = statics
-
-    got_grads = lax.all_to_all(send_grads, "sp", split_axis=0, concat_axis=0, tiled=True)
     rows_here = got_rows.reshape(own_slots, width)
     rows_there = swapped(rows_here, "tp", 1)
-    head_coef = shifted(jnp.stack([to_decay[:8], to_input[:8], direct[:8]]), "sp", -1)
-    mixers = {0: mixer_out}
-    half = group // 2
-    mixers[half] = swapped(mixer_out, "sp", half)
     weight_gate = gate_proj[0]
     weight_up = up_proj[0]
     weight_down = down_proj[0]
     pres = tuple(
         (times(rows, weight_gate), times(rows, weight_up)) for rows in (rows_here, rows_there)
     )
-    got_grads, mixers[half], pres, rows_there = lax.optimization_barrier(
-        (got_grads, mixers[half], pres, rows_there)
-    )
-    for k in range(1, half):
-        mixers[k] = swapped(mixer_out, "sp", k)
-        mixers[k ^ half] = swapped(mixers[half], "sp", k)
+    gates = (next_decay, decay_value[:1], to_decay, to_input, direct)
+    got_grads, mixers, pres, rows_there, gates = lax.optimization_barrier(
+        (got_grads, mixers, pres, rows_there, gates)
+    )
+    next_decay, first_decay, to_decay, to_input, direct = gates
     grads_here = got_grads.reshape(own_slots, width)
     grads_there = swapped(grads_here, "tp", 1)
 
@@ -341,42 +373,29 @@
     partial_h = cols_of(gate_h, weight_gate) + cols_of(up_h, weight_up)
     shared = (partial_h + from_there.astype(f32)).astype(bf16).reshape(experts, share, width)
     back = lax.all_to_all(shared, "sp", split_axis=0, concat_axis=0, tiled=True)
+    head_coef = shifted(jnp.stack([to_decay[:8], to_input[:8], direct[:8]]), "sp", -1)
     down_grad = rows_of(hidden_h, grads_here) + rows_of(hidden_t, grads_there)
     gate_weight_grad = rows_of(rows_here, gate_h) + rows_of(rows_there, gate_t)
     up_weight_grad = rows_of(rows_here, up_h) + rows_of(rows_there, up_t)
     weight_grads = (gate_weight_grad.astype(bf16), up_weight_grad.astype(bf16), down_grad.astype(bf16))
-    back, weight_grads, mixers, head_coef = lax.optimization_barrier(
-        (back, weight_grads, mixers, head_coef)
-    )
+    back, weight_grads, head_coef = lax.optimization_barrier((back, weight_grads, head_coef))
 
     mine_back = rows_of(placing, back.reshape(own_slots, width)).astype(bf16)
     other_back = swapped(mine_back, "tp", 1)
     out_rows = width // experts
     where = place[None].astype(jnp.int32)
-    if out_rows % 128 == 0:
-        input_grad, *pieces = combine_call(where, mine_back, other_back, cotangent, group)
-    else:
-        input_grad = (
-            mine_back.astype(f32) + other_back.astype(f32) + cotangent.astype(f32)
-        ).astype(bf16)
-        split_grad = input_grad.reshape(tok_rows, outer, group, out_rows)
-        pieces = [
-            lax.dynamic_slice_in_dim(split_grad, place % group ^ k, 1, 2).reshape(tok_rows, -1)
-            for k in range(group)
-        ]
-
-    grads = [pieces[0]]
-    for k in range(1, group):
-        grads.append(swapped(pieces[k], "sp", k))
+    input_grad, pieces = combine_call(mine_back, other_back, cotangent, group, out_rows)
+
+    groups = [[base + peer for peer in range(group)] for base in range(0, experts, group)]
+    grads = lax.all_to_all(
+        pieces, "sp", split_axis=0, concat_axis=0, tiled=True, axis_index_groups=groups
+    )
     gate_grad, local, cumul, ends = mixer_call(
         input_grad, out_weight, gelu_value, slope, next_decay, first_decay, experts
     )
     head = shifted(jnp.stack([local[:8], cumul[:8]]), "sp", -1)
     ends = lax.all_to_all(ends, "sp", split_axis=0, concat_axis=0, tiled=True)
-    grads, ends, head = lax.optimization_barrier((grads, ends, head))
-    product = rows_of(grads[0], mixers[0])
-    for k in range(1, group):
-        product = product + rows_of(grads[k], mixers[k])
+    product = product_call(where, grads, [mixers[k] for k in range(group)])
     product = product.reshape(outer, out_rows, channels)
     level = place // group
 

time: 299 us -> 260 us (0.87)
  waiting for transfers between devices: 116 us -> 91.5 us
  matrix products: 67.1 us -> 55.5 us
  starting transfers between devices: 65.8 us -> 56.8 us
  Pallas kernels: 19 us -> 24.4 us
    all_to_all x1, waiting for transfers between devices: 27.9 us -> 0.01 us  [on_device(): lax.all_to_all(send_rows, 'sp', split_axis=0, concat_axis=0, tiled=True)]
    ppermute x19 -> x12, waiting for transfers between devices: 59 us -> 32.4 us  [swapped(): return lax.ppermute(value, axis, [(s, s ^ mask) for s in range(count)])]
    all_to_all x1, waiting for transfers between devices: 0.01 us -> 21.3 us  [on_device(): back = lax.all_to_all(shared, 'sp', split_axis=0, concat_axis=0, tiled=True)]
    ppermute x19 -> x12, starting transfers between devices: 31.5 us -> 12.4 us  [swapped(): return lax.ppermute(value, axis, [(s, s ^ mask) for s in range(count)])]
    dot_general x43 -> x35, matrix products: 67.1 us -> 55.5 us  [dot(): lax.dot_general(left, right, (contract, ((), ())), preferred_element_type...]
    all_to_all x0 -> x1, starting transfers between devices: none -> 11.2 us  [on_device(): lax.all_to_all(pieces, 'sp', split_axis=0, concat_axis=0, tiled=True, axi...]
    pallas_call x1 -> x2, Pallas kernels: 4.15 us -> 9.64 us  [the longest x1 5.57 us: product_call(): pl.pallas_call(product_kernel, grid_spec=pltpu.PrefetchScalarGridSpec(num...]
    all_to_all x0 -> x1, waiting for transfers between devices: none -> 5.21 us  [on_device(): lax.all_to_all(pieces, 'sp', split_axis=0, concat_axis=0, tiled=True, axi...]
  transfers between devices with their start and end apart: 26 -> 20, of which waited for: 13 -> 9; matrix products, arithmetic and copies ran while one was open for 23% -> 24% of each run, Pallas kernels for 3% -> 8%
where the time goes in v1:
time: 260 us; the launch traced here: 258 us
  waiting for transfers between devices  91.5 us (35%)
  starting transfers between devices  56.8 us (22%)
  matrix products  55.5 us (21%)
  Pallas kernels  24.4 us (9%)
  local copies, waits for them, and re-layouts  14.7 us (6%)
  other arithmetic  13.8 us (5%)
    dot_general x35, matrix products, dot(): lax.dot_general(left, right, (contract, ((), ())), preferred_element_type...  55.5 us
    ppermute x3, waiting for transfers between devices, shifted(): return lax.ppermute(value, axis, pairs)  32.5 us
    ppermute x12, waiting for transfers between devices, swapped(): return lax.ppermute(value, axis, [(s, s ^ mask) for s in range(count)])  32.4 us
    all_to_all x1, waiting for transfers between devices, on_device(): back = lax.all_to_all(shared, 'sp', split_axis=0, concat_axis=0, tiled=True)  21.3 us
    ppermute x12, starting transfers between devices, swapped(): return lax.ppermute(value, axis, [(s, s ^ mask) for s in range(count)])  12.4 us
    all_to_all x1, starting transfers between devices, on_device(): lax.all_to_all(pieces, 'sp', split_axis=0, concat_axis=0, tiled=True, axi...  11.2 us
    all_to_all x1, starting transfers between devices, on_device(): lax.all_to_all(send_rows, 'sp', split_axis=0, concat_axis=0, tiled=True)  8.52 us
    all_to_all x1, starting transfers between devices, on_device(): lax.all_to_all(send_grads, 'sp', split_axis=0, concat_axis=0, tiled=True)  7.79 us
  transfers between devices with their start and end apart: 20, of which 9 were waited for; matrix products, arithmetic and copies ran while one was open for 24% of the time, Pallas kernels for 8%

profile of v1, /device:TPU:0, one launch (start us, length us, event | category | flops | bytes accessed | tf_op | source)
XLA Modules:
  0.0 258.1 jit_solution(12784336291664349334)
XLA Ops:
  0.7 1.0 copy.85
  1.9 1.2 reduce-window.6
  3.7 0.7 multiply_add_fusion.1
  4.5 3.3 %convolution_convert_fusion = bf16[512,2048]{1,0:T(8,128)(2,1)} fusion(pred[512,256]{1,0:T(8,128)(4,1)S(1)} %compare_reduce_fusion, bf16[256,2048]{1,0:T(8,128)(2,1)} %param.16), kind=kOutput, calls=%fused_computation.6 | convolution fusion | flops 537919488 | bytes 3276800 | tf_op jit(solution)/shard_map/dot_general | solution.py:17
  7.8 8.5 %all-to-all-start = ((bf16[16,32,2048]{2,1,0:T(8,128)(2,1)}), bf16[16,32,2048]{2,1,0:T(8,128)(2,1)}, u32[]{:S(2)}, u32[]{:S(2)}) async-start(bf16[16,32,2048]{2,1,0:T(8,128)(2,1)} %bitcast.155), calls=%async_computation | async-start | bytes 4194304 | tf_op jit(solution)/shard_map/all_to_all | solution.py:288
  16.4 3.2 %fusion.22 = (f32[256,1024]{1,0:T(8,128)}, bf16[256,1024]{1,0:T(8,128)(2,1)}, f32[256,1024]{1,0:T(8,128)}) fusion(f32[256,1024]{1,0:T(8,128)S(1)} %copy-done.8, bf16[256,1024]{1,0:T(8,128)(2,1)} %param.25), kind=kLoop, calls=%fused_computation.56 | loop fusion | flops 5767168 | bytes 4194304 | tf_op jit(solution)/shard_map/mul | solution.py:297
  19.5 2.8 %collective-permute-start.4 = (bf16[256,1024]{1,0:T(8,128)(2,1)}, bf16[256,1024]{1,0:T(8,128)(2,1)}, u32[]{:S(2)}, u32[]{:S(2)}) collective-permute-start(bf16[256,1024]{1,0:T(8,128)(2,1)} %get-tuple-element.81.refs_8_), channel_id=1, source_target_pairs={{0,6},{2,4},{4,2},{6,0},{8,14},{10,12},{12,10},{14,8},{16,22},{18,... | collective-permute-start | bytes 1572872 | tf_op jit(solution)/shard_map/ppermute | solution.py:40
  23.0 1.9 collective-permute-start
  24.9 0.7 slice_convert_fusion
  25.6 3.4 %collective-permute-start.1 = (f32[4,1024]{1,0:T(4,128)S(1)}, f32[4,1024]{1,0:T(4,128)S(1)}, u32[]{:S(2)}, u32[]{:S(2)}) collective-permute-start(f32[4,1024]{1,0:T(4,128)S(1)} %pad_maximum_fusion.4), channel_id=1, source_target_pairs={{0,2},{2,4},{4,6},{6,8},{8,10},{10,12},{12,14},{14,16},{16,18},{18... | collective-permute-start | bytes 49160 | tf_op jit(solution)/shard_map/ppermute | solution.py:35
  29.9 3.3 %multiply_convert_fusion = bf16[512,2048]{1,0:T(8,128)(2,1)} fusion(pred[512,256]{1,0:T(8,128)(4,1)S(1)} %compare_reduce_fusion, bf16[256,2048]{1,0:T(8,128)(2,1)} %cot_ref.1, f32[512]{0:T(512)S(1)} %fusion.19), kind=kOutput, calls=%fused_computation.5 | convolution fusion | flops 538968064 | bytes 3278848 | tf_op jit(solution)/shard_map/dot_general | solution.py:17
  33.7 1.1 convert_element_type.88
  34.9 32.5 %collective-permute-done.1 = f32[4,1024]{1,0:T(4,128)S(1)} collective-permute-done((f32[4,1024]{1,0:T(4,128)S(1)}, f32[4,1024]{1,0:T(4,128)S(1)}, u32[]{:S(2)}, u32[]{:S(2)}) %collective-permute-start.1) | collective-permute-done | bytes 16416 | tf_op jit(solution)/shard_map/ppermute | solution.py:35
  68.0 7.8 %all-to-all-start.1 = ((bf16[16,32,2048]{2,1,0:T(8,128)(2,1)}), bf16[16,32,2048]{2,1,0:T(8,128)(2,1)}, u32[]{:S(2)}, u32[]{:S(2)}) async-start(bf16[16,32,2048]{2,1,0:T(8,128)(2,1)} %bitcast.154), calls=%async_computation.1 | async-start | bytes 4194304 | tf_op jit(solution)/shard_map/all_to_all | solution.py:307
  75.8 2.7 %collective-permute-start.7 = (bf16[256,1024]{1,0:T(8,128)(2,1)}, bf16[256,1024]{1,0:T(8,128)(2,1)}, u32[]{:S(2)}, u32[]{:S(2)}) collective-permute-start(bf16[256,1024]{1,0:T(8,128)(2,1)} %collective-permute-done.refs_12_), channel_id=1, source_target_pairs={{0,6},{2,4},{4,2},{6,0},{8,14},{10,12},{12,10},{14,8},{16,22},{18,... | collective-permute-start | bytes 1572872 | tf_op jit(solution)/shard_map/ppermute | solution.py:40
  78.5 1.3 fusion.111
  82.3 3.1 %subtract_multiply_fusion = (f32[256,1024]{1,0:T(8,128)S(1)}, f32[256,1024]{1,0:T(8,128)}, f32[256,1024]{1,0:T(8,128)}, f32[256,1024]{1,0:T(8,128)S(1)}) fusion(f32[256,1024]{1,0:T(8,128)S(1)} %get-tuple-element.100, f32[256,1024]{1,0:T(8,128)S(1)} %convolution_dynamic-update-slice_fusion, f32[256,1024]{1,0:T(8,128)S(1)} %copy-done.23, ...), kind=kLoop, calls=%fused_computation.87 | loop fusion | flops 7340032 | bytes 9441536 | tf_op jit(solution)/shard_map/mul | solution.py:337
  85.4 4.2 %fusion.9 = f32[512,512]{1,0:T(8,128)} fusion(bf16[512,2048]{1,0:T(8,128)(2,1)} %bitcast.3, bf16[1,2048,512]{2,1,0:T(8,128)(2,1)S(1)} %copy-done), kind=kOutput, calls=%fused_computation.17 | convolution fusion | flops 1073741824 | bytes 5242880 | tf_op jit(solution)/shard_map/dot_general | solution.py:17
  90.3 1.1 concatenate.24.next_ref
  91.4 0.8 copy-done.5
  92.2 3.8 %fusion.16 = f32[512,512]{1,0:T(8,128)} fusion(bf16[512,2048]{1,0:T(8,128)(2,1)} %bitcast.3, bf16[1,2048,512]{2,1,0:T(8,128)(2,1)S(1)} %copy-done.5), kind=kOutput, calls=%fused_computation.24 | convolution fusion | flops 1073741824 | bytes 5242880 | tf_op jit(solution)/shard_map/dot_general | solution.py:17
  96.9 2.2 fusion.7
  99.1 2.2 fusion.14
  101.4 9.7 %collective-permute-done.7.refs_15_ = bf16[256,1024]{1,0:T(8,128)(2,1)} collective-permute-done((bf16[256,1024]{1,0:T(8,128)(2,1)}, bf16[256,1024]{1,0:T(8,128)(2,1)}, u32[]{:S(2)}, u32[]{:S(2)}) %collective-permute-start.7) | collective-permute-done | bytes 524320 | tf_op jit(solution)/shard_map/ppermute | solution.py:40
  111.1 10.7 %collective-permute-done.6.refs_14_ = bf16[256,1024]{1,0:T(8,128)(2,1)} collective-permute-done((bf16[256,1024]{1,0:T(8,128)(2,1)}, bf16[256,1024]{1,0:T(8,128)(2,1)}, u32[]{:S(2)}, u32[]{:S(2)}) %collective-permute-start.6) | collective-permute-done | bytes 524320 | tf_op jit(solution)/shard_map/ppermute | solution.py:40
  121.8 4.7 %collective-permute-done.5.refs_13_ = bf16[256,1024]{1,0:T(8,128)(2,1)} collective-permute-done((bf16[256,1024]{1,0:T(8,128)(2,1)}, bf16[256,1024]{1,0:T(8,128)(2,1)}, u32[]{:S(2)}, u32[]{:S(2)}) %collective-permute-start.5) | collective-permute-done | bytes 524320 | tf_op jit(solution)/shard_map/ppermute | solution.py:40
  126.7 5.4 %multiply_convert_fusion.4 = (bf16[512,512]{1,0:T(8,128)(2,1)S(1)}, bf16[512,512]{1,0:T(8,128)(2,1)S(1)}, bf16[512,512]{1,0:T(8,128)(2,1)}) fusion(f32[512,512]{1,0:T(8,128)} %fusion.16, f32[512,512]{1,0:T(8,128)} %fusion.9, bf16[512,2048]{1,0:T(8,128)(2,1)} %bitcast.26, bf16[1,512,2048]{2,1,0:T(8,128)(2,1)} %param.22), kind=kOutput, calls=%fused_computation.82 | convolution fusion | flops 1077673984 | bytes 7864320 | tf_op jit(solution)/shard_map/dot_general | solution.py:17
  132.1 1.6 multiply_convert_fusion.2
  133.8 1.2 copy-done.6
  135.0 1.3 fusion.11
  136.3 1.3 add_convert_fusion.4
  138.1 1.5 fusion.5
  139.6 2.3 collective-permute-done.10
  141.9 2.7 %add_convert_fusion.3 = bf16[512,2048]{1,0:T(8,128)(2,1)} fusion(bf16[512,2048]{1,0:T(8,128)(2,1)S(1)} %collective-permute-done.10, f32[512,2048]{1,0:T(8,128)S(1)} %fusion.5, bf16[512,512]{1,0:T(8,128)(2,1)S(1)} %get-tuple-element.66, bf16[1,2048,512]{2,1,0:T(8,128)(2,1)S(1)} %copy-done.6), kind=kOutput, calls=%fused_computation.3 | convolution fusion | flops 1077936128 | bytes 11010048 | tf_op jit(solution)/shard_map/dot_general | solution.py:17
  144.5 6.4 %all-to-all-start.2 = ((bf16[16,32,2048]{2,1,0:T(8,128)(2,1)}), bf16[16,32,2048]{2,1,0:T(8,128)(2,1)}, u32[]{:S(2)}, u32[]{:S(2)}) async-start(bf16[16,32,2048]{2,1,0:T(8,128)(2,1)} %bitcast.156), calls=%async_computation.2 | async-start | bytes 4194304 | tf_op jit(solution)/shard_map/all_to_all | solution.py:375
  151.0 0.8 slice_bitcast_fusion.5
  151.7 0.8 slice_bitcast_fusion.3
  152.5 1.4 collective-permute-start.11
  154.0 2.3 fusion.116
  156.4 1.3 fusion.115
  158.5 1.3 fusion.43
  159.9 4.4 %add_convert_fusion.1 = bf16[2048,512]{1,0:T(8,128)(2,1)} fusion(f32[2048,512]{1,0:T(8,128)S(1)} %fusion.116, bf16[512,2048]{1,0:T(8,128)(2,1)} %bitcast.3, bf16[512,512]{1,0:T(8,128)(2,1)S(1)} %copy-done.12), kind=kOutput, calls=%fused_computation.1 | convolution fusion | flops 1075838976 | bytes 8912896 | tf_op jit(solution)/shard_map/dot_general | solution.py:17
  164.2 4.4 %add_convert_fusion.2 = bf16[2048,512]{1,0:T(8,128)(2,1)} fusion(f32[2048,512]{1,0:T(8,128)S(1)} %fusion.115, bf16[512,2048]{1,0:T(8,128)(2,1)} %bitcast.3, bf16[512,512]{1,0:T(8,128)(2,1)S(1)} %copy-done.20), kind=kOutput, calls=%fused_computation.2 | convolution fusion | flops 1075838976 | bytes 8912896 | tf_op jit(solution)/shard_map/dot_general | solution.py:17
  168.6 4.3 %add_convert_fusion = bf16[512,2048]{1,0:T(8,128)(2,1)} fusion(f32[512,2048]{1,0:T(8,128)S(1)} %fusion.43, bf16[512,512]{1,0:T(8,128)(2,1)S(1)} %copy-done.21, bf16[512,2048]{1,0:T(8,128)(2,1)} %bitcast.26), kind=kOutput, calls=%fused_computation | convolution fusion | flops 1075838976 | bytes 8912896 | tf_op jit(solution)/shard_map/dot_general | solution.py:17
  172.9 21.3 %all-to-all-done.2 = bf16[16,32,2048]{2,1,0:T(8,128)(2,1)} async-done(((bf16[16,32,2048]{2,1,0:T(8,128)(2,1)}), bf16[16,32,2048]{2,1,0:T(8,128)(2,1)}, u32[]{:S(2)}, u32[]{:S(2)}) %all-to-all-start.2) | async-done | bytes 2097184 | tf_op jit(solution)/shard_map/all_to_all | solution.py:375
  194.2 2.3 convolution_convert_fusion.1.mine_ref
  196.7 2.6 %collective-permute-done.12.other_ref = bf16[256,2048]{1,0:T(8,128)(2,1)S(1)} collective-permute-done((bf16[256,2048]{1,0:T(8,128)(2,1)S(1)}, bf16[256,2048]{1,0:T(8,128)(2,1)S(1)}, u32[]{:S(2)}, u32[]{:S(2)}) %collective-permute-start.12) | collective-permute-done | bytes 1048608 | tf_op jit(solution)/shard_map/ppermute | solution.py:40
  199.3 1.0 copy-done.22
  200.3 4.1 %combine.1 = (bf16[256,2048]{1,0:T(8,128)(2,1)}, bf16[8,256,256]{2,1,0:T(8,128)(2,1)}) custom-call(bf16[256,2048]{1,0:T(8,128)(2,1)} %copy-done.10, bf16[256,2048]{1,0:T(8,128)(2,1)} %copy-done.22, bf16[256,2048]{1,0:T(8,128)(2,1)} %cot_ref.1), custom_call_target="tpu_custom_call" | custom-call | flops 268435456 | bytes 5242880 | tf_op jit(solution)/shard_map/combine/pallas_call | solution.py:196
  204.4 11.2 %all-to-all-start.3 = ((bf16[8,256,256]{2,1,0:T(8,128)(2,1)}), bf16[8,256,256]{2,1,0:T(8,128)(2,1)S(1)}, u32[]{:S(2)}, u32[]{:S(2)}) async-start(bf16[8,256,256]{2,1,0:T(8,128)(2,1)} %get-tuple-element.80), calls=%async_computation.3 | async-start | bytes 2097152 | tf_op jit(solution)/shard_map/all_to_all | solution.py:390
  215.5 7.2 %mixer.1 = (bf16[256,1024]{1,0:T(8,128)(2,1)}, f32[256,1024]{1,0:T(8,128)}, f32[256,1024]{1,0:T(8,128)}, f32[16,2,1024]{2,1,0:T(2,128)}) custom-call(bf16[256,2048]{1,0:T(8,128)(2,1)} %get-tuple-element.50.grad_ref, bf16[2048,1024]{1,0:T(8,128)(2,1)} %weight_ref.1, f32[256,1024]{1,0:T(8,128)} %get-tuple-element.90.gelu_ref, ...), custom_call_target="tpu_custom_call" | custom-call | flops 1073741824 | bytes 8388608 | tf_op jit(solution)/shard_map/mixer/pallas_call | solution.py:92
  222.8 0.8 slice_bitcast_fusion.2
  223.5 0.8 slice_bitcast_fusion.1
  224.3 1.3 collective-permute-start.14
  225.6 5.2 %all-to-all-done.3.refs_0_.refs_1_.refs_2_.refs_3_.refs_4_.refs_5_.refs_6_.refs_7_ = bf16[8,256,256]{2,1,0:T(8,128)(2,1)S(1)} async-done(((bf16[8,256,256]{2,1,0:T(8,128)(2,1)}), bf16[8,256,256]{2,1,0:T(8,128)(2,1)S(1)}, u32[]{:S(2)}, u32[]{:S(2)}) %all-to-all-start.3) | async-done | bytes 1048608 | tf_op jit(solution)/shard_map/all_to_all | solution.py:390
  230.8 4.5 %all-to-all-start.4 = ((f32[16,2,1024]{2,1,0:T(2,128)}), f32[16,2,1024]{2,1,0:T(2,128)S(1)}, u32[]{:S(2)}, u32[]{:S(2)}) async-start(f32[16,2,1024]{2,1,0:T(2,128)} %get-tuple-element.94), calls=%async_computation.4 | async-start | bytes 262144 | tf_op jit(solution)/shard_map/all_to_all | solution.py:397
  235.3 5.6 %product.1 = f32[256,1024]{1,0:T(8,128)} custom-call(s32[1]{0:T(128)} %bitcast.35.level_ref.where_ref, bf16[8,256,256]{2,1,0:T(8,128)(2,1)} %copy-done.2, bf16[8,256,256]{2,1,0:T(8,128)(2,1)} %copy-done.2, bf16[8,256,256]{2,1,0:T(8,128)(2,1)} %copy-done.2, bf16[8,256,256]{2,1,0:T(8,128)(2,1)} %copy-done.2, bf16[8,256,256]{2,1,0:T(8,128)(2,1)} %copy-done.2, ...), custom_call_target="tpu_custom_call" | custom-call | flops 1073741824 | bytes 6291456 | tf_op jit(solution)/shard_map/product/pallas_call | solution.py:228
  240.9 1.8 fusion.45
  242.7 2.8 %collective-permute-start.13 = (bf16[128,1024]{1,0:T(8,128)(2,1)}, bf16[128,1024]{1,0:T(8,128)(2,1)S(1)}, u32[]{:S(2)}, u32[]{:S(2)}) collective-permute-start(bf16[128,1024]{1,0:T(8,128)(2,1)} %fusion.45), channel_id=1, source_target_pairs={{0,16},{2,18},{4,20},{6,22},{8,24},{10,26},{12,28},{14,30},{16,0},... | collective-permute-start | bytes 786440 | tf_op jit(solution)/shard_map/ppermute | solution.py:40
  246.1 0.7 pad_maximum_fusion.1.head_coef_ref
  246.8 0.7 copy-done.30
  247.4 7.5 %tail.1 = bf16[256,1024]{1,0:T(8,128)(2,1)} custom-call(s32[1]{0:T(128)} %bitcast.35.level_ref.where_ref, f32[16,2,1024]{2,1,0:T(2,128)} %copy-done.30, f32[256,1024]{1,0:T(8,128)} %get-tuple-element.95.local_ref, f32[256,1024]{1,0:T(8,128)} %get-tuple-element.96.cumul_ref, f32[256,1024]{1,0:T(8,128)} %get-tuple-element.73.to_decay_ref, ...), custom_call_target="tpu_custom_call" | custom-call | flops 268435456 | bytes 7340032 | tf_op jit(solution)/shard_map/tail/pallas_call | solution.py:156
  254.9 2.3 collective-permute-done.13
  257.3 0.9 bitcast_add_fusion
  (130 shorter events, 9.9 us)
Async XLA Ops:
  0.6 84.8 %copy-start = (bf16[1,2048,512]{2,1,0:T(8,128)(2,1)S(1)}, bf16[1,2048,512]{2,1,0:T(8,128)(2,1)}, u32[]{:S(2)}) copy-start(bf16[1,2048,512]{2,1,0:T(8,128)(2,1)} %param.21) | copy-start | bytes 6291460
  7.8 8.5 %copy-start.8 = (f32[256,1024]{1,0:T(8,128)S(1)}, f32[256,1024]{1,0:T(8,128)}, u32[]{:S(2)}) copy-start(f32[256,1024]{1,0:T(8,128)} %param.26) | copy-start | bytes 3145732
  7.8 59.6 %all-to-all-start = ((bf16[16,32,2048]{2,1,0:T(8,128)(2,1)}), bf16[16,32,2048]{2,1,0:T(8,128)(2,1)}, u32[]{:S(2)}, u32[]{:S(2)}) async-start(bf16[16,32,2048]{2,1,0:T(8,128)(2,1)} %bitcast.155), calls=%async_computation | async-start | bytes 4194304 | tf_op jit(solution)/shard_map/all_to_all | solution.py:288
  16.3 12.7 %copy-start.34 = (f32[1024]{0:T(1024)S(1)}, f32[1024]{0:T(1024)}, u32[]{:S(2)}) copy-start(f32[1024]{0:T(1024)} %param.30) | copy-start | bytes 12292
  16.4 12.7 %copy-start.31 = (bf16[4,1024]{1,0:T(4,128)(2,1)S(1)}, bf16[4,1024]{1,0:T(4,128)(2,1)}, u32[]{:S(2)}) copy-start(bf16[4,1024]{1,0:T(4,128)(2,1)} %taps_ref.1) | copy-start | bytes 24580
  16.4 13.3 %copy-start.35 = (f32[256,2]{0,1:T(2,128)S(1)}, f32[256,2]{0,1:T(2,128)}, u32[]{:S(2)}) copy-start(f32[256,2]{0,1:T(2,128)} %param.19) | copy-start | bytes 6148
  19.5 76.4 %collective-permute-start.4 = (bf16[256,1024]{1,0:T(8,128)(2,1)}, bf16[256,1024]{1,0:T(8,128)(2,1)}, u32[]{:S(2)}, u32[]{:S(2)}) collective-permute-start(bf16[256,1024]{1,0:T(8,128)(2,1)} %get-tuple-element.81.refs_8_), channel_id=1, source_target_pairs={{0,6},{2,4},{4,2},{6,0},{8,14},{10,12},{12,10},{14,8},{16,22},{18,... | collective-permute-start | bytes 1572872 | tf_op jit(solution)/shard_map/ppermute | solution.py:40
  22.3 79.1 %collective-permute-start.3 = (bf16[256,1024]{1,0:T(8,128)(2,1)}, bf16[256,1024]{1,0:T(8,128)(2,1)}, u32[]{:S(2)}, u32[]{:S(2)}) collective-permute-start(bf16[256,1024]{1,0:T(8,128)(2,1)} %get-tuple-element.81.refs_8_), channel_id=1, source_target_pairs={{0,4},{2,6},{4,0},{6,2},{8,12},{10,14},{12,8},{14,10},{16,20},{18,... | collective-permute-start | bytes 1572872 | tf_op jit(solution)/shard_map/ppermute | solution.py:40
  22.9 78.5 %collective-permute-start.2 = (bf16[256,1024]{1,0:T(8,128)(2,1)}, bf16[256,1024]{1,0:T(8,128)(2,1)}, u32[]{:S(2)}, u32[]{:S(2)}) collective-permute-start(bf16[256,1024]{1,0:T(8,128)(2,1)} %get-tuple-element.81.refs_8_), channel_id=1, source_target_pairs={{0,2},{2,0},{4,6},{6,4},{8,10},{10,8},{12,14},{14,12},{16,18},{18,... | collective-permute-start | bytes 1572872 | tf_op jit(solution)/shard_map/ppermute | solution.py:40
  23.0 44.4 %collective-permute-start = (bf16[256,1024]{1,0:T(8,128)(2,1)}, bf16[256,1024]{1,0:T(8,128)(2,1)}, u32[]{:S(2)}, u32[]{:S(2)}) collective-permute-start(bf16[256,1024]{1,0:T(8,128)(2,1)} %get-tuple-element.81.refs_8_), channel_id=1, source_target_pairs={{0,8},{2,10},{4,12},{6,14},{8,0},{10,2},{12,4},{14,6},{16,24},{18,... | collective-permute-start | bytes 1572872 | tf_op jit(solution)/shard_map/ppermute | solution.py:40
  25.6 41.7 %collective-permute-start.1 = (f32[4,1024]{1,0:T(4,128)S(1)}, f32[4,1024]{1,0:T(4,128)S(1)}, u32[]{:S(2)}, u32[]{:S(2)}) collective-permute-start(f32[4,1024]{1,0:T(4,128)S(1)} %pad_maximum_fusion.4), channel_id=1, source_target_pairs={{0,2},{2,4},{4,6},{6,8},{8,10},{10,12},{12,14},{14,16},{16,18},{18... | collective-permute-start | bytes 49160 | tf_op jit(solution)/shard_map/ppermute | solution.py:35
  67.4 0.6 copy-start.32
  67.4 11.1 %copy-start.33 = (f32[1,1024]{1,0:T(1,128)S(1)}, f32[1,1024]{1,0:T(1,128)}, u32[]{:S(2)}) copy-start(f32[1,1024]{1,0:T(1,128)} %get-tuple-element.116) | copy-start | bytes 12292
  68.0 58.6 %all-to-all-start.1 = ((bf16[16,32,2048]{2,1,0:T(8,128)(2,1)}), bf16[16,32,2048]{2,1,0:T(8,128)(2,1)}, u32[]{:S(2)}, u32[]{:S(2)}) async-start(bf16[16,32,2048]{2,1,0:T(8,128)(2,1)} %bitcast.154), calls=%async_computation.1 | async-start | bytes 4194304 | tf_op jit(solution)/shard_map/all_to_all | solution.py:307
  75.8 4.0 %copy-start.28 = (bf16[8,128,128]{2,1,0:T(8,128)(2,1)S(1)}, bf16[8,128,128]{2,1,0:T(8,128)(2,1)}, u32[]{:S(2)}) copy-start(bf16[8,128,128]{2,1,0:T(8,128)(2,1)} %input_w_ref.1) | copy-start | bytes 786436
  75.8 35.3 %collective-permute-start.7 = (bf16[256,1024]{1,0:T(8,128)(2,1)}, bf16[256,1024]{1,0:T(8,128)(2,1)}, u32[]{:S(2)}, u32[]{:S(2)}) collective-permute-start(bf16[256,1024]{1,0:T(8,128)(2,1)} %collective-permute-done.refs_12_), channel_id=1, source_target_pairs={{0,6},{2,4},{4,2},{6,0},{8,14},{10,12},{12,10},{14,8},{16,22},{18,... | collective-permute-start | bytes 1572872 | tf_op jit(solution)/shard_map/ppermute | solution.py:40
  78.5 2.6 copy-start.29
  79.8 2.5 copy-start.9
  79.8 2.5 copy-start.23
  79.8 2.5 copy-start.36
  81.2 15.4 %collective-permute-start.8 = (bf16[512,2048]{1,0:T(8,128)(2,1)}, bf16[512,2048]{1,0:T(8,128)(2,1)S(1)}, u32[]{:S(2)}, u32[]{:S(2)}) collective-permute-start(bf16[512,2048]{1,0:T(8,128)(2,1)} %bitcast.3), channel_id=1, source_target_pairs={{0,1},{1,0},{2,3},{3,2},{4,5},{5,4},{6,7},{7,6},{8,9},{9,8},{10,11... | collective-permute-start | bytes 6291464 | tf_op jit(solution)/shard_map/ppermute | solution.py:40
  85.4 66.4 %copy-start.7 = (f32[256,1024]{1,0:T(8,128)}, f32[256,1024]{1,0:T(8,128)S(1)}, u32[]{:S(2)}) copy-start(f32[256,1024]{1,0:T(8,128)S(1)} %get-tuple-element.74.to_input_ref) | copy-start | bytes 3145732
  90.2 2.0 copy-start.5
  96.0 25.9 %collective-permute-start.6 = (bf16[256,1024]{1,0:T(8,128)(2,1)}, bf16[256,1024]{1,0:T(8,128)(2,1)}, u32[]{:S(2)}, u32[]{:S(2)}) collective-permute-start(bf16[256,1024]{1,0:T(8,128)(2,1)} %collective-permute-done.refs_12_), channel_id=1, source_target_pairs={{0,4},{2,6},{4,0},{6,2},{8,12},{10,14},{12,8},{14,10},{16,20},{18,... | collective-permute-start | bytes 1572872 | tf_op jit(solution)/shard_map/ppermute | solution.py:40
  96.6 2.6 copy-start.3
  96.6 30.0 %collective-permute-start.5 = (bf16[256,1024]{1,0:T(8,128)(2,1)}, bf16[256,1024]{1,0:T(8,128)(2,1)}, u32[]{:S(2)}, u32[]{:S(2)}) collective-permute-start(bf16[256,1024]{1,0:T(8,128)(2,1)} %collective-permute-done.refs_12_), channel_id=1, source_target_pairs={{0,2},{2,0},{4,6},{6,4},{8,10},{10,8},{12,14},{14,12},{16,18},{18,... | collective-permute-start | bytes 1572872 | tf_op jit(solution)/shard_map/ppermute | solution.py:40
  126.6 5.5 %copy-start.24 = (f32[512,512]{1,0:T(8,128)S(1)}, f32[512,512]{1,0:T(8,128)}, u32[]{:S(2)}) copy-start(f32[512,512]{1,0:T(8,128)} %fusion.7) | copy-start | bytes 3145732
  126.6 5.5 %copy-start.26 = (f32[512,512]{1,0:T(8,128)S(1)}, f32[512,512]{1,0:T(8,128)}, u32[]{:S(2)}) copy-start(f32[512,512]{1,0:T(8,128)} %fusion.14) | copy-start | bytes 3145732
  126.6 5.5 %copy-start.37 = (bf16[1,512,2048]{2,1,0:T(8,128)(2,1)S(1)}, bf16[1,512,2048]{2,1,0:T(8,128)(2,1)}, u32[]{:S(2)}) copy-start(bf16[1,512,2048]{2,1,0:T(8,128)(2,1)} %param.22) | copy-start | bytes 6291460
  126.6 5.5 %collective-permute-start.9 = (bf16[512,2048]{1,0:T(8,128)(2,1)}, bf16[512,2048]{1,0:T(8,128)(2,1)S(1)}, u32[]{:S(2)}, u32[]{:S(2)}) collective-permute-start(bf16[512,2048]{1,0:T(8,128)(2,1)} %bitcast.26), channel_id=1, source_target_pairs={{0,1},{1,0},{2,3},{3,2},{4,5},{5,4},{6,7},{7,6},{8,9},{9,8},{10,11... | collective-permute-start | bytes 6291464 | tf_op jit(solution)/shard_map/ppermute | solution.py:40
  132.1 6.0 %copy-start.11 = (bf16[512,512]{1,0:T(8,128)(2,1)}, bf16[512,512]{1,0:T(8,128)(2,1)S(1)}, u32[]{:S(2)}) copy-start(bf16[512,512]{1,0:T(8,128)(2,1)S(1)} %get-tuple-element.67) | copy-start | bytes 1572868
  132.1 9.8 %copy-start.19 = (bf16[512,512]{1,0:T(8,128)(2,1)}, bf16[512,512]{1,0:T(8,128)(2,1)S(1)}, u32[]{:S(2)}) copy-start(bf16[512,512]{1,0:T(8,128)(2,1)S(1)} %get-tuple-element.66) | copy-start | bytes 1572868
  132.1 1.7 copy-start.17
  132.1 2.9 %copy-start.6 = (bf16[1,2048,512]{2,1,0:T(8,128)(2,1)S(1)}, bf16[1,2048,512]{2,1,0:T(8,128)(2,1)}, u32[]{:S(2)}) copy-start(bf16[1,2048,512]{2,1,0:T(8,128)(2,1)} %param.20) | copy-start | bytes 6291460
  133.8 2.5 copy-start.13
  133.8 2.5 copy-start.16
  137.6 4.2 %collective-permute-start.10 = (bf16[512,2048]{1,0:T(8,128)(2,1)S(1)}, bf16[512,2048]{1,0:T(8,128)(2,1)S(1)}, u32[]{:S(2)}, u32[]{:S(2)}) collective-permute-start(bf16[512,2048]{1,0:T(8,128)(2,1)S(1)} %add_convert_fusion.4), channel_id=1, source_target_pairs={{0,1},{1,0},{2,3},{3,2},{4,5},{5,4},{6,7},{7,6},{8,9},{9,8},{10,11... | collective-permute-start | bytes 6291464 | tf_op jit(solution)/shard_map/ppermute | solution.py:40
  144.5 9.4 %copy-start.4 = (bf16[512,2048]{1,0:T(8,128)(2,1)S(1)}, bf16[512,2048]{1,0:T(8,128)(2,1)}, u32[]{:S(2)}) copy-start(bf16[512,2048]{1,0:T(8,128)(2,1)} %copy-done.3) | copy-start | bytes 6291460
  144.5 49.7 %all-to-all-start.2 = ((bf16[16,32,2048]{2,1,0:T(8,128)(2,1)}), bf16[16,32,2048]{2,1,0:T(8,128)(2,1)}, u32[]{:S(2)}, u32[]{:S(2)}) async-start(bf16[16,32,2048]{2,1,0:T(8,128)(2,1)} %bitcast.156), calls=%async_computation.2 | async-start | bytes 4194304 | tf_op jit(solution)/shard_map/all_to_all | solution.py:375
  152.5 3.8 %copy-start.14 = (bf16[512,512]{1,0:T(8,128)(2,1)S(1)}, bf16[512,512]{1,0:T(8,128)(2,1)}, u32[]{:S(2)}) copy-start(bf16[512,512]{1,0:T(8,128)(2,1)} %copy-done.13) | copy-start | bytes 1572868
  152.5 20.4 %collective-permute-start.11 = (f32[3,8,1024]{2,1,0:T(8,128)S(1)}, f32[3,8,1024]{2,1,0:T(8,128)S(1)}, u32[]{:S(2)}, u32[]{:S(2)}) collective-permute-start(f32[3,8,1024]{2,1,0:T(8,128)S(1)} %pad_maximum_fusion.2), channel_id=1, source_target_pairs={{2,0},{4,2},{6,4},{8,6},{10,8},{12,10},{14,12},{16,14},{18,16},{20... | collective-permute-start | bytes 294920 | tf_op jit(solution)/shard_map/ppermute | solution.py:35
  156.3 1.6 copy-start.18
  156.3 1.8 copy-start.25
  156.4 2.1 copy-start.27
  158.5 1.4 copy-start.12
  159.9 4.4 %copy-start.20 = (bf16[512,512]{1,0:T(8,128)(2,1)S(1)}, bf16[512,512]{1,0:T(8,128)(2,1)}, u32[]{:S(2)}) copy-start(bf16[512,512]{1,0:T(8,128)(2,1)} %copy-done.19) | copy-start | bytes 1572868
  164.2 4.4 %copy-start.21 = (bf16[512,512]{1,0:T(8,128)(2,1)S(1)}, bf16[512,512]{1,0:T(8,128)(2,1)}, u32[]{:S(2)}) copy-start(bf16[512,512]{1,0:T(8,128)(2,1)} %get-tuple-element.72) | copy-start | bytes 1572868
  196.6 2.7 %copy-start.10 = (bf16[256,2048]{1,0:T(8,128)(2,1)}, bf16[256,2048]{1,0:T(8,128)(2,1)S(1)}, u32[]{:S(2)}) copy-start(bf16[256,2048]{1,0:T(8,128)(2,1)S(1)} %convolution_convert_fusion.1.mine_ref) | copy-start | bytes 3145732
  196.6 2.7 %collective-permute-start.12 = (bf16[256,2048]{1,0:T(8,128)(2,1)S(1)}, bf16[256,2048]{1,0:T(8,128)(2,1)S(1)}, u32[]{:S(2)}, u32[]{:S(2)}) collective-permute-start(bf16[256,2048]{1,0:T(8,128)(2,1)S(1)} %convolution_convert_fusion.1.mine_ref), channel_id=1, source_target_pairs={{0,1},{1,0},{2,3},{3,2},{4,5},{5,4},{6,7},{7,6},{8,9},{9,8},{10,11... | collective-permute-start | bytes 3145736 | tf_op jit(solution)/shard_map/ppermute | solution.py:40
  199.3 1.0 copy-start.22
  204.4 26.4 %all-to-all-start.3 = ((bf16[8,256,256]{2,1,0:T(8,128)(2,1)}), bf16[8,256,256]{2,1,0:T(8,128)(2,1)S(1)}, u32[]{:S(2)}, u32[]{:S(2)}) async-start(bf16[8,256,256]{2,1,0:T(8,128)(2,1)} %get-tuple-element.80), calls=%async_computation.3 | async-start | bytes 2097152 | tf_op jit(solution)/shard_map/all_to_all | solution.py:390
  224.3 21.2 %collective-permute-start.14 = (f32[2,8,1024]{2,1,0:T(8,128)S(1)}, f32[2,8,1024]{2,1,0:T(8,128)S(1)}, u32[]{:S(2)}, u32[]{:S(2)}) collective-permute-start(f32[2,8,1024]{2,1,0:T(8,128)S(1)} %pad_maximum_fusion.3), channel_id=1, source_target_pairs={{2,0},{4,2},{6,4},{8,6},{10,8},{12,10},{14,12},{16,14},{18,16},{20... | collective-permute-start | bytes 196616 | tf_op jit(solution)/shard_map/ppermute | solution.py:35
  230.8 4.5 %copy-start.2 = (bf16[8,256,256]{2,1,0:T(8,128)(2,1)}, bf16[8,256,256]{2,1,0:T(8,128)(2,1)S(1)}, u32[]{:S(2)}) copy-start(bf16[8,256,256]{2,1,0:T(8,128)(2,1)S(1)} %all-to-all-done.3.refs_0_.refs_1_.refs_2_.refs_3_.refs_4_.refs_5_.refs_6_.refs_7_) | copy-start | bytes 3145732
  230.8 15.9 %all-to-all-start.4 = ((f32[16,2,1024]{2,1,0:T(2,128)}), f32[16,2,1024]{2,1,0:T(2,128)S(1)}, u32[]{:S(2)}, u32[]{:S(2)}) async-start(f32[16,2,1024]{2,1,0:T(2,128)} %get-tuple-element.94), calls=%async_computation.4 | async-start | bytes 262144 | tf_op jit(solution)/shard_map/all_to_all | solution.py:397
  242.7 14.6 %collective-permute-start.13 = (bf16[128,1024]{1,0:T(8,128)(2,1)}, bf16[128,1024]{1,0:T(8,128)(2,1)S(1)}, u32[]{:S(2)}, u32[]{:S(2)}) collective-permute-start(bf16[128,1024]{1,0:T(8,128)(2,1)} %fusion.45), channel_id=1, source_target_pairs={{0,16},{2,18},{4,20},{6,22},{8,24},{10,26},{12,28},{14,30},{16,0},... | collective-permute-start | bytes 786440 | tf_op jit(solution)/shard_map/ppermute | solution.py:40
  246.8 0.7 copy-start.30
  247.4 9.8 %copy-start.15 = (f32[256,1024]{1,0:T(8,128)S(1)}, f32[256,1024]{1,0:T(8,128)}, u32[]{:S(2)}) copy-start(f32[256,1024]{1,0:T(8,128)} %product.1) | copy-start | bytes 3145732
  247.4 10.7 %copy-start.1 = (bf16[1,2048,512]{2,1,0:T(8,128)(2,1)S(1)}, bf16[1,2048,512]{2,1,0:T(8,128)(2,1)}, u32[]{:S(2)}) copy-start(bf16[1,2048,512]{2,1,0:T(8,128)(2,1)} %param.21) | copy-start | bytes 6291460

commit v2 on v1

--- a/solution.py
+++ b/solution.py
@@ -69,42 +69,50 @@
     return decay_out, value_out
 
 
-def mixer_kernel(grad_ref, weight_ref, gelu_ref, slope_ref, next_ref, first_ref,
-                 gate_ref, local_ref, cumul_ref, ends_ref):
-    mixer = jnp.dot(grad_ref[...], weight_ref[...], preferred_element_type=f32)
-    gate_ref[...] = (mixer * slope_ref[...]).astype(bf16)
-    decays, values = back_scan(next_ref[...], mixer * gelu_ref[...])
-    for tile, (part_a, part_b) in enumerate(zip(decays, values)):
-        cumul_ref[tile * 8 : tile * 8 + 8] = part_a
-        local_ref[tile * 8 : tile * 8 + 8] = part_b
-    first = first_ref[...]
-    end_a = first * decays[0][:1]
-    end_b = first * values[0][:1]
-    for peer in range(ends_ref.shape[0]):
-        ends_ref[peer] = jnp.concatenate([end_a, end_b], axis=0)
+def held(count):
+    return [pl.BlockSpec(memory_space=pltpu.VMEM)] * count
+
+
+def params(mib):
+    return pltpu.CompilerParams(vmem_limit_bytes=mib << 20)
+
+
+def mixer_kernel(block, grad_ref, weight_ref, gelu_ref, slope_ref, next_ref, first_ref,
+                 gate_ref, local_ref, cumul_ref, ends_ref, head_ref):
+    def turn(index, _):
+        cols = pl.ds(pl.multiple_of(index * block, block), block)
+        mixer = jnp.dot(grad_ref[...], weight_ref[:, cols], preferred_element_type=f32)
+        gate_ref[:, cols] = (mixer * slope_ref[:, cols]).astype(bf16)
+        decays, values = back_scan(next_ref[:, cols], mixer * gelu_ref[:, cols])
+        for tile, (part_a, part_b) in enumerate(zip(decays, values)):
+            cumul_ref[tile * 8 : tile * 8 + 8, cols] = part_a
+            local_ref[tile * 8 : tile * 8 + 8, cols] = part_b
+        head_ref[0, :, cols] = values[0]
+        head_ref[1, :, cols] = decays[0]
+        first = first_ref[:, cols]
+        both = jnp.concatenate([first * decays[0][:1], first * values[0][:1]], axis=0)
+        for peer in range(ends_ref.shape[0]):
+            ends_ref[peer, :, cols] = both
+        return 0
+
+    lax.fori_loop(0, weight_ref.shape[1] // block, turn, 0)
 
 
 def mixer_call(input_grad, out_weight, gelu, slope, next_decay, first, peers):
     rows, width = input_grad.shape
     channels = out_weight.shape[1]
-    block = 256
-    wide = pl.BlockSpec((rows, block), lambda i: (0, i))
     return pl.pallas_call(
-        mixer_kernel,
-        grid=(channels // block,),
-        in_specs=[
-            pl.BlockSpec((rows, width), lambda i: (0, 0)),
-            pl.BlockSpec((width, block), lambda i: (0, i)),
-            wide, wide, wide,
-            pl.BlockSpec((1, block), lambda i: (0, i)),
-        ],
-        out_specs=[wide, wide, wide, pl.BlockSpec((peers, 2, block), lambda i: (0, 0, i))],
+        functools.partial(mixer_kernel, 256),
+        in_specs=held(6),
+        out_specs=held(5),
         out_shape=[
             jax.ShapeDtypeStruct((rows, channels), bf16),
             jax.ShapeDtypeStruct((rows, channels), f32),
             jax.ShapeDtypeStruct((rows, channels), f32),
             jax.ShapeDtypeStruct((peers, 2, channels), f32),
+            jax.ShapeDtypeStruct((2, 8, channels), f32),
         ],
+        compiler_params=params(20),
         cost_estimate=pl.CostEstimate(
             flops=2 * rows * width * channels, bytes_accessed=8 << 20, transcendentals=0
         ),
@@ -116,6 +124,10 @@
                 head_ref, head_coef_ref, taps_ref, decay_w_ref, input_w_ref, out_ref):
     mine = where_ref[0]
     count = ends_ref.shape[0]
+    block = decay_w_ref.shape[1]
+    rows = local_ref.shape[0]
+    taps = taps_ref[...].astype(f32)
+
     carry = jnp.zeros_like(local_ref[:1])
     head_carry = carry
     for place in reversed(range(1, count)):
@@ -123,123 +135,102 @@
         longer = ends[1:2] + ends[0:1] * carry
         head_carry = jnp.where(place > mine + 1, longer, head_carry)
         carry = jnp.where(place > mine, longer, carry)
-    decay_w = decay_w_ref[0]
-    input_w = input_w_ref[0]
-
-    def conv_grad(carried, to_decay, to_input, direct):
-        decay_pre = (carried * to_decay).astype(bf16)
-        input_pre = (carried * to_input).astype(bf16)
-        return carried * direct + cols_of(decay_pre, decay_w) + cols_of(input_pre, input_w)
-
-    main = conv_grad(
-        local_ref[...] + cumul_ref[...] * carry, to_decay_ref[...], to_input_ref[...], direct_ref[...]
-    )
-    halo = conv_grad(
-        head_ref[...] + head_coef_ref[0] * head_carry,
-        head_coef_ref[1], head_coef_ref[2], head_coef_ref[3],
-    )
-    rows = main.shape[0]
-    whole = jnp.concatenate([main, halo], axis=0)
-    taps = taps_ref[...].astype(f32)
-    total = taps[0:1] * pltpu.roll(whole, whole.shape[0] - 3, 0)
-    for tap in range(1, 3):
-        total = total + taps[tap : tap + 1] * pltpu.roll(whole, whole.shape[0] - 3 + tap, 0)
-    total = total + taps[3:4] * whole
-    out_ref[...] = total[:rows].astype(bf16)
-
-
-def tail_call(mine, ends, local, cumul, to_decay, to_input, direct, head, head_coef, taps, decay_w, input_w):
-    rows, channels = local.shape
-    count = ends.shape[0]
-    block = decay_w.shape[1]
-    wide = pl.BlockSpec((rows, block), lambda i, s: (0, i))
+
+    for index in range(decay_w_ref.shape[0]):
+        cols = slice(index * block, (index + 1) * block)
+        decay_w = decay_w_ref[index]
+        input_w = input_w_ref[index]
+
+        def conv_grad(carried, to_decay, to_input, direct):
+            decay_pre = (carried * to_decay).astype(bf16)
+            input_pre = (carried * to_input).astype(bf16)
+            return carried * direct + cols_of(decay_pre, decay_w) + cols_of(input_pre, input_w)
+
+        main = conv_grad(
+            local_ref[:, cols] + cumul_ref[:, cols] * carry[:, cols],
+            to_decay_ref[:, cols], to_input_ref[:, cols], direct_ref[:, cols],
+        )
+        halo = conv_grad(
+            head_ref[0, :, cols] + head_ref[1, :, cols] * head_carry[:, cols],
+            head_coef_ref[0, :, cols], head_coef_ref[1, :, cols], head_coef_ref[2, :, cols],
+        )
+        whole = jnp.concatenate([main, halo], axis=0)
+        total = taps[0:1, cols] * pltpu.roll(whole, whole.shape[0] - 3, 0)
+        for tap in range(1, 3):
+            total = total + taps[tap : tap + 1, cols] * pltpu.roll(whole, whole.shape[0] - 3 + tap, 0)
+        total = total + taps[3:4, cols] * whole
+        out_ref[:, cols] = total[:rows].astype(bf16)
+
+
+def tail_call(where, *arrays):
+    rows, channels = arrays[1].shape
+    block = arrays[-1].shape[1]
     return pl.pallas_call(
         tail_kernel,
-        grid_spec=pltpu.PrefetchScalarGridSpec(
-            num_scalar_prefetch=1,
-            grid=(channels // block,),
-            in_specs=[
-                pl.BlockSpec((count, 2, block), lambda i, s: (0, 0, i)),
-                wide, wide, wide, wide, wide,
-                pl.BlockSpec((8, block), lambda i, s: (0, i)),
-                pl.BlockSpec((4, 8, block), lambda i, s: (0, 0, i)),
-                pl.BlockSpec((4, block), lambda i, s: (0, i)),
-                pl.BlockSpec((1, block, block), lambda i, s: (i, 0, 0)),
-                pl.BlockSpec((1, block, block), lambda i, s: (i, 0, 0)),
-            ],
-            out_specs=wide,
-        ),
+        in_specs=[pl.BlockSpec(memory_space=pltpu.SMEM)] + held(len(arrays)),
+        out_specs=pl.BlockSpec(memory_space=pltpu.VMEM),
         out_shape=jax.ShapeDtypeStruct((rows, channels), bf16),
+        compiler_params=params(14),
         cost_estimate=pl.CostEstimate(
             flops=8 * rows * block * channels, bytes_accessed=7 << 20, transcendentals=0
         ),
         name="tail",
-    )(mine, ends, local, cumul, to_decay, to_input, direct, head, head_coef, taps, decay_w, input_w)
+    )(where, *arrays)
 
 
 def combine_kernel(lanes, mine_ref, other_ref, cot_ref, grad_ref, piece_ref):
-    total = mine_ref[...].astype(f32) + other_ref[...].astype(f32) + cot_ref[...].astype(f32)
-    total = total.astype(bf16)
-    grad_ref[...] = total
     group, _, cut = piece_ref.shape
     for peer in range(group):
         for level in range(cut // lanes):
             column = (level * group + peer) * lanes
-            piece_ref[peer, :, level * lanes : (level + 1) * lanes] = total[:, column : column + lanes]
+            cols = slice(column, column + lanes)
+            total = mine_ref[:, cols].astype(f32) + other_ref[:, cols].astype(f32)
+            total = (total + cot_ref[:, cols].astype(f32)).astype(bf16)
+            grad_ref[:, cols] = total
+            piece_ref[peer, :, level * lanes : (level + 1) * lanes] = total
 
 
 def combine_call(mine, other, cotangent, group, lanes):
     rows, width = mine.shape
-    block = rows // 4
-    cut = width // group
-    wide = pl.BlockSpec((block, width), lambda i: (i, 0))
     return pl.pallas_call(
         functools.partial(combine_kernel, lanes),
-        grid=(4,),
-        in_specs=[wide, wide, wide],
-        out_specs=[wide, pl.BlockSpec((group, block, cut), lambda i: (0, i, 0))],
+        in_specs=held(3),
+        out_specs=held(2),
         out_shape=[
             jax.ShapeDtypeStruct((rows, width), bf16),
-            jax.ShapeDtypeStruct((group, rows, cut), bf16),
+            jax.ShapeDtypeStruct((group, rows, width // group), bf16),
         ],
+        compiler_params=params(10),
         cost_estimate=pl.CostEstimate(flops=1 << 28, bytes_accessed=5 << 20, transcendentals=0),
         name="combine",
     )(mine, other, cotangent)
 
 
-def product_kernel(level_ref, *refs):
-    count = len(refs) // 2
-    out_refs = refs[2 * count :]
-    total = rows_of(refs[0][0], refs[count][...])
-    for k in range(1, count):
-        total = total + rows_of(refs[k][0], refs[count + k][...])
-    full_ref = out_refs[0]
-    full_ref[...] = total
-
-
-def product_call(where, grads, mixers):
-    group, rows, cut = grads.shape
+def product_kernel(mask, where_ref, grads_ref, *refs):
+    group = grads_ref.shape[0]
+    lanes = refs[-1].shape[0]
+    inner = lax.rem(where_ref[0], group)
+    level = (where_ref[0] // group) ^ mask
+    cols = pl.ds(pl.multiple_of(level * lanes, lanes), lanes)
+    total = rows_of(grads_ref[inner, :, cols], refs[0][...])
+    for k in range(1, group):
+        total = total + rows_of(grads_ref[inner ^ k, :, cols], refs[k][...])
+    refs[-1][...] = total.astype(refs[-1].dtype)
+
+
+def product_call(mask, kind, lanes, where, grads, mixers):
+    group, rows, _ = grads.shape
     channels = mixers[0].shape[1]
-    block = channels // 4
-
-    def grad_spec(k):
-        return pl.BlockSpec((1, rows, cut), lambda i, s: (jnp.bitwise_xor(lax.rem(s[0], group), k), 0, 0))
-
     return pl.pallas_call(
-        product_kernel,
-        grid_spec=pltpu.PrefetchScalarGridSpec(
-            num_scalar_prefetch=1,
-            grid=(channels // block,),
-            in_specs=[grad_spec(k) for k in range(group)]
-            + [pl.BlockSpec((rows, block), lambda i, s: (0, i))] * group,
-            out_specs=[pl.BlockSpec((cut, block), lambda i, s: (0, i))],
+        functools.partial(product_kernel, mask),
+        in_specs=[pl.BlockSpec(memory_space=pltpu.SMEM)] + held(1 + group),
+        out_specs=pl.BlockSpec(memory_space=pltpu.VMEM),
+        out_shape=jax.ShapeDtypeStruct((lanes, channels), kind),
+        compiler_params=params(14),
+        cost_estimate=pl.CostEstimate(
+            flops=2 * group * rows * lanes * channels, bytes_accessed=6 << 20, transcendentals=0
         ),
-        out_shape=[jax.ShapeDtypeStruct((cut, channels), f32)],
-        cost_estimate=pl.CostEstimate(
-            flops=2 * group * rows * cut * channels, bytes_accessed=6 << 20, transcendentals=0
-        ),
-        name="product",
-    )(where, *([grads] * group), *mixers)[0]
+    )(where, grads, *mixers)
 
 
 def on_device(
@@ -299,14 +290,12 @@
     half = group // 2
     mixers = {0: mixer_out}
     mixers[half] = swapped(mixer_out, "sp", half)
+    send_grads, mixers[half], gelu_value, slope, edge, got_rows = lax.optimization_barrier(
+        (send_grads, mixers[half], gelu_value, slope, edge, got_rows)
+    )
+    got_grads = lax.all_to_all(send_grads, "sp", split_axis=0, concat_axis=0, tiled=True)
     for k in range(1, half):
         mixers[k] = swapped(mixer_out, "sp", k)
-    send_grads, mixers[half], gelu_value, slope, edge, got_rows = lax.optimization_barrier(
-        (send_grads, mixers[half], gelu_value, slope, edge, got_rows)
-    )
-    got_grads = lax.all_to_all(send_grads, "sp", split_axis=0, concat_axis=0, tiled=True)
-    for k in range(1, half):
-        mixers[k ^ half] = swapped(mixers[half], "sp", k)
     extended = jnp.concatenate([edge[:3], recur_input.astype(f32)], axis=0)
     prev_state = edge[3:]
     taps = conv_taps.astype(f32)
@@ -350,6 +339,8 @@
         (got_grads, mixers, pres, rows_there, gates)
     )
     next_decay, first_decay, to_decay, to_input, direct = gates
+    for k in range(1, half):
+        mixers[k ^ half] = swapped(mixers[half], "sp", k)
     grads_here = got_grads.reshape(own_slots, width)
     grads_there = swapped(grads_here, "tp", 1)
 
@@ -378,7 +369,9 @@
     gate_weight_grad = rows_of(rows_here, gate_h) + rows_of(rows_there, gate_t)
     up_weight_grad = rows_of(rows_here, up_h) + rows_of(rows_there, up_t)
     weight_grads = (gate_weight_grad.astype(bf16), up_weight_grad.astype(bf16), down_grad.astype(bf16))
-    back, weight_grads, head_coef = lax.optimization_barrier((back, weight_grads, head_coef))
+    back, weight_grads, head_coef, mixers = lax.optimization_barrier(
+        (back, weight_grads, head_coef, mixers)
+    )
 
     mine_back = rows_of(placing, back.reshape(own_slots, width)).astype(bf16)
     other_back = swapped(mine_back, "tp", 1)
@@ -390,27 +383,34 @@
     grads = lax.all_to_all(
         pieces, "sp", split_axis=0, concat_axis=0, tiled=True, axis_index_groups=groups
     )
-    gate_grad, local, cumul, ends = mixer_call(
+    gate_grad, local, cumul, ends, head = mixer_call(
         input_grad, out_weight, gelu_value, slope, next_decay, first_decay, experts
     )
-    head = shifted(jnp.stack([local[:8], cumul[:8]]), "sp", -1)
+    head = shifted(head, "sp", -1)
     ends = lax.all_to_all(ends, "sp", split_axis=0, concat_axis=0, tiled=True)
-    product = product_call(where, grads, [mixers[k] for k in range(group)])
-    product = product.reshape(outer, out_rows, channels)
-    level = place // group
-
-    def block_for(index):
-        return lax.dynamic_slice_in_dim(product, index, 1, 0)[0]
-
-    out_weight_grad = block_for(level)
-    for k in range(1, outer):
-        received = swapped(block_for(level ^ k).astype(bf16), "sp", k * group)
-        out_weight_grad = out_weight_grad + received.astype(f32)
-
-    head_coef = jnp.concatenate([head[1:], head_coef], axis=0)
+    mixers = [mixers[k] for k in range(group)]
+    if out_rows % 128 == 0:
+        def block_for(mask, kind):
+            return product_call(mask, kind, out_rows, where, grads, mixers)
+    else:
+        full = sum(
+            rows_of(lax.dynamic_index_in_dim(grads, place % group ^ k, 0, False), mixers[k])
+            for k in range(group)
+        ).reshape(outer, out_rows, channels)
+
+        def block_for(mask, kind):
+            return lax.dynamic_index_in_dim(full, place // group ^ mask, 0, False).astype(kind)
+
+    received = []
+    for mask in range(1, outer):
+        received.append(swapped(block_for(mask, bf16), "sp", mask * group))
+    out_weight_grad = block_for(0, f32)
+    for part in received:
+        out_weight_grad = out_weight_grad + part.astype(f32)
+
     recur_grad = tail_call(
         where, ends, local, cumul, to_decay, to_input, direct,
-        head[0], head_coef, conv_taps, decay_gate_w, input_gate_w,
+        head, head_coef, conv_taps, decay_gate_w, input_gate_w,
     )
     return (
         weight_grads[0][None],

time: 260 us -> 285 us (1.096)
  the two profiles are of different devices: /device:TPU:0 before, /device:TPU:14 now
where the time goes in v2:
time: 285 us; the launch traced here: 282 us
  waiting for transfers between devices  82.3 us (29%)
  matrix products  78.1 us (27%)
  starting transfers between devices  54.8 us (19%)
  local copies, waits for them, and re-layouts  34.2 us (12%)
  other arithmetic  19.3 us (7%)
  Pallas kernels  12.4 us (4%)
    dot_general x35, matrix products, dot(): lax.dot_general(left, right, (contract, ((), ())), preferred_element_type...  78.1 us
    ppermute x3, waiting for transfers between devices, shifted(): return lax.ppermute(value, axis, pairs)  62.5 us
    unnamed x125, local copies, waits for them, and re-layouts  29.4 us
    all_to_all x1, waiting for transfers between devices, on_device(): lax.all_to_all(send_grads, 'sp', split_axis=0, concat_axis=0, tiled=True)  14.6 us
    ppermute x12, starting transfers between devices, swapped(): return lax.ppermute(value, axis, [(s, s ^ mask) for s in range(count)])  10.5 us
    all_to_all x1, starting transfers between devices, on_device(): lax.all_to_all(pieces, 'sp', split_axis=0, concat_axis=0, tiled=True, axi...  9.38 us
    ppermute x3, starting transfers between devices, shifted(): return lax.ppermute(value, axis, pairs)  9.21 us
    all_to_all x1, starting transfers between devices, on_device(): ends = lax.all_to_all(ends, 'sp', split_axis=0, concat_axis=0, tiled=True)  7.69 us
  transfers between devices with their start and end apart: 20, of which 6 were waited for; matrix products, arithmetic and copies ran while one was open for 30% of the time, Pallas kernels for 4%

profile of v2, /device:TPU:14, one launch (start us, length us, event | category | flops | bytes accessed | tf_op | source)
XLA Modules:
  0.0 282.3 jit_solution(1946340694660393009)
XLA Ops:
  1.9 1.2 reduce-window.6
  4.5 3.3 %convolution_convert_fusion = bf16[512,2048]{1,0:T(8,128)(2,1)} fusion(pred[512,256]{1,0:T(8,128)(4,1)S(1)} %compare_reduce_fusion, bf16[256,2048]{1,0:T(8,128)(2,1)} %param.16), kind=kOutput, calls=%fused_computation.6 | convolution fusion | flops 537919488 | bytes 3276800 | tf_op jit(solution)/shard_map/dot_general | solution.py:17
  7.8 7.3 %all-to-all-start = ((bf16[16,32,2048]{2,1,0:T(8,128)(2,1)}), bf16[16,32,2048]{2,1,0:T(8,128)(2,1)}, u32[]{:S(2)}, u32[]{:S(2)}) async-start(bf16[16,32,2048]{2,1,0:T(8,128)(2,1)} %bitcast.144), calls=%async_computation | async-start | bytes 4194304 | tf_op jit(solution)/shard_map/all_to_all | solution.py:279
  15.2 3.5 %fusion.22 = (f32[256,1024]{1,0:T(8,128)}, bf16[256,1024]{1,0:T(8,128)(2,1)S(1)}, f32[256,1024]{1,0:T(8,128)}) fusion(f32[256,1024]{1,0:T(8,128)} %param.26, bf16[256,1024]{1,0:T(8,128)(2,1)S(1)} %copy-done.57), kind=kLoop, calls=%fused_computation.56 | loop fusion | flops 5767168 | bytes 4194304 | tf_op jit(solution)/shard_map/mul | solution.py:288
  19.9 2.8 collective-permute-start.4
  24.2 4.3 %collective-permute-start.1 = (f32[4,1024]{1,0:T(4,128)S(1)}, f32[4,1024]{1,0:T(4,128)S(1)}, u32[]{:S(2)}, u32[]{:S(2)}) collective-permute-start(f32[4,1024]{1,0:T(4,128)S(1)} %pad_maximum_fusion.2), channel_id=1, source_target_pairs={{0,2},{2,4},{4,6},{6,8},{8,10},{10,12},{12,14},{14,16},{16,18},{18... | collective-permute-start | bytes 49160 | tf_op jit(solution)/shard_map/ppermute | solution.py:35
  29.4 3.3 %multiply_convert_fusion = bf16[512,2048]{1,0:T(8,128)(2,1)} fusion(pred[512,256]{1,0:T(8,128)(4,1)S(1)} %compare_reduce_fusion, bf16[256,2048]{1,0:T(8,128)(2,1)} %cot_ref.1, f32[512]{0:T(512)S(1)} %fusion.19), kind=kOutput, calls=%fused_computation.5 | convolution fusion | flops 538968064 | bytes 3278848 | tf_op jit(solution)/shard_map/dot_general | solution.py:17
  33.7 30.8 %collective-permute-done.1 = f32[4,1024]{1,0:T(4,128)S(1)} collective-permute-done((f32[4,1024]{1,0:T(4,128)S(1)}, f32[4,1024]{1,0:T(4,128)S(1)}, u32[]{:S(2)}, u32[]{:S(2)}) %collective-permute-start.1) | collective-permute-done | bytes 16416 | tf_op jit(solution)/shard_map/ppermute | solution.py:35
  65.2 4.3 %fusion.110 = (bf16[256,1024]{1,0:T(8,128)(2,1)S(1)}, f32[256,1024]{1,0:T(8,128)}) fusion(f32[256,1024]{1,0:T(8,128)} %convert_element_type.82, f32[1024]{0:T(1024)} %bitcast.154, f32[3,1024]{1,0:T(4,128)} %bitcast.150, f32[1024]{0:T(1024)} %bitcast.153, f32[1024]{0:T(1024)} %bitcast.152, f32[1024]{0:T(1024)S(1)} %bitcast.151), kind=kLoop, calls=%fused_computation.178 | loop fusion | flops 2883584 | bytes 2650112 | tf_op jit(solution)/shard_map/convert_element_type | solution.py:306
  77.8 5.3 %all-to-all-start.1 = ((bf16[16,32,2048]{2,1,0:T(8,128)(2,1)}), bf16[16,32,2048]{2,1,0:T(8,128)(2,1)}, u32[]{:S(2)}, u32[]{:S(2)}) async-start(bf16[16,32,2048]{2,1,0:T(8,128)(2,1)} %bitcast.143), calls=%async_computation.1 | async-start | bytes 4194304 | tf_op jit(solution)/shard_map/all_to_all | solution.py:296
  83.1 1.7 convolution_dynamic-update-slice_fusion.6
  84.8 1.6 convolution_dynamic-update-slice_fusion.5
  86.5 1.6 convolution_dynamic-update-slice_fusion.4
  88.1 1.6 convolution_dynamic-update-slice_fusion.3
  89.7 1.6 convolution_dynamic-update-slice_fusion.2
  91.4 1.6 convolution_dynamic-update-slice_fusion.1
  93.0 1.6 convolution_dynamic-update-slice_fusion
  94.7 5.5 %subtract_multiply_fusion = (f32[256,1024]{1,0:T(8,128)}, f32[256,1024]{1,0:T(8,128)}, f32[256,1024]{1,0:T(8,128)}, f32[256,1024]{1,0:T(8,128)S(1)}) fusion(f32[256,1024]{1,0:T(8,128)} %get-tuple-element.112, f32[256,1024]{1,0:T(8,128)} %convolution_dynamic-update-slice_fusion, f32[256,1024]{1,0:T(8,128)} %param.31, f32[1024]{0:T(1024)S(1)} %broadcast_multiply_fusion, ...), kind=kLoop, calls=%fused_computation.87 | loop fusion | flops 7340032 | bytes 9441536 | tf_op jit(solution)/shard_map/mul | solution.py:326
  100.3 1.1 concatenate.21.next_ref
  102.1 3.8 %fusion.16 = f32[512,512]{1,0:T(8,128)} fusion(bf16[512,2048]{1,0:T(8,128)(2,1)} %bitcast.3, bf16[1,2048,512]{2,1,0:T(8,128)(2,1)S(1)} %copy-done.40), kind=kOutput, calls=%fused_computation.24 | convolution fusion | flops 1073741824 | bytes 5242880 | tf_op jit(solution)/shard_map/dot_general | solution.py:17
  105.9 3.8 %fusion.9 = f32[512,512]{1,0:T(8,128)} fusion(bf16[512,2048]{1,0:T(8,128)(2,1)} %bitcast.3, bf16[1,2048,512]{2,1,0:T(8,128)(2,1)S(1)} %copy-done), kind=kOutput, calls=%fused_computation.17 | convolution fusion | flops 1073741824 | bytes 5242880 | tf_op jit(solution)/shard_map/dot_general | solution.py:17
  109.8 3.8 %fusion.14 = f32[512,512]{1,0:T(8,128)} fusion(bf16[512,2048]{1,0:T(8,128)(2,1)} %collective-permute-done.5, bf16[1,2048,512]{2,1,0:T(8,128)(2,1)S(1)} %copy-done.40), kind=kOutput, calls=%fused_computation.22 | convolution fusion | flops 1073741824 | bytes 5242880 | tf_op jit(solution)/shard_map/dot_general | solution.py:17
  113.6 3.8 %fusion.7 = f32[512,512]{1,0:T(8,128)} fusion(bf16[512,2048]{1,0:T(8,128)(2,1)} %collective-permute-done.5, bf16[1,2048,512]{2,1,0:T(8,128)(2,1)S(1)} %copy-done), kind=kOutput, calls=%fused_computation.15 | convolution fusion | flops 1073741824 | bytes 5242880 | tf_op jit(solution)/shard_map/dot_general | solution.py:17
  117.4 14.6 %all-to-all-done.1 = bf16[16,32,2048]{2,1,0:T(8,128)(2,1)} async-done(((bf16[16,32,2048]{2,1,0:T(8,128)(2,1)}), bf16[16,32,2048]{2,1,0:T(8,128)(2,1)}, u32[]{:S(2)}, u32[]{:S(2)}) %all-to-all-start.1) | async-done | bytes 2097184 | tf_op jit(solution)/shard_map/all_to_all | solution.py:296
  132.0 5.4 %multiply_convert_fusion.4 = (bf16[512,512]{1,0:T(8,128)(2,1)S(1)}, bf16[512,512]{1,0:T(8,128)(2,1)S(1)}, bf16[512,512]{1,0:T(8,128)(2,1)}) fusion(f32[512,512]{1,0:T(8,128)} %fusion.16, f32[512,512]{1,0:T(8,128)} %fusion.9, bf16[512,2048]{1,0:T(8,128)(2,1)} %bitcast.26, bf16[1,512,2048]{2,1,0:T(8,128)(2,1)} %param.22), kind=kOutput, calls=%fused_computation.82 | convolution fusion | flops 1077673984 | bytes 7864320 | tf_op jit(solution)/shard_map/dot_general | solution.py:17
  137.5 1.7 multiply_convert_fusion.2
  140.0 1.3 fusion.11
  141.3 1.3 add_convert_fusion.4
  143.1 1.3 fusion.5
  144.4 2.5 collective-permute-done.7
  146.9 2.8 %add_convert_fusion.3 = bf16[512,2048]{1,0:T(8,128)(2,1)} fusion(bf16[512,2048]{1,0:T(8,128)(2,1)S(1)} %collective-permute-done.7, f32[512,2048]{1,0:T(8,128)S(1)} %fusion.5, bf16[512,512]{1,0:T(8,128)(2,1)S(1)} %get-tuple-element.72, bf16[1,2048,512]{2,1,0:T(8,128)(2,1)S(1)} %copy-done.41), kind=kOutput, calls=%fused_computation.3 | convolution fusion | flops 1077936128 | bytes 11010048 | tf_op jit(solution)/shard_map/dot_general | solution.py:17
  149.8 5.4 %all-to-all-start.2 = ((bf16[16,32,2048]{2,1,0:T(8,128)(2,1)}), bf16[16,32,2048]{2,1,0:T(8,128)(2,1)}, u32[]{:S(2)}, u32[]{:S(2)}) async-start(bf16[16,32,2048]{2,1,0:T(8,128)(2,1)} %bitcast.145), calls=%async_computation.2 | async-start | bytes 4194304 | tf_op jit(solution)/shard_map/all_to_all | solution.py:366
  155.7 1.5 collective-permute-start.11
  157.2 1.5 collective-permute-start.9
  160.2 2.5 collective-permute-start.8
  162.7 3.0 %fusion.114 = f32[2048,512]{1,0:T(8,128)S(1)} fusion(bf16[512,2048]{1,0:T(8,128)(2,1)} %collective-permute-done.5, bf16[512,512]{1,0:T(8,128)(2,1)} %copy-done.44), kind=kOutput, calls=%fused_computation.181 | convolution fusion | flops 1073741824 | bytes 6815744 | tf_op jit(solution)/shard_map/dot_general | solution.py:17
  165.6 2.9 %fusion.113 = f32[2048,512]{1,0:T(8,128)S(1)} fusion(bf16[512,2048]{1,0:T(8,128)(2,1)} %collective-permute-done.5, bf16[512,512]{1,0:T(8,128)(2,1)S(1)} %get-tuple-element.118), kind=kOutput, calls=%fused_computation.180 | convolution fusion | flops 1073741824 | bytes 6815744 | tf_op jit(solution)/shard_map/dot_general | solution.py:17
  168.6 4.4 %add_convert_fusion.1 = bf16[2048,512]{1,0:T(8,128)(2,1)} fusion(f32[2048,512]{1,0:T(8,128)S(1)} %fusion.114, bf16[512,2048]{1,0:T(8,128)(2,1)} %bitcast.3, bf16[512,512]{1,0:T(8,128)(2,1)S(1)} %get-tuple-element.73), kind=kOutput, calls=%fused_computation.1 | convolution fusion | flops 1075838976 | bytes 8912896 | tf_op jit(solution)/shard_map/dot_general | solution.py:17
  172.9 4.5 %add_convert_fusion.2 = bf16[2048,512]{1,0:T(8,128)(2,1)} fusion(f32[2048,512]{1,0:T(8,128)S(1)} %fusion.113, bf16[512,2048]{1,0:T(8,128)(2,1)} %bitcast.3, bf16[512,512]{1,0:T(8,128)(2,1)S(1)} %copy-done.49), kind=kOutput, calls=%fused_computation.2 | convolution fusion | flops 1075838976 | bytes 8912896 | tf_op jit(solution)/shard_map/dot_general | solution.py:17
  177.4 1.3 fusion.43
  178.8 4.3 %add_convert_fusion = bf16[512,2048]{1,0:T(8,128)(2,1)} fusion(f32[512,2048]{1,0:T(8,128)S(1)} %fusion.43, bf16[512,512]{1,0:T(8,128)(2,1)S(1)} %copy-done.51, bf16[512,2048]{1,0:T(8,128)(2,1)} %bitcast.26), kind=kOutput, calls=%fused_computation | convolution fusion | flops 1075838976 | bytes 8912896 | tf_op jit(solution)/shard_map/dot_general | solution.py:17
  183.1 22.1 %collective-permute-done.8.head_coef_ref = f32[3,8,1024]{2,1,0:T(8,128)S(1)} collective-permute-done((f32[3,8,1024]{2,1,0:T(8,128)S(1)}, f32[3,8,1024]{2,1,0:T(8,128)S(1)}, u32[]{:S(2)}, u32[]{:S(2)}) %collective-permute-start.8) | collective-permute-done | bytes 98336 | tf_op jit(solution)/shard_map/ppermute | solution.py:35
  208.3 2.4 convolution_convert_fusion.1.mine_ref
  210.8 2.6 collective-permute-done.12.other_ref
  213.4 1.6 combine.1
  216.0 9.4 %all-to-all-start.3 = ((bf16[8,256,256]{2,1,0:T(8,128)(2,1)}), bf16[8,256,256]{2,1,0:T(8,128)(2,1)S(1)}, u32[]{:S(2)}, u32[]{:S(2)}) async-start(bf16[8,256,256]{2,1,0:T(8,128)(2,1)} %copy-done.25), calls=%async_computation.3 | async-start | bytes 2097152 | tf_op jit(solution)/shard_map/all_to_all | solution.py:383
  225.4 2.2 copy-done.9
  227.6 1.2 copy-done.10
  228.8 1.2 copy-done.11
  230.1 1.2 copy-done.12
  231.3 1.2 copy-done.30
  232.5 3.8 %mixer.1 = (bf16[256,1024]{1,0:T(8,128)(2,1)}, f32[256,1024]{1,0:T(8,128)S(1)}, f32[256,1024]{1,0:T(8,128)S(1)}, f32[16,2,1024]{2,1,0:T(2,128)}, f32[2,8,1024]{2,1,0:T(8,128)S(1)}) custom-call(bf16[256,2048]{1,0:T(8,128)(2,1)S(1)} %copy-done.30, bf16[2048,1024]{1,0:T(8,128)(2,1)S(1)} %copy-done.9, f32[256,1024]{1,0:T(8,128)S(1)} %copy-done.12, ...), custom_call_target="tpu_custom_call" | custom-call | flops 1073741824 | bytes 8388608 | tf_op jit(solution)/shard_map/mixer/pallas_call | solution.py:104
  238.9 7.7 %all-to-all-start.4 = ((f32[16,2,1024]{2,1,0:T(2,128)}), f32[16,2,1024]{2,1,0:T(2,128)S(1)}, u32[]{:S(2)}, u32[]{:S(2)}) async-start(f32[16,2,1024]{2,1,0:T(2,128)} %get-tuple-element.105), calls=%async_computation.4 | async-start | bytes 262144 | tf_op jit(solution)/shard_map/all_to_all | solution.py:390
  250.8 2.8 %shard_map.208 = bf16[128,1024]{1,0:T(8,128)(2,1)} custom-call(s32[1]{0:T(128)} %bitcast.35.where_ref, bf16[8,256,256]{2,1,0:T(8,128)(2,1)S(1)} %all-to-all-done.3.grads_ref, bf16[256,1024]{1,0:T(8,128)(2,1)S(1)} %copy-done.3, bf16[256,1024]{1,0:T(8,128)(2,1)S(1)} %copy-done.14, bf16[256,1024]{1,0:T(8,128)(2,1)} %collective-permute-done.3.refs_2_, ...), custom_call_target="tpu_custom_call" | custom-call | flops 536870912 | bytes 6291456 | tf_op jit(solution)/shard_map/pallas_call | solution.py:224
  253.7 2.4 collective-permute-start.13
  256.0 2.5 collective-permute-start.14
  258.5 9.6 %collective-permute-done.14.head_ref = f32[2,8,1024]{2,1,0:T(8,128)S(1)} collective-permute-done((f32[2,8,1024]{2,1,0:T(8,128)S(1)}, f32[2,8,1024]{2,1,0:T(8,128)S(1)}, u32[]{:S(2)}, u32[]{:S(2)}) %collective-permute-start.14) | collective-permute-done | bytes 65568 | tf_op jit(solution)/shard_map/ppermute | solution.py:35
  268.7 1.2 copy-done.6
  269.9 1.2 copy-done.7
  271.1 1.2 copy-done.27
  272.4 1.2 copy-done.29
  276.3 1.9 tail.1
  278.2 2.3 shard_map.207
  280.4 1.8 convert_add_fusion.1
  (173 shorter events, 34.9 us)
Async XLA Ops:
  0.6 105.3 %copy-start = (bf16[1,2048,512]{2,1,0:T(8,128)(2,1)S(1)}, bf16[1,2048,512]{2,1,0:T(8,128)(2,1)}, u32[]{:S(2)}) copy-start(bf16[1,2048,512]{2,1,0:T(8,128)(2,1)} %param.21) | copy-start | bytes 6291460
  4.5 24.8 %copy-start.45 = (pred[512,256]{1,0:T(8,128)(4,1)}, pred[512,256]{1,0:T(8,128)(4,1)S(1)}, u32[]{:S(2)}) copy-start(pred[512,256]{1,0:T(8,128)(4,1)S(1)} %compare_reduce_fusion) | copy-start | bytes 393220
  7.8 7.3 %copy-start.57 = (bf16[256,1024]{1,0:T(8,128)(2,1)S(1)}, bf16[256,1024]{1,0:T(8,128)(2,1)}, u32[]{:S(2)}) copy-start(bf16[256,1024]{1,0:T(8,128)(2,1)} %param.25) | copy-start | bytes 1572868
  7.8 56.7 %all-to-all-start = ((bf16[16,32,2048]{2,1,0:T(8,128)(2,1)}), bf16[16,32,2048]{2,1,0:T(8,128)(2,1)}, u32[]{:S(2)}, u32[]{:S(2)}) async-start(bf16[16,32,2048]{2,1,0:T(8,128)(2,1)} %bitcast.144), calls=%async_computation | async-start | bytes 4194304 | tf_op jit(solution)/shard_map/all_to_all | solution.py:279
  15.1 13.3 %copy-start.59 = (f32[1024]{0:T(1024)S(1)}, f32[1024]{0:T(1024)}, u32[]{:S(2)}) copy-start(f32[1024]{0:T(1024)} %param.30) | copy-start | bytes 12292
  15.1 13.4 %copy-start.35 = (bf16[4,1024]{1,0:T(4,128)(2,1)S(1)}, bf16[4,1024]{1,0:T(4,128)(2,1)}, u32[]{:S(2)}) copy-start(bf16[4,1024]{1,0:T(4,128)(2,1)} %taps_ref.1) | copy-start | bytes 24580
  15.1 14.0 %copy-start.60 = (f32[256,2]{0,1:T(2,128)S(1)}, f32[256,2]{0,1:T(2,128)}, u32[]{:S(2)}) copy-start(f32[256,2]{0,1:T(2,128)} %param.19) | copy-start | bytes 6148
  18.6 15.1 %copy-start.2 = (bf16[256,1024]{1,0:T(8,128)(2,1)}, bf16[256,1024]{1,0:T(8,128)(2,1)S(1)}, u32[]{:S(2)}) copy-start(bf16[256,1024]{1,0:T(8,128)(2,1)S(1)} %get-tuple-element.92.refs_0_) | copy-start | bytes 1572868
  18.6 45.9 %collective-permute-start = (bf16[256,1024]{1,0:T(8,128)(2,1)S(1)}, bf16[256,1024]{1,0:T(8,128)(2,1)}, u32[]{:S(2)}, u32[]{:S(2)}) collective-permute-start(bf16[256,1024]{1,0:T(8,128)(2,1)S(1)} %get-tuple-element.92.refs_0_), channel_id=1, source_target_pairs={{0,8},{2,10},{4,12},{6,14},{8,0},{10,2},{12,4},{14,6},{16,24},{18,... | collective-permute-start | bytes 1572872 | tf_op jit(solution)/shard_map/ppermute | solution.py:40
  19.2 98.2 %collective-permute-start.2 = (bf16[256,1024]{1,0:T(8,128)(2,1)S(1)}, bf16[256,1024]{1,0:T(8,128)(2,1)S(1)}, u32[]{:S(2)}, u32[]{:S(2)}) collective-permute-start(bf16[256,1024]{1,0:T(8,128)(2,1)S(1)} %get-tuple-element.92.refs_0_), channel_id=1, source_target_pairs={{0,2},{2,0},{4,6},{6,4},{8,10},{10,8},{12,14},{14,12},{16,18},{18,... | collective-permute-start | bytes 1572872 | tf_op jit(solution)/shard_map/ppermute | solution.py:40
  19.8 97.7 %collective-permute-start.3 = (bf16[256,1024]{1,0:T(8,128)(2,1)S(1)}, bf16[256,1024]{1,0:T(8,128)(2,1)}, u32[]{:S(2)}, u32[]{:S(2)}) collective-permute-start(bf16[256,1024]{1,0:T(8,128)(2,1)S(1)} %get-tuple-element.92.refs_0_), channel_id=1, source_target_pairs={{0,4},{2,6},{4,0},{6,2},{8,12},{10,14},{12,8},{14,10},{16,20},{18,... | collective-permute-start | bytes 1572872 | tf_op jit(solution)/shard_map/ppermute | solution.py:40
  19.9 97.5 %collective-permute-start.4 = (bf16[256,1024]{1,0:T(8,128)(2,1)S(1)}, bf16[256,1024]{1,0:T(8,128)(2,1)}, u32[]{:S(2)}, u32[]{:S(2)}) collective-permute-start(bf16[256,1024]{1,0:T(8,128)(2,1)S(1)} %get-tuple-element.92.refs_0_), channel_id=1, source_target_pairs={{0,6},{2,4},{4,2},{6,0},{8,14},{10,12},{12,10},{14,8},{16,22},{18,... | collective-permute-start | bytes 1572872 | tf_op jit(solution)/shard_map/ppermute | solution.py:40
  24.2 40.4 %collective-permute-start.1 = (f32[4,1024]{1,0:T(4,128)S(1)}, f32[4,1024]{1,0:T(4,128)S(1)}, u32[]{:S(2)}, u32[]{:S(2)}) collective-permute-start(f32[4,1024]{1,0:T(4,128)S(1)} %pad_maximum_fusion.2), channel_id=1, source_target_pairs={{0,2},{2,4},{4,6},{6,8},{8,10},{10,12},{12,14},{14,16},{16,18},{18... | collective-permute-start | bytes 49160 | tf_op jit(solution)/shard_map/ppermute | solution.py:35
  28.5 4.2 %copy-start.56 = (bf16[256,1024]{1,0:T(8,128)(2,1)S(1)}, bf16[256,1024]{1,0:T(8,128)(2,1)}, u32[]{:S(2)}) copy-start(bf16[256,1024]{1,0:T(8,128)(2,1)} %param.24) | copy-start | bytes 1572868
  65.2 11.6 %copy-start.31 = (bf16[8,128,128]{2,1,0:T(8,128)(2,1)S(1)}, bf16[8,128,128]{2,1,0:T(8,128)(2,1)}, u32[]{:S(2)}) copy-start(bf16[8,128,128]{2,1,0:T(8,128)(2,1)} %input_w_ref.1) | copy-start | bytes 786436
  69.4 7.3 %copy-start.42 = (bf16[256,1024]{1,0:T(8,128)(2,1)}, bf16[256,1024]{1,0:T(8,128)(2,1)S(1)}, u32[]{:S(2)}) copy-start(bf16[256,1024]{1,0:T(8,128)(2,1)S(1)} %get-tuple-element.111) | copy-start | bytes 1572868
  77.8 32.0 %collective-permute-start.5 = (bf16[512,2048]{1,0:T(8,128)(2,1)}, bf16[512,2048]{1,0:T(8,128)(2,1)}, u32[]{:S(2)}, u32[]{:S(2)}) collective-permute-start(bf16[512,2048]{1,0:T(8,128)(2,1)} %bitcast.3), channel_id=1, source_target_pairs={{0,1},{1,0},{2,3},{3,2},{4,5},{5,4},{6,7},{7,6},{8,9},{9,8},{10,11... | collective-permute-start | bytes 6291464 | tf_op jit(solution)/shard_map/ppermute | solution.py:40
  77.8 54.3 %all-to-all-start.1 = ((bf16[16,32,2048]{2,1,0:T(8,128)(2,1)}), bf16[16,32,2048]{2,1,0:T(8,128)(2,1)}, u32[]{:S(2)}, u32[]{:S(2)}) async-start(bf16[16,32,2048]{2,1,0:T(8,128)(2,1)} %bitcast.143), calls=%async_computation.1 | async-start | bytes 4194304 | tf_op jit(solution)/shard_map/all_to_all | solution.py:296
  83.1 11.6 %copy-start.43 = (f32[256,1024]{1,0:T(8,128)S(1)}, f32[256,1024]{1,0:T(8,128)}, u32[]{:S(2)}) copy-start(f32[256,1024]{1,0:T(8,128)} %param.26) | copy-start | bytes 3145732
  100.2 2.0 copy-start.40
  117.4 20.0 %copy-start.13 = (bf16[256,1024]{1,0:T(8,128)(2,1)}, bf16[256,1024]{1,0:T(8,128)(2,1)S(1)}, u32[]{:S(2)}) copy-start(bf16[256,1024]{1,0:T(8,128)(2,1)S(1)} %collective-permute-done.2.refs_1_) | copy-start | bytes 1572868
  132.0 5.4 %copy-start.52 = (f32[512,512]{1,0:T(8,128)S(1)}, f32[512,512]{1,0:T(8,128)}, u32[]{:S(2)}) copy-start(f32[512,512]{1,0:T(8,128)} %fusion.14) | copy-start | bytes 3145732
  132.0 5.4 %copy-start.54 = (f32[512,512]{1,0:T(8,128)S(1)}, f32[512,512]{1,0:T(8,128)}, u32[]{:S(2)}) copy-start(f32[512,512]{1,0:T(8,128)} %fusion.7) | copy-start | bytes 3145732
  132.0 5.4 %copy-start.61 = (bf16[1,512,2048]{2,1,0:T(8,128)(2,1)S(1)}, bf16[1,512,2048]{2,1,0:T(8,128)(2,1)}, u32[]{:S(2)}) copy-start(bf16[1,512,2048]{2,1,0:T(8,128)(2,1)} %param.22) | copy-start | bytes 6291460
  132.0 5.4 %collective-permute-start.6 = (bf16[512,2048]{1,0:T(8,128)(2,1)}, bf16[512,2048]{1,0:T(8,128)(2,1)S(1)}, u32[]{:S(2)}, u32[]{:S(2)}) collective-permute-start(bf16[512,2048]{1,0:T(8,128)(2,1)} %bitcast.26), channel_id=1, source_target_pairs={{0,1},{1,0},{2,3},{3,2},{4,5},{5,4},{6,7},{7,6},{8,9},{9,8},{10,11... | collective-permute-start | bytes 6291464 | tf_op jit(solution)/shard_map/ppermute | solution.py:40
  137.4 9.5 %copy-start.48 = (bf16[512,512]{1,0:T(8,128)(2,1)}, bf16[512,512]{1,0:T(8,128)(2,1)S(1)}, u32[]{:S(2)}) copy-start(bf16[512,512]{1,0:T(8,128)(2,1)S(1)} %get-tuple-element.72) | copy-start | bytes 1572868
  137.4 1.7 copy-start.46
  137.5 2.5 copy-start.41
  139.2 2.1 copy-start.44
  142.6 4.3 %collective-permute-start.7 = (bf16[512,2048]{1,0:T(8,128)(2,1)S(1)}, bf16[512,2048]{1,0:T(8,128)(2,1)S(1)}, u32[]{:S(2)}, u32[]{:S(2)}) collective-permute-start(bf16[512,2048]{1,0:T(8,128)(2,1)S(1)} %add_convert_fusion.4), channel_id=1, source_target_pairs={{0,1},{1,0},{2,3},{3,2},{4,5},{5,4},{6,7},{7,6},{8,9},{9,8},{10,11... | collective-permute-start | bytes 6291464 | tf_op jit(solution)/shard_map/ppermute | solution.py:40
  149.7 9.7 %copy-start.5 = (f32[256,1024]{1,0:T(8,128)S(1)}, f32[256,1024]{1,0:T(8,128)}, u32[]{:S(2)}) copy-start(f32[256,1024]{1,0:T(8,128)} %get-tuple-element.80.to_input_ref) | copy-start | bytes 3145732
  149.8 58.5 %all-to-all-start.2 = ((bf16[16,32,2048]{2,1,0:T(8,128)(2,1)}), bf16[16,32,2048]{2,1,0:T(8,128)(2,1)}, u32[]{:S(2)}, u32[]{:S(2)}) async-start(bf16[16,32,2048]{2,1,0:T(8,128)(2,1)} %bitcast.145), calls=%async_computation.2 | async-start | bytes 4194304 | tf_op jit(solution)/shard_map/all_to_all | solution.py:366
  155.2 50.7 %collective-permute-start.10 = (bf16[256,1024]{1,0:T(8,128)(2,1)}, bf16[256,1024]{1,0:T(8,128)(2,1)S(1)}, u32[]{:S(2)}, u32[]{:S(2)}) collective-permute-start(bf16[256,1024]{1,0:T(8,128)(2,1)} %collective-permute-done.refs_4_), channel_id=1, source_target_pairs={{0,4},{2,6},{4,0},{6,2},{8,12},{10,14},{12,8},{14,10},{16,20},{18,... | collective-permute-start | bytes 1572872 | tf_op jit(solution)/shard_map/ppermute | solution.py:40
  155.7 50.9 %collective-permute-start.11 = (bf16[256,1024]{1,0:T(8,128)(2,1)}, bf16[256,1024]{1,0:T(8,128)(2,1)S(1)}, u32[]{:S(2)}, u32[]{:S(2)}) collective-permute-start(bf16[256,1024]{1,0:T(8,128)(2,1)} %collective-permute-done.refs_4_), channel_id=1, source_target_pairs={{0,6},{2,4},{4,2},{6,0},{8,14},{10,12},{12,10},{14,8},{16,22},{18,... | collective-permute-start | bytes 1572872 | tf_op jit(solution)/shard_map/ppermute | solution.py:40
  157.2 50.3 %collective-permute-start.9 = (bf16[256,1024]{1,0:T(8,128)(2,1)}, bf16[256,1024]{1,0:T(8,128)(2,1)S(1)}, u32[]{:S(2)}, u32[]{:S(2)}) collective-permute-start(bf16[256,1024]{1,0:T(8,128)(2,1)} %collective-permute-done.refs_4_), channel_id=1, source_target_pairs={{0,2},{2,0},{4,6},{6,4},{8,10},{10,8},{12,14},{14,12},{16,18},{18,... | collective-permute-start | bytes 1572872 | tf_op jit(solution)/shard_map/ppermute | solution.py:40
  160.2 45.0 %collective-permute-start.8 = (f32[3,8,1024]{2,1,0:T(8,128)S(1)}, f32[3,8,1024]{2,1,0:T(8,128)S(1)}, u32[]{:S(2)}, u32[]{:S(2)}) collective-permute-start(f32[3,8,1024]{2,1,0:T(8,128)S(1)} %pad_maximum_fusion.1), channel_id=1, source_target_pairs={{2,0},{4,2},{6,4},{8,6},{10,8},{12,10},{14,12},{16,14},{18,16},{20... | collective-permute-start | bytes 294920 | tf_op jit(solution)/shard_map/ppermute | solution.py:35
  168.5 4.4 %copy-start.49 = (bf16[512,512]{1,0:T(8,128)(2,1)S(1)}, bf16[512,512]{1,0:T(8,128)(2,1)}, u32[]{:S(2)}) copy-start(bf16[512,512]{1,0:T(8,128)(2,1)} %copy-done.48) | copy-start | bytes 1572868
  172.9 4.5 %copy-start.47 = (bf16[512,2048]{1,0:T(8,128)(2,1)S(1)}, bf16[512,2048]{1,0:T(8,128)(2,1)}, u32[]{:S(2)}) copy-start(bf16[512,2048]{1,0:T(8,128)(2,1)} %copy-done.46) | copy-start | bytes 6291460
  172.9 4.5 %copy-start.53 = (f32[512,512]{1,0:T(8,128)S(1)}, f32[512,512]{1,0:T(8,128)}, u32[]{:S(2)}) copy-start(f32[512,512]{1,0:T(8,128)} %fusion.14) | copy-start | bytes 3145732
  172.9 4.5 %copy-start.55 = (f32[512,512]{1,0:T(8,128)S(1)}, f32[512,512]{1,0:T(8,128)}, u32[]{:S(2)}) copy-start(f32[512,512]{1,0:T(8,128)} %fusion.7) | copy-start | bytes 3145732
  177.4 1.4 copy-start.51
  183.1 30.3 %copy-start.8 = (bf16[256,2048]{1,0:T(8,128)(2,1)S(1)}, bf16[256,2048]{1,0:T(8,128)(2,1)}, u32[]{:S(2)}) copy-start(bf16[256,2048]{1,0:T(8,128)(2,1)} %cot_ref.1) | copy-start | bytes 3145732
  210.7 2.7 collective-permute-start.12
  216.0 22.9 %all-to-all-start.3 = ((bf16[8,256,256]{2,1,0:T(8,128)(2,1)}), bf16[8,256,256]{2,1,0:T(8,128)(2,1)S(1)}, u32[]{:S(2)}, u32[]{:S(2)}) async-start(bf16[8,256,256]{2,1,0:T(8,128)(2,1)} %copy-done.25), calls=%async_computation.3 | async-start | bytes 2097152 | tf_op jit(solution)/shard_map/all_to_all | solution.py:383
  225.4 2.2 copy-start.9
  227.6 1.2 copy-start.10
  228.8 1.2 copy-start.11
  230.1 1.2 copy-start.12
  231.3 1.2 copy-start.30
  232.5 14.1 %copy-start.3 = (bf16[256,1024]{1,0:T(8,128)(2,1)S(1)}, bf16[256,1024]{1,0:T(8,128)(2,1)}, u32[]{:S(2)}) copy-start(bf16[256,1024]{1,0:T(8,128)(2,1)} %copy-done.2) | copy-start | bytes 1572868
  238.9 29.7 %all-to-all-start.4 = ((f32[16,2,1024]{2,1,0:T(2,128)}), f32[16,2,1024]{2,1,0:T(2,128)S(1)}, u32[]{:S(2)}, u32[]{:S(2)}) async-start(f32[16,2,1024]{2,1,0:T(2,128)} %get-tuple-element.105), calls=%async_computation.4 | async-start | bytes 262144 | tf_op jit(solution)/shard_map/all_to_all | solution.py:390
  250.8 5.2 %copy-start.39 = (f32[2,8,1024]{2,1,0:T(8,128)S(1)}, f32[2,8,1024]{2,1,0:T(8,128)}, u32[]{:S(2)}) copy-start(f32[2,8,1024]{2,1,0:T(8,128)} %copy-done.38) | copy-start | bytes 196612
  253.7 26.8 %collective-permute-start.13 = (bf16[128,1024]{1,0:T(8,128)(2,1)}, bf16[128,1024]{1,0:T(8,128)(2,1)}, u32[]{:S(2)}, u32[]{:S(2)}) collective-permute-start(bf16[128,1024]{1,0:T(8,128)(2,1)} %shard_map.208), channel_id=1, source_target_pairs={{0,16},{2,18},{4,20},{6,22},{8,24},{10,26},{12,28},{14,30},{16,0},... | collective-permute-start | bytes 786440 | tf_op jit(solution)/shard_map/ppermute | solution.py:40
  256.0 12.0 %collective-permute-start.14 = (f32[2,8,1024]{2,1,0:T(8,128)S(1)}, f32[2,8,1024]{2,1,0:T(8,128)S(1)}, u32[]{:S(2)}, u32[]{:S(2)}) collective-permute-start(f32[2,8,1024]{2,1,0:T(8,128)S(1)} %copy-done.39), channel_id=1, source_target_pairs={{2,0},{4,2},{6,4},{8,6},{10,8},{12,10},{14,12},{16,14},{18,16},{20... | collective-permute-start | bytes 196616 | tf_op jit(solution)/shard_map/ppermute | solution.py:35
  268.7 1.2 copy-start.6
  269.9 1.2 copy-start.7
  271.1 1.2 copy-start.27
  272.4 1.2 copy-start.29
  276.3 1.9 copy-start.4
  276.3 1.9 copy-start.15
  276.3 1.9 copy-start.18
  276.3 1.9 copy-start.21
  276.3 1.9 copy-start.24
  278.2 4.1 %copy-start.1 = (bf16[1,2048,512]{2,1,0:T(8,128)(2,1)S(1)}, bf16[1,2048,512]{2,1,0:T(8,128)(2,1)}, u32[]{:S(2)}) copy-start(bf16[1,2048,512]{2,1,0:T(8,128)(2,1)} %param.21) | copy-start | bytes 6291460
  (18 other events, 15.7 us)

commit v3 on v2

--- a/solution.py
+++ b/solution.py
@@ -77,42 +77,49 @@
     return pltpu.CompilerParams(vmem_limit_bytes=mib << 20)
 
 
-def mixer_kernel(block, grad_ref, weight_ref, gelu_ref, slope_ref, next_ref, first_ref,
+def mixer_kernel(grad_ref, weight_ref, gelu_ref, slope_ref, next_ref, first_ref,
                  gate_ref, local_ref, cumul_ref, ends_ref, head_ref):
-    def turn(index, _):
-        cols = pl.ds(pl.multiple_of(index * block, block), block)
-        mixer = jnp.dot(grad_ref[...], weight_ref[:, cols], preferred_element_type=f32)
-        gate_ref[:, cols] = (mixer * slope_ref[:, cols]).astype(bf16)
-        decays, values = back_scan(next_ref[:, cols], mixer * gelu_ref[:, cols])
-        for tile, (part_a, part_b) in enumerate(zip(decays, values)):
-            cumul_ref[tile * 8 : tile * 8 + 8, cols] = part_a
-            local_ref[tile * 8 : tile * 8 + 8, cols] = part_b
-        head_ref[0, :, cols] = values[0]
-        head_ref[1, :, cols] = decays[0]
-        first = first_ref[:, cols]
-        both = jnp.concatenate([first * decays[0][:1], first * values[0][:1]], axis=0)
-        for peer in range(ends_ref.shape[0]):
-            ends_ref[peer, :, cols] = both
-        return 0
-
-    lax.fori_loop(0, weight_ref.shape[1] // block, turn, 0)
+    mixer = jnp.dot(grad_ref[...], weight_ref[...], preferred_element_type=f32)
+    gate_ref[...] = (mixer * slope_ref[...]).astype(bf16)
+    decays, values = back_scan(next_ref[...], mixer * gelu_ref[...])
+    for tile in range(0, len(values), 2):
+        rows = slice(tile * 8, tile * 8 + 16)
+        cumul_ref[rows] = jnp.concatenate(decays[tile : tile + 2], axis=0).astype(bf16)
+        local_ref[rows] = jnp.concatenate(values[tile : tile + 2], axis=0).astype(bf16)
+    head_ref[0] = values[0]
+    head_ref[1] = decays[0]
+    first = first_ref[...]
+    both = jnp.concatenate([first * decays[0][:1], first * values[0][:1]], axis=0)
+    for peer in range(ends_ref.shape[0]):
+        ends_ref[peer] = both
 
 
 def mixer_call(input_grad, out_weight, gelu, slope, next_decay, first, peers):
     rows, width = input_grad.shape
     channels = out_weight.shape[1]
+    block = 256
+    wide = pl.BlockSpec((rows, block), lambda i: (0, i))
     return pl.pallas_call(
-        functools.partial(mixer_kernel, 256),
-        in_specs=held(6),
-        out_specs=held(5),
+        mixer_kernel,
+        grid=(channels // block,),
+        in_specs=[
+            pl.BlockSpec((rows, width), lambda i: (0, 0)),
+            pl.BlockSpec((width, block), lambda i: (0, i)),
+            wide, wide, wide,
+            pl.BlockSpec((1, block), lambda i: (0, i)),
+        ],
+        out_specs=[
+            wide, wide, wide,
+            pl.BlockSpec((peers, 2, block), lambda i: (0, 0, i)),
+            pl.BlockSpec((2, 8, block), lambda i: (0, 0, i)),
+        ],
         out_shape=[
             jax.ShapeDtypeStruct((rows, channels), bf16),
-            jax.ShapeDtypeStruct((rows, channels), f32),
-            jax.ShapeDtypeStruct((rows, channels), f32),
+            jax.ShapeDtypeStruct((rows, channels), bf16),
+            jax.ShapeDtypeStruct((rows, channels), bf16),
             jax.ShapeDtypeStruct((peers, 2, channels), f32),
             jax.ShapeDtypeStruct((2, 8, channels), f32),
         ],
-        compiler_params=params(20),
         cost_estimate=pl.CostEstimate(
             flops=2 * rows * width * channels, bytes_accessed=8 << 20, transcendentals=0
         ),
@@ -139,6 +146,10 @@
     for index in range(decay_w_ref.shape[0]):
         cols = slice(index * block, (index + 1) * block)
         decay_w = decay_w_ref[index]
+
+        def wide(ref):
+            return ref[:, cols].astype(f32)
+
         input_w = input_w_ref[index]
 
         def conv_grad(carried, to_decay, to_input, direct):
@@ -147,8 +158,8 @@
             return carried * direct + cols_of(decay_pre, decay_w) + cols_of(input_pre, input_w)
 
         main = conv_grad(
-            local_ref[:, cols] + cumul_ref[:, cols] * carry[:, cols],
-            to_decay_ref[:, cols], to_input_ref[:, cols], direct_ref[:, cols],
+            wide(local_ref) + wide(cumul_ref) * carry[:, cols],
+            wide(to_decay_ref), wide(to_input_ref), wide(direct_ref),
         )
         halo = conv_grad(
             head_ref[0, :, cols] + head_ref[1, :, cols] * head_carry[:, cols],
@@ -163,16 +174,30 @@
 
 
 def tail_call(where, *arrays):
-    rows, channels = arrays[1].shape
-    block = arrays[-1].shape[1]
+    ends, local, decay_w = arrays[0], arrays[1], arrays[-1]
+    rows, channels = local.shape
+    width = decay_w.shape[1]
+    block = 2 * width
+    wide = pl.BlockSpec((rows, block), lambda i, s: (0, i))
+    gate = pl.BlockSpec((2, width, width), lambda i, s: (i, 0, 0))
     return pl.pallas_call(
         tail_kernel,
-        in_specs=[pl.BlockSpec(memory_space=pltpu.SMEM)] + held(len(arrays)),
-        out_specs=pl.BlockSpec(memory_space=pltpu.VMEM),
+        grid_spec=pltpu.PrefetchScalarGridSpec(
+            num_scalar_prefetch=1,
+            grid=(channels // block,),
+            in_specs=[
+                pl.BlockSpec((ends.shape[0], 2, block), lambda i, s: (0, 0, i)),
+                wide, wide, wide, wide, wide,
+                pl.BlockSpec((2, 8, block), lambda i, s: (0, 0, i)),
+                pl.BlockSpec((3, 8, block), lambda i, s: (0, 0, i)),
+                pl.BlockSpec((4, block), lambda i, s: (0, i)),
+                gate, gate,
+            ],
+            out_specs=wide,
+        ),
         out_shape=jax.ShapeDtypeStruct((rows, channels), bf16),
-        compiler_params=params(14),
         cost_estimate=pl.CostEstimate(
-            flops=8 * rows * block * channels, bytes_accessed=7 << 20, transcendentals=0
+            flops=8 * rows * width * channels, bytes_accessed=7 << 20, transcendentals=0
         ),
         name="tail",
     )(where, *arrays)
@@ -206,30 +231,59 @@
     )(mine, other, cotangent)
 
 
-def product_kernel(mask, where_ref, grads_ref, *refs):
-    group = grads_ref.shape[0]
-    lanes = refs[-1].shape[0]
+def product_kernel(where_ref, grads_ref, *refs):
+    group, _, _ = grads_ref.shape
+    sources, (send_ref, own_ref), (buffer, sems) = refs[:group], refs[group : group + 2], refs[group + 2 :]
+    lanes, channels = own_ref.shape
+    copies = [pltpu.make_async_copy(sources[k], buffer.at[k], sems.at[k]) for k in range(group)]
+    for copy in copies:
+        copy.start()
     inner = lax.rem(where_ref[0], group)
-    level = (where_ref[0] // group) ^ mask
-    cols = pl.ds(pl.multiple_of(level * lanes, lanes), lanes)
-    total = rows_of(grads_ref[inner, :, cols], refs[0][...])
-    for k in range(1, group):
-        total = total + rows_of(grads_ref[inner ^ k, :, cols], refs[k][...])
-    refs[-1][...] = total.astype(refs[-1].dtype)
-
-
-def product_call(mask, kind, lanes, where, grads, mixers):
-    group, rows, _ = grads.shape
+    level = where_ref[0] // group
+    half = group // 2
+    block = 512
+
+    def partial(mask, cols, first):
+        side = pl.ds(pl.multiple_of((level ^ mask) * lanes, lanes), lanes)
+        total = None
+        for k in range(first, first + half):
+            part = rows_of(grads_ref[inner ^ k, :, side], buffer[k, :, cols])
+            total = part if total is None else total + part
+        return total
+
+    for copy in copies[:half]:
+        copy.wait()
+    spans = [slice(start, start + block) for start in range(0, channels, block)]
+    firsts = {(mask, n): partial(mask, cols, 0) for mask in (1, 0) for n, cols in enumerate(spans)}
+    for copy in copies[half:]:
+        copy.wait()
+    for n, cols in enumerate(spans):
+        send_ref[:, cols] = (firsts[1, n] + partial(1, cols, half)).astype(bf16)
+        own_ref[:, cols] = firsts[0, n] + partial(0, cols, half)
+
+
+def product_call(lanes, where, grads, mixers):
+    group, rows, cut = grads.shape
     channels = mixers[0].shape[1]
     return pl.pallas_call(
-        functools.partial(product_kernel, mask),
-        in_specs=[pl.BlockSpec(memory_space=pltpu.SMEM)] + held(1 + group),
-        out_specs=pl.BlockSpec(memory_space=pltpu.VMEM),
-        out_shape=jax.ShapeDtypeStruct((lanes, channels), kind),
-        compiler_params=params(14),
+        product_kernel,
+        in_specs=[pl.BlockSpec(memory_space=pltpu.SMEM)]
+        + held(1)
+        + [pl.BlockSpec(memory_space=pl.ANY)] * group,
+        out_specs=held(2),
+        out_shape=[
+            jax.ShapeDtypeStruct((lanes, channels), bf16),
+            jax.ShapeDtypeStruct((lanes, channels), f32),
+        ],
+        scratch_shapes=[
+            pltpu.VMEM((group, rows, channels), bf16),
+            pltpu.SemaphoreType.DMA((group,)),
+        ],
+        compiler_params=params(24),
         cost_estimate=pl.CostEstimate(
-            flops=2 * group * rows * lanes * channels, bytes_accessed=6 << 20, transcendentals=0
+            flops=2 * group * rows * cut * channels, bytes_accessed=6 << 20, transcendentals=0
         ),
+        name="product",
     )(where, grads, *mixers)
 
 
@@ -290,8 +344,8 @@
     half = group // 2
     mixers = {0: mixer_out}
     mixers[half] = swapped(mixer_out, "sp", half)
-    send_grads, mixers[half], gelu_value, slope, edge, got_rows = lax.optimization_barrier(
-        (send_grads, mixers[half], gelu_value, slope, edge, got_rows)
+    send_grads, gelu_value, slope, edge, got_rows = lax.optimization_barrier(
+        (send_grads, gelu_value, slope, edge, got_rows)
     )
     got_grads = lax.all_to_all(send_grads, "sp", split_axis=0, concat_axis=0, tiled=True)
     for k in range(1, half):
@@ -334,11 +388,13 @@
     pres = tuple(
         (times(rows, weight_gate), times(rows, weight_up)) for rows in (rows_here, rows_there)
     )
-    gates = (next_decay, decay_value[:1], to_decay, to_input, direct)
-    got_grads, mixers, pres, rows_there, gates = lax.optimization_barrier(
-        (got_grads, mixers, pres, rows_there, gates)
-    )
-    next_decay, first_decay, to_decay, to_input, direct = gates
+    head_coef = jnp.stack([to_decay[:8], to_input[:8], direct[:8]])
+    gates = (
+        next_decay, decay_value[:1], head_coef,
+        to_decay.astype(bf16), to_input.astype(bf16), direct.astype(bf16),
+    )
+    got_grads, pres, rows_there, gates = lax.optimization_barrier((got_grads, pres, rows_there, gates))
+    next_decay, first_decay, head_coef, to_decay, to_input, direct = gates
     for k in range(1, half):
         mixers[k ^ half] = swapped(mixers[half], "sp", k)
     grads_here = got_grads.reshape(own_slots, width)
@@ -364,7 +420,7 @@
     partial_h = cols_of(gate_h, weight_gate) + cols_of(up_h, weight_up)
     shared = (partial_h + from_there.astype(f32)).astype(bf16).reshape(experts, share, width)
     back = lax.all_to_all(shared, "sp", split_axis=0, concat_axis=0, tiled=True)
-    head_coef = shifted(jnp.stack([to_decay[:8], to_input[:8], direct[:8]]), "sp", -1)
+    head_coef = shifted(head_coef, "sp", -1)
     down_grad = rows_of(hidden_h, grads_here) + rows_of(hidden_t, grads_there)
     gate_weight_grad = rows_of(rows_here, gate_h) + rows_of(rows_there, gate_t)
     up_weight_grad = rows_of(rows_here, up_h) + rows_of(rows_there, up_t)
@@ -389,22 +445,22 @@
     head = shifted(head, "sp", -1)
     ends = lax.all_to_all(ends, "sp", split_axis=0, concat_axis=0, tiled=True)
     mixers = [mixers[k] for k in range(group)]
-    if out_rows % 128 == 0:
-        def block_for(mask, kind):
-            return product_call(mask, kind, out_rows, where, grads, mixers)
+    received = []
+    if outer == 2 and out_rows % 128 == 0:
+        send, out_weight_grad = product_call(out_rows, where, grads, mixers)
+        received.append(swapped(send, "sp", group))
     else:
         full = sum(
             rows_of(lax.dynamic_index_in_dim(grads, place % group ^ k, 0, False), mixers[k])
             for k in range(group)
         ).reshape(outer, out_rows, channels)
 
-        def block_for(mask, kind):
-            return lax.dynamic_index_in_dim(full, place // group ^ mask, 0, False).astype(kind)
-
-    received = []
-    for mask in range(1, outer):
-        received.append(swapped(block_for(mask, bf16), "sp", mask * group))
-    out_weight_grad = block_for(0, f32)
+        def block_for(mask):
+            return lax.dynamic_index_in_dim(full, place // group ^ mask, 0, False)
+
+        for mask in range(1, outer):
+            received.append(swapped(block_for(mask).astype(bf16), "sp", mask * group))
+        out_weight_grad = block_for(0)
     for part in received:
         out_weight_grad = out_weight_grad + part.astype(f32)
 

time: 285 us -> 299 us (1.049)
  the two profiles are of different devices: /device:TPU:14 before, /device:TPU:0 now
where the time goes in v3:
time: 299 us; the launch traced here: 294 us
  waiting for transfers between devices  109 us (36%)
  matrix products  75.6 us (25%)
  starting transfers between devices  58 us (19%)
  other arithmetic  17.4 us (6%)
  local copies, waits for them, and re-layouts  17.2 us (6%)
  Pallas kernels  15.3 us (5%)
    dot_general x35, matrix products, dot(): lax.dot_general(left, right, (contract, ((), ())), preferred_element_type...  75.6 us
    ppermute x12, waiting for transfers between devices, swapped(): return lax.ppermute(value, axis, [(s, s ^ mask) for s in range(count)])  51.3 us
    all_to_all x1, waiting for transfers between devices, on_device(): lax.all_to_all(send_rows, 'sp', split_axis=0, concat_axis=0, tiled=True)  31.1 us
    all_to_all x1, waiting for transfers between devices, on_device(): lax.all_to_all(send_grads, 'sp', split_axis=0, concat_axis=0, tiled=True)  13.8 us
    ppermute x12, starting transfers between devices, swapped(): return lax.ppermute(value, axis, [(s, s ^ mask) for s in range(count)])  12.7 us
    unnamed x113, local copies, waits for them, and re-layouts  12.6 us
    all_to_all x1, starting transfers between devices, on_device(): lax.all_to_all(send_grads, 'sp', split_axis=0, concat_axis=0, tiled=True)  10.6 us
    all_to_all x1, starting transfers between devices, on_device(): back = lax.all_to_all(shared, 'sp', split_axis=0, concat_axis=0, tiled=True)  10 us
  transfers between devices with their start and end apart: 20, of which 11 were waited for; matrix products, arithmetic and copies ran while one was open for 21% of the time, Pallas kernels for 5%

profile of v3, /device:TPU:0, one launch (start us, length us, event | category | flops | bytes accessed | tf_op | source)
XLA Modules:
  0.0 293.6 jit_solution(14934230613655148431)
XLA Ops:
  1.9 1.2 reduce-window.6
  4.5 3.3 %convolution_convert_fusion = bf16[512,2048]{1,0:T(8,128)(2,1)} fusion(pred[512,256]{1,0:T(8,128)(4,1)S(1)} %compare_reduce_fusion, bf16[256,2048]{1,0:T(8,128)(2,1)} %param.16), kind=kOutput, calls=%fused_computation.6 | convolution fusion | flops 537919488 | bytes 3276800 | tf_op jit(solution)/shard_map/dot_general | solution.py:17
  7.8 8.5 %all-to-all-start = ((bf16[16,32,2048]{2,1,0:T(8,128)(2,1)}), bf16[16,32,2048]{2,1,0:T(8,128)(2,1)}, u32[]{:S(2)}, u32[]{:S(2)}) async-start(bf16[16,32,2048]{2,1,0:T(8,128)(2,1)} %bitcast.144), calls=%async_computation | async-start | bytes 4194304 | tf_op jit(solution)/shard_map/all_to_all | solution.py:333
  17.9 3.8 %collective-permute-start = (f32[4,1024]{1,0:T(4,128)S(1)}, f32[4,1024]{1,0:T(4,128)S(1)}, u32[]{:S(2)}, u32[]{:S(2)}) collective-permute-start(f32[4,1024]{1,0:T(4,128)S(1)} %pad_maximum_fusion.2), channel_id=1, source_target_pairs={{0,2},{2,4},{4,6},{6,8},{8,10},{10,12},{12,14},{14,16},{16,18},{18... | collective-permute-start | bytes 49160 | tf_op jit(solution)/shard_map/ppermute | solution.py:35
  22.6 2.0 multiply_convert_fusion
  24.6 2.1 multiply_convert_fusion.1
  28.3 31.1 %all-to-all-done = bf16[16,32,2048]{2,1,0:T(8,128)(2,1)} async-done(((bf16[16,32,2048]{2,1,0:T(8,128)(2,1)}), bf16[16,32,2048]{2,1,0:T(8,128)(2,1)}, u32[]{:S(2)}, u32[]{:S(2)}) %all-to-all-start) | async-done | bytes 2097184 | tf_op jit(solution)/shard_map/all_to_all | solution.py:333
  59.5 4.2 %fusion.115 = (bf16[256,1024]{1,0:T(8,128)(2,1)S(1)}, f32[256,1024]{1,0:T(8,128)}) fusion(f32[256,1024]{1,0:T(8,128)} %convert_element_type.90, f32[1024]{0:T(1024)} %bitcast.154, f32[3,1024]{1,0:T(4,128)} %bitcast.150, f32[1024]{0:T(1024)S(1)} %bitcast.153, f32[1024]{0:T(1024)S(1)} %bitcast.152, f32[1024]{0:T(1024)S(1)} %bitcast.151), kind=kLoop, calls=%fused_computation.181 | loop fusion | flops 2883584 | bytes 2650112 | tf_op jit(solution)/shard_map/convert_element_type | solution.py:360
  63.7 1.6 convolution_dynamic-update-slice_fusion.15
  65.2 1.6 convolution_dynamic-update-slice_fusion.14
  66.8 1.6 convolution_dynamic-update-slice_fusion.13
  68.4 1.6 convolution_dynamic-update-slice_fusion.12
  69.9 1.6 convolution_dynamic-update-slice_fusion.11
  71.5 1.6 convolution_dynamic-update-slice_fusion.10
  73.0 1.6 convolution_dynamic-update-slice_fusion.9
  74.6 1.6 convolution_dynamic-update-slice_fusion.8
  78.6 10.6 %all-to-all-start.1 = ((bf16[16,32,2048]{2,1,0:T(8,128)(2,1)}), bf16[16,32,2048]{2,1,0:T(8,128)(2,1)}, u32[]{:S(2)}, u32[]{:S(2)}) async-start(bf16[16,32,2048]{2,1,0:T(8,128)(2,1)} %bitcast.143), calls=%async_computation.1 | async-start | bytes 4194304 | tf_op jit(solution)/shard_map/all_to_all | solution.py:350
  89.2 1.7 convolution_dynamic-update-slice_fusion.4
  90.8 1.6 convolution_dynamic-update-slice_fusion.3
  92.5 1.6 convolution_dynamic-update-slice_fusion.2
  94.1 1.6 convolution_dynamic-update-slice_fusion.1
  95.8 1.6 convolution_dynamic-update-slice_fusion
  98.1 5.5 %fusion.113 = (bf16[256,1024]{1,0:T(8,128)(2,1)}, f32[256,1024]{1,0:T(8,128)S(1)}, bf16[256,1024]{1,0:T(8,128)(2,1)}, f32[256,1024]{1,0:T(8,128)S(1)}, bf16[256,...) fusion(f32[256,1024]{1,0:T(8,128)} %get-tuple-element.112, ...), kind=kLoop, calls=%fused_computation.180 | loop fusion | flops 8126464 | bytes 11014400 | tf_op jit(solution)/shard_map/convert_element_type | solution.py:394
  104.3 1.1 concatenate.21.next_ref
  105.5 3.8 %fusion.16 = f32[512,512]{1,0:T(8,128)} fusion(bf16[512,2048]{1,0:T(8,128)(2,1)} %bitcast.3, bf16[1,2048,512]{2,1,0:T(8,128)(2,1)S(1)} %copy-done.23), kind=kOutput, calls=%fused_computation.24 | convolution fusion | flops 1073741824 | bytes 5242880 | tf_op jit(solution)/shard_map/dot_general | solution.py:17
  109.3 3.8 %fusion.9 = f32[512,512]{1,0:T(8,128)} fusion(bf16[512,2048]{1,0:T(8,128)(2,1)} %bitcast.3, bf16[1,2048,512]{2,1,0:T(8,128)(2,1)S(1)} %copy-done), kind=kOutput, calls=%fused_computation.17 | convolution fusion | flops 1073741824 | bytes 5242880 | tf_op jit(solution)/shard_map/dot_general | solution.py:17
  113.1 2.2 fusion.14
  115.3 2.2 fusion.7
  117.6 13.8 %all-to-all-done.1 = bf16[16,32,2048]{2,1,0:T(8,128)(2,1)} async-done(((bf16[16,32,2048]{2,1,0:T(8,128)(2,1)}), bf16[16,32,2048]{2,1,0:T(8,128)(2,1)}, u32[]{:S(2)}, u32[]{:S(2)}) %all-to-all-start.1) | async-done | bytes 2097184 | tf_op jit(solution)/shard_map/all_to_all | solution.py:350
  131.3 5.4 %multiply_convert_fusion.5 = (bf16[512,512]{1,0:T(8,128)(2,1)S(1)}, bf16[512,512]{1,0:T(8,128)(2,1)S(1)}, bf16[512,512]{1,0:T(8,128)(2,1)}) fusion(f32[512,512]{1,0:T(8,128)} %fusion.16, f32[512,512]{1,0:T(8,128)} %fusion.9, bf16[512,2048]{1,0:T(8,128)(2,1)} %bitcast.29, bf16[1,512,2048]{2,1,0:T(8,128)(2,1)} %param.22), kind=kOutput, calls=%fused_computation.83 | convolution fusion | flops 1077673984 | bytes 7864320 | tf_op jit(solution)/shard_map/dot_general | solution.py:17
  136.8 1.7 multiply_convert_fusion.3
  139.5 1.3 fusion.11
  140.8 1.3 add_convert_fusion.4
  142.5 1.3 fusion.5
  143.8 2.5 collective-permute-done.3
  146.3 2.9 add_convert_fusion.3
  149.2 10.0 %all-to-all-start.2 = ((bf16[16,32,2048]{2,1,0:T(8,128)(2,1)}), bf16[16,32,2048]{2,1,0:T(8,128)(2,1)}, u32[]{:S(2)}, u32[]{:S(2)}) async-start(bf16[16,32,2048]{2,1,0:T(8,128)(2,1)} %bitcast.145), calls=%async_computation.2 | async-start | bytes 4194304 | tf_op jit(solution)/shard_map/all_to_all | solution.py:422
  159.3 1.9 collective-permute-start.8
  161.2 1.5 collective-permute-start.5
  162.7 1.5 collective-permute-start.6
  164.7 42.2 %collective-permute-done.8.refs_4_ = bf16[256,1024]{1,0:T(8,128)(2,1)S(1)} collective-permute-done((bf16[256,1024]{1,0:T(8,128)(2,1)S(1)}, bf16[256,1024]{1,0:T(8,128)(2,1)S(1)}, u32[]{:S(2)}, u32[]{:S(2)}) %collective-permute-start.8) | collective-permute-done | bytes 524320 | tf_op jit(solution)/shard_map/ppermute | solution.py:40
  206.9 2.5 collective-permute-start.10
  209.8 3.0 %fusion.119 = f32[2048,512]{1,0:T(8,128)S(1)} fusion(bf16[512,2048]{1,0:T(8,128)(2,1)} %copy-done.21, bf16[512,512]{1,0:T(8,128)(2,1)} %copy-done.31), kind=kOutput, calls=%fused_computation.184 | convolution fusion | flops 1073741824 | bytes 6815744 | tf_op jit(solution)/shard_map/dot_general | solution.py:17
  212.8 4.5 %add_convert_fusion.1 = bf16[2048,512]{1,0:T(8,128)(2,1)} fusion(f32[2048,512]{1,0:T(8,128)S(1)} %fusion.119, bf16[512,2048]{1,0:T(8,128)(2,1)} %bitcast.3, bf16[512,512]{1,0:T(8,128)(2,1)S(1)} %copy-done.28), kind=kOutput, calls=%fused_computation.1 | convolution fusion | flops 1075838976 | bytes 8912896 | tf_op jit(solution)/shard_map/dot_general | solution.py:17
  217.3 1.3 fusion.118
  218.6 4.5 %add_convert_fusion.2 = bf16[2048,512]{1,0:T(8,128)(2,1)} fusion(f32[2048,512]{1,0:T(8,128)S(1)} %fusion.118, bf16[512,2048]{1,0:T(8,128)(2,1)} %bitcast.3, bf16[512,512]{1,0:T(8,128)(2,1)S(1)} %copy-done.35), kind=kOutput, calls=%fused_computation.2 | convolution fusion | flops 1075838976 | bytes 8912896 | tf_op jit(solution)/shard_map/dot_general | solution.py:17
  223.1 1.1 collective-permute-start.9
  224.2 1.3 fusion.43
  225.6 1.3 collective-permute-start.4
  226.9 4.3 %add_convert_fusion = bf16[512,2048]{1,0:T(8,128)(2,1)} fusion(f32[512,2048]{1,0:T(8,128)S(1)} %fusion.43, bf16[512,512]{1,0:T(8,128)(2,1)S(1)} %copy-done.36, bf16[512,2048]{1,0:T(8,128)(2,1)} %bitcast.29), kind=kOutput, calls=%fused_computation | convolution fusion | flops 1075838976 | bytes 8912896 | tf_op jit(solution)/shard_map/dot_general | solution.py:17
  232.0 1.7 collective-permute-done.10.refs_6_
  235.3 1.4 collective-permute-done.9.refs_5_
  238.4 2.3 convolution_convert_fusion.1.mine_ref
  240.8 2.6 collective-permute-done.12.other_ref
  243.5 1.8 combine.1
  246.3 4.2 %all-to-all-start.3 = ((bf16[8,256,256]{2,1,0:T(8,128)(2,1)}), bf16[8,256,256]{2,1,0:T(8,128)(2,1)S(1)}, u32[]{:S(2)}, u32[]{:S(2)}) async-start(bf16[8,256,256]{2,1,0:T(8,128)(2,1)} %copy-done.4), calls=%async_computation.3 | async-start | bytes 2097152 | tf_op jit(solution)/shard_map/all_to_all | solution.py:439
  250.6 7.2 %mixer.1 = (bf16[256,1024]{1,0:T(8,128)(2,1)}, bf16[256,1024]{1,0:T(8,128)(2,1)}, bf16[256,1024]{1,0:T(8,128)(2,1)}, f32[16,2,1024]{2,1,0:T(2,128)}, f32[2,8,1024]{2,1,0:T(8,128)}) custom-call(bf16[256,2048]{1,0:T(8,128)(2,1)} %get-tuple-element.53.grad_ref, bf16[2048,1024]{1,0:T(8,128)(2,1)} %weight_ref.1, f32[256,1024]{1,0:T(8,128)} %get-tuple-element.92.gelu_ref, ...), custom_call_target="tpu_custom_call" | custom-call | flops 1073741824 | bytes 8388608 | tf_op jit(solution)/shard_map/mixer/pallas_call | solution.py:102
  257.7 7.7 %all-to-all-done.3.grads_ref = bf16[8,256,256]{2,1,0:T(8,128)(2,1)S(1)} async-done(((bf16[8,256,256]{2,1,0:T(8,128)(2,1)}), bf16[8,256,256]{2,1,0:T(8,128)(2,1)S(1)}, u32[]{:S(2)}, u32[]{:S(2)}) %all-to-all-start.3) | async-done | bytes 1048608 | tf_op jit(solution)/shard_map/all_to_all | solution.py:439
  265.4 5.5 %all-to-all-start.4 = ((f32[16,2,1024]{2,1,0:T(2,128)}), f32[16,2,1024]{2,1,0:T(2,128)S(1)}, u32[]{:S(2)}, u32[]{:S(2)}) async-start(f32[16,2,1024]{2,1,0:T(2,128)} %get-tuple-element.96), calls=%async_computation.4 | async-start | bytes 262144 | tf_op jit(solution)/shard_map/all_to_all | solution.py:446
  275.1 1.8 product.1
  277.7 2.8 collective-permute-start.13
  280.5 1.3 collective-permute-start.14
  281.8 4.9 %collective-permute-done.14.head_ref = f32[2,8,1024]{2,1,0:T(8,128)S(1)} collective-permute-done((f32[2,8,1024]{2,1,0:T(8,128)S(1)}, f32[2,8,1024]{2,1,0:T(8,128)S(1)}, u32[]{:S(2)}, u32[]{:S(2)}) %collective-permute-start.14) | collective-permute-done | bytes 65568 | tf_op jit(solution)/shard_map/ppermute | solution.py:35
  287.3 4.6 %tail.1 = bf16[256,1024]{1,0:T(8,128)(2,1)} custom-call(s32[1]{0:T(128)} %bitcast.35.where_ref, f32[16,2,1024]{2,1,0:T(2,128)} %copy-done.43, bf16[256,1024]{1,0:T(8,128)(2,1)} %get-tuple-element.97.local_ref, bf16[256,1024]{1,0:T(8,128)(2,1)} %get-tuple-element.98.cumul_ref, bf16[256,1024]{1,0:T(8,128)(2,1)} %get-tuple-element.99.to_decay_ref, ...), custom_call_target="tpu_custom_call" | custom-call | flops 268435456 | bytes 7340032 | tf_op jit(solution)/shard_map/tail/pallas_call | solution.py:183
  (160 shorter events, 25.5 us)
Async XLA Ops:
  0.6 108.6 %copy-start = (bf16[1,2048,512]{2,1,0:T(8,128)(2,1)S(1)}, bf16[1,2048,512]{2,1,0:T(8,128)(2,1)}, u32[]{:S(2)}) copy-start(bf16[1,2048,512]{2,1,0:T(8,128)(2,1)} %param.21) | copy-start | bytes 6291460
  7.8 13.9 %copy-start.52 = (f32[256,2]{0,1:T(2,128)S(1)}, f32[256,2]{0,1:T(2,128)}, u32[]{:S(2)}) copy-start(f32[256,2]{0,1:T(2,128)} %param.19) | copy-start | bytes 6148
  7.8 14.1 %copy-start.51 = (f32[1024]{0:T(1024)S(1)}, f32[1024]{0:T(1024)}, u32[]{:S(2)}) copy-start(f32[1024]{0:T(1024)} %param.30) | copy-start | bytes 12292
  7.8 14.2 %copy-start.46 = (bf16[4,1024]{1,0:T(4,128)(2,1)S(1)}, bf16[4,1024]{1,0:T(4,128)(2,1)}, u32[]{:S(2)}) copy-start(bf16[4,1024]{1,0:T(4,128)(2,1)} %taps_ref.1) | copy-start | bytes 24580
  7.8 14.8 %copy-start.2 = (bf16[256,2048]{1,0:T(8,128)(2,1)S(1)}, bf16[256,2048]{1,0:T(8,128)(2,1)}, u32[]{:S(2)}) copy-start(bf16[256,2048]{1,0:T(8,128)(2,1)} %cot_ref.1) | copy-start | bytes 3145732
  7.8 51.6 %all-to-all-start = ((bf16[16,32,2048]{2,1,0:T(8,128)(2,1)}), bf16[16,32,2048]{2,1,0:T(8,128)(2,1)}, u32[]{:S(2)}, u32[]{:S(2)}) async-start(bf16[16,32,2048]{2,1,0:T(8,128)(2,1)} %bitcast.144), calls=%async_computation | async-start | bytes 4194304 | tf_op jit(solution)/shard_map/all_to_all | solution.py:333
  17.9 10.5 %collective-permute-start = (f32[4,1024]{1,0:T(4,128)S(1)}, f32[4,1024]{1,0:T(4,128)S(1)}, u32[]{:S(2)}, u32[]{:S(2)}) collective-permute-start(f32[4,1024]{1,0:T(4,128)S(1)} %pad_maximum_fusion.2), channel_id=1, source_target_pairs={{0,2},{2,4},{4,6},{6,8},{8,10},{10,12},{12,14},{14,16},{16,18},{18... | collective-permute-start | bytes 49160 | tf_op jit(solution)/shard_map/ppermute | solution.py:35
  21.6 3.0 %copy-start.26 = (f32[256,1024]{1,0:T(8,128)S(1)}, f32[256,1024]{1,0:T(8,128)}, u32[]{:S(2)}) copy-start(f32[256,1024]{1,0:T(8,128)} %param.26) | copy-start | bytes 3145732
  21.7 3.0 %copy-start.44 = (bf16[256,1024]{1,0:T(8,128)(2,1)S(1)}, bf16[256,1024]{1,0:T(8,128)(2,1)}, u32[]{:S(2)}) copy-start(bf16[256,1024]{1,0:T(8,128)(2,1)} %param.25) | copy-start | bytes 1572868
  24.6 2.6 copy-start.42
  24.6 34.8 %copy-start.49 = (f32[1,1024]{1,0:T(1,128)S(1)}, f32[1,1024]{1,0:T(1,128)}, u32[]{:S(2)}) copy-start(f32[1,1024]{1,0:T(1,128)} %get-tuple-element.127) | copy-start | bytes 12292
  24.6 34.8 %copy-start.50 = (f32[1,1024]{1,0:T(1,128)S(1)}, f32[1,1024]{1,0:T(1,128)}, u32[]{:S(2)}) copy-start(f32[1,1024]{1,0:T(1,128)} %get-tuple-element.128) | copy-start | bytes 12292
  28.3 31.1 %copy-start.48 = (f32[4,1024]{1,0:T(4,128)}, f32[4,1024]{1,0:T(4,128)S(1)}, u32[]{:S(2)}) copy-start(f32[4,1024]{1,0:T(4,128)S(1)} %collective-permute-done) | copy-start | bytes 49156
  59.4 16.7 %copy-start.37 = (bf16[8,128,128]{2,1,0:T(8,128)(2,1)S(1)}, bf16[8,128,128]{2,1,0:T(8,128)(2,1)}, u32[]{:S(2)}) copy-start(bf16[8,128,128]{2,1,0:T(8,128)(2,1)} %input_w_ref.1) | copy-start | bytes 786436
  63.7 14.1 %copy-start.25 = (bf16[256,1024]{1,0:T(8,128)(2,1)}, bf16[256,1024]{1,0:T(8,128)(2,1)S(1)}, u32[]{:S(2)}) copy-start(bf16[256,1024]{1,0:T(8,128)(2,1)S(1)} %get-tuple-element.111) | copy-start | bytes 1572868
  78.6 19.6 %copy-start.53 = (pred[256]{0:T(512)(128)(4,1)S(1)}, pred[256]{0:T(512)(128)(4,1)}, u32[]{:S(2)}) copy-start(pred[256]{0:T(512)(128)(4,1)} %add_compare_fusion) | copy-start | bytes 772
  78.6 52.8 %all-to-all-start.1 = ((bf16[16,32,2048]{2,1,0:T(8,128)(2,1)}), bf16[16,32,2048]{2,1,0:T(8,128)(2,1)}, u32[]{:S(2)}, u32[]{:S(2)}) async-start(bf16[16,32,2048]{2,1,0:T(8,128)(2,1)} %bitcast.143), calls=%async_computation.1 | async-start | bytes 4194304 | tf_op jit(solution)/shard_map/all_to_all | solution.py:350
  90.8 22.3 %collective-permute-start.1 = (bf16[512,2048]{1,0:T(8,128)(2,1)}, bf16[512,2048]{1,0:T(8,128)(2,1)S(1)}, u32[]{:S(2)}, u32[]{:S(2)}) collective-permute-start(bf16[512,2048]{1,0:T(8,128)(2,1)} %bitcast.3), channel_id=1, source_target_pairs={{0,1},{1,0},{2,3},{3,2},{4,5},{5,4},{6,7},{7,6},{8,9},{9,8},{10,11... | collective-permute-start | bytes 6291464 | tf_op jit(solution)/shard_map/ppermute | solution.py:40
  103.6 1.8 copy-start.23
  113.1 2.2 copy-start.21
  131.3 5.4 %copy-start.38 = (f32[512,512]{1,0:T(8,128)S(1)}, f32[512,512]{1,0:T(8,128)}, u32[]{:S(2)}) copy-start(f32[512,512]{1,0:T(8,128)} %fusion.14) | copy-start | bytes 3145732
  131.3 5.4 %copy-start.40 = (f32[512,512]{1,0:T(8,128)S(1)}, f32[512,512]{1,0:T(8,128)}, u32[]{:S(2)}) copy-start(f32[512,512]{1,0:T(8,128)} %fusion.7) | copy-start | bytes 3145732
  131.3 5.4 %copy-start.54 = (bf16[1,512,2048]{2,1,0:T(8,128)(2,1)S(1)}, bf16[1,512,2048]{2,1,0:T(8,128)(2,1)}, u32[]{:S(2)}) copy-start(bf16[1,512,2048]{2,1,0:T(8,128)(2,1)} %param.22) | copy-start | bytes 6291460
  131.3 5.4 %collective-permute-start.2 = (bf16[512,2048]{1,0:T(8,128)(2,1)}, bf16[512,2048]{1,0:T(8,128)(2,1)S(1)}, u32[]{:S(2)}, u32[]{:S(2)}) collective-permute-start(bf16[512,2048]{1,0:T(8,128)(2,1)} %bitcast.29), channel_id=1, source_target_pairs={{0,1},{1,0},{2,3},{3,2},{4,5},{5,4},{6,7},{7,6},{8,9},{9,8},{10,11... | collective-permute-start | bytes 6291464 | tf_op jit(solution)/shard_map/ppermute | solution.py:40
  136.7 5.8 %copy-start.27 = (bf16[512,512]{1,0:T(8,128)(2,1)}, bf16[512,512]{1,0:T(8,128)(2,1)S(1)}, u32[]{:S(2)}) copy-start(bf16[512,512]{1,0:T(8,128)(2,1)S(1)} %get-tuple-element.69) | copy-start | bytes 1572868
  136.7 9.6 %copy-start.34 = (bf16[512,512]{1,0:T(8,128)(2,1)}, bf16[512,512]{1,0:T(8,128)(2,1)S(1)}, u32[]{:S(2)}) copy-start(bf16[512,512]{1,0:T(8,128)(2,1)S(1)} %get-tuple-element.68) | copy-start | bytes 1572868
  136.7 1.7 copy-start.32
  136.8 2.7 copy-start.24
  138.5 2.3 copy-start.29
  138.5 2.3 copy-start.31
  142.1 4.2 %collective-permute-start.3 = (bf16[512,2048]{1,0:T(8,128)(2,1)S(1)}, bf16[512,2048]{1,0:T(8,128)(2,1)S(1)}, u32[]{:S(2)}, u32[]{:S(2)}) collective-permute-start(bf16[512,2048]{1,0:T(8,128)(2,1)S(1)} %add_convert_fusion.4), channel_id=1, source_target_pairs={{0,1},{1,0},{2,3},{3,2},{4,5},{5,4},{6,7},{7,6},{8,9},{9,8},{10,11... | collective-permute-start | bytes 6291464 | tf_op jit(solution)/shard_map/ppermute | solution.py:40
  149.2 10.0 %copy-start.3 = (bf16[256,1024]{1,0:T(8,128)(2,1)S(1)}, bf16[256,1024]{1,0:T(8,128)(2,1)}, u32[]{:S(2)}) copy-start(bf16[256,1024]{1,0:T(8,128)(2,1)} %get-tuple-element.81.refs_0_) | copy-start | bytes 1572868
  149.2 88.6 %all-to-all-start.2 = ((bf16[16,32,2048]{2,1,0:T(8,128)(2,1)}), bf16[16,32,2048]{2,1,0:T(8,128)(2,1)}, u32[]{:S(2)}, u32[]{:S(2)}) async-start(bf16[16,32,2048]{2,1,0:T(8,128)(2,1)} %bitcast.145), calls=%async_computation.2 | async-start | bytes 4194304 | tf_op jit(solution)/shard_map/all_to_all | solution.py:422
  159.3 53.5 %copy-start.28 = (bf16[512,512]{1,0:T(8,128)(2,1)S(1)}, bf16[512,512]{1,0:T(8,128)(2,1)}, u32[]{:S(2)}) copy-start(bf16[512,512]{1,0:T(8,128)(2,1)} %copy-done.27) | copy-start | bytes 1572868
  159.3 47.6 %collective-permute-start.8 = (bf16[256,1024]{1,0:T(8,128)(2,1)S(1)}, bf16[256,1024]{1,0:T(8,128)(2,1)S(1)}, u32[]{:S(2)}, u32[]{:S(2)}) collective-permute-start(bf16[256,1024]{1,0:T(8,128)(2,1)S(1)} %copy-done.3), channel_id=1, source_target_pairs={{0,8},{2,10},{4,12},{6,14},{8,0},{10,2},{12,4},{14,6},{16,24},{18,... | collective-permute-start | bytes 1572872 | tf_op jit(solution)/shard_map/ppermute | solution.py:40
  161.2 61.9 %collective-permute-start.5 = (bf16[256,1024]{1,0:T(8,128)(2,1)S(1)}, bf16[256,1024]{1,0:T(8,128)(2,1)S(1)}, u32[]{:S(2)}, u32[]{:S(2)}) collective-permute-start(bf16[256,1024]{1,0:T(8,128)(2,1)S(1)} %copy-done.3), channel_id=1, source_target_pairs={{0,2},{2,0},{4,6},{6,4},{8,10},{10,8},{12,14},{14,12},{16,18},{18,... | collective-permute-start | bytes 1572872 | tf_op jit(solution)/shard_map/ppermute | solution.py:40
  162.7 62.9 %collective-permute-start.6 = (bf16[256,1024]{1,0:T(8,128)(2,1)S(1)}, bf16[256,1024]{1,0:T(8,128)(2,1)S(1)}, u32[]{:S(2)}, u32[]{:S(2)}) collective-permute-start(bf16[256,1024]{1,0:T(8,128)(2,1)S(1)} %copy-done.3), channel_id=1, source_target_pairs={{0,4},{2,6},{4,0},{6,2},{8,12},{10,14},{12,8},{14,10},{16,20},{18,... | collective-permute-start | bytes 1572872 | tf_op jit(solution)/shard_map/ppermute | solution.py:40
  164.1 67.1 %collective-permute-start.7 = (bf16[256,1024]{1,0:T(8,128)(2,1)S(1)}, bf16[256,1024]{1,0:T(8,128)(2,1)S(1)}, u32[]{:S(2)}, u32[]{:S(2)}) collective-permute-start(bf16[256,1024]{1,0:T(8,128)(2,1)S(1)} %copy-done.3), channel_id=1, source_target_pairs={{0,6},{2,4},{4,2},{6,0},{8,14},{10,12},{12,10},{14,8},{16,22},{18,... | collective-permute-start | bytes 1572872 | tf_op jit(solution)/shard_map/ppermute | solution.py:40
  206.9 16.2 %copy-start.7 = (bf16[256,1024]{1,0:T(8,128)(2,1)}, bf16[256,1024]{1,0:T(8,128)(2,1)S(1)}, u32[]{:S(2)}) copy-start(bf16[256,1024]{1,0:T(8,128)(2,1)S(1)} %collective-permute-done.8.refs_4_) | copy-start | bytes 1572868
  206.9 26.8 %collective-permute-start.10 = (bf16[256,1024]{1,0:T(8,128)(2,1)S(1)}, bf16[256,1024]{1,0:T(8,128)(2,1)S(1)}, u32[]{:S(2)}, u32[]{:S(2)}) collective-permute-start(bf16[256,1024]{1,0:T(8,128)(2,1)S(1)} %collective-permute-done.8.refs_4_), channel_id=1, source_target_pairs={{0,4},{2,6},{4,0},{6,2},{8,12},{10,14},{12,8},{14,10},{16,20},{18,... | collective-permute-start | bytes 1572872 | tf_op jit(solution)/shard_map/ppermute | solution.py:40
  209.4 25.1 %collective-permute-start.11 = (bf16[256,1024]{1,0:T(8,128)(2,1)S(1)}, bf16[256,1024]{1,0:T(8,128)(2,1)S(1)}, u32[]{:S(2)}, u32[]{:S(2)}) collective-permute-start(bf16[256,1024]{1,0:T(8,128)(2,1)S(1)} %collective-permute-done.8.refs_4_), channel_id=1, source_target_pairs={{0,6},{2,4},{4,2},{6,0},{8,14},{10,12},{12,10},{14,8},{16,22},{18,... | collective-permute-start | bytes 1572872 | tf_op jit(solution)/shard_map/ppermute | solution.py:40
  212.8 4.5 %copy-start.22 = (bf16[512,2048]{1,0:T(8,128)(2,1)S(1)}, bf16[512,2048]{1,0:T(8,128)(2,1)}, u32[]{:S(2)}) copy-start(bf16[512,2048]{1,0:T(8,128)(2,1)} %copy-done.21) | copy-start | bytes 6291460
  212.8 4.5 %copy-start.30 = (bf16[512,512]{1,0:T(8,128)(2,1)S(1)}, bf16[512,512]{1,0:T(8,128)(2,1)}, u32[]{:S(2)}) copy-start(bf16[512,512]{1,0:T(8,128)(2,1)} %copy-done.29) | copy-start | bytes 1572868
  217.3 1.3 copy-start.35
  218.6 5.6 %copy-start.33 = (bf16[512,2048]{1,0:T(8,128)(2,1)S(1)}, bf16[512,2048]{1,0:T(8,128)(2,1)}, u32[]{:S(2)}) copy-start(bf16[512,2048]{1,0:T(8,128)(2,1)} %copy-done.32) | copy-start | bytes 6291460
  218.6 5.6 %copy-start.39 = (f32[512,512]{1,0:T(8,128)S(1)}, f32[512,512]{1,0:T(8,128)}, u32[]{:S(2)}) copy-start(f32[512,512]{1,0:T(8,128)} %fusion.14) | copy-start | bytes 3145732
  218.6 5.6 %copy-start.41 = (f32[512,512]{1,0:T(8,128)S(1)}, f32[512,512]{1,0:T(8,128)}, u32[]{:S(2)}) copy-start(f32[512,512]{1,0:T(8,128)} %fusion.7) | copy-start | bytes 3145732
  223.1 3.8 %copy-start.36 = (bf16[512,512]{1,0:T(8,128)(2,1)S(1)}, bf16[512,512]{1,0:T(8,128)(2,1)}, u32[]{:S(2)}) copy-start(bf16[512,512]{1,0:T(8,128)(2,1)} %get-tuple-element.74) | copy-start | bytes 1572868
  223.1 2.5 copy-start.9
  223.1 13.6 %collective-permute-start.9 = (bf16[256,1024]{1,0:T(8,128)(2,1)S(1)}, bf16[256,1024]{1,0:T(8,128)(2,1)S(1)}, u32[]{:S(2)}, u32[]{:S(2)}) collective-permute-start(bf16[256,1024]{1,0:T(8,128)(2,1)S(1)} %collective-permute-done.8.refs_4_), channel_id=1, source_target_pairs={{0,2},{2,0},{4,6},{6,4},{8,10},{10,8},{12,14},{14,12},{16,18},{18,... | collective-permute-start | bytes 1572872 | tf_op jit(solution)/shard_map/ppermute | solution.py:40
  225.6 5.6 %copy-start.11 = (bf16[256,1024]{1,0:T(8,128)(2,1)}, bf16[256,1024]{1,0:T(8,128)(2,1)S(1)}, u32[]{:S(2)}) copy-start(bf16[256,1024]{1,0:T(8,128)(2,1)S(1)} %collective-permute-done.6.refs_2_) | copy-start | bytes 1572868
  225.6 12.2 %collective-permute-start.4 = (f32[3,8,1024]{2,1,0:T(8,128)S(1)}, f32[3,8,1024]{2,1,0:T(8,128)S(1)}, u32[]{:S(2)}, u32[]{:S(2)}) collective-permute-start(f32[3,8,1024]{2,1,0:T(8,128)S(1)} %pad_maximum_fusion.1), channel_id=1, source_target_pairs={{2,0},{4,2},{6,4},{8,6},{10,8},{12,10},{14,12},{16,14},{18,16},{20... | collective-permute-start | bytes 294920 | tf_op jit(solution)/shard_map/ppermute | solution.py:35
  240.8 2.7 collective-permute-start.12
  246.3 19.1 %all-to-all-start.3 = ((bf16[8,256,256]{2,1,0:T(8,128)(2,1)}), bf16[8,256,256]{2,1,0:T(8,128)(2,1)S(1)}, u32[]{:S(2)}, u32[]{:S(2)}) async-start(bf16[8,256,256]{2,1,0:T(8,128)(2,1)} %copy-done.4), calls=%async_computation.3 | async-start | bytes 2097152 | tf_op jit(solution)/shard_map/all_to_all | solution.py:439
  250.5 20.4 %copy-start.10 = (bf16[256,1024]{1,0:T(8,128)(2,1)S(1)}, bf16[256,1024]{1,0:T(8,128)(2,1)}, u32[]{:S(2)}) copy-start(bf16[256,1024]{1,0:T(8,128)(2,1)} %copy-done.9) | copy-start | bytes 1572868
  250.5 20.4 %copy-start.12 = (bf16[256,1024]{1,0:T(8,128)(2,1)S(1)}, bf16[256,1024]{1,0:T(8,128)(2,1)}, u32[]{:S(2)}) copy-start(bf16[256,1024]{1,0:T(8,128)(2,1)} %copy-done.11) | copy-start | bytes 1572868
  250.6 20.4 %copy-start.14 = (bf16[256,1024]{1,0:T(8,128)(2,1)S(1)}, bf16[256,1024]{1,0:T(8,128)(2,1)}, u32[]{:S(2)}) copy-start(bf16[256,1024]{1,0:T(8,128)(2,1)} %copy-done.13) | copy-start | bytes 1572868
  265.4 21.2 %all-to-all-start.4 = ((f32[16,2,1024]{2,1,0:T(2,128)}), f32[16,2,1024]{2,1,0:T(2,128)S(1)}, u32[]{:S(2)}, u32[]{:S(2)}) async-start(f32[16,2,1024]{2,1,0:T(2,128)} %get-tuple-element.96), calls=%async_computation.4 | async-start | bytes 262144 | tf_op jit(solution)/shard_map/all_to_all | solution.py:446
  270.9 1.0 copy-start.8
  275.1 5.4 %copy-start.55 = (f32[2,8,1024]{2,1,0:T(8,128)S(1)}, f32[2,8,1024]{2,1,0:T(8,128)}, u32[]{:S(2)}) copy-start(f32[2,8,1024]{2,1,0:T(8,128)} %get-tuple-element.102) | copy-start | bytes 196612
  277.7 15.0 %copy-start.6 = (f32[128,1024]{1,0:T(8,128)S(1)}, f32[128,1024]{1,0:T(8,128)}, u32[]{:S(2)}) copy-start(f32[128,1024]{1,0:T(8,128)} %copy-done.5) | copy-start | bytes 1572868
  277.7 15.0 %collective-permute-start.13 = (bf16[128,1024]{1,0:T(8,128)(2,1)S(1)}, bf16[128,1024]{1,0:T(8,128)(2,1)S(1)}, u32[]{:S(2)}, u32[]{:S(2)}) collective-permute-start(bf16[128,1024]{1,0:T(8,128)(2,1)S(1)} %get-tuple-element.90), channel_id=1, source_target_pairs={{0,16},{2,18},{4,20},{6,22},{8,24},{10,26},{12,28},{14,30},{16,0},... | collective-permute-start | bytes 786440 | tf_op jit(solution)/shard_map/ppermute | solution.py:40
  280.5 6.1 %collective-permute-start.14 = (f32[2,8,1024]{2,1,0:T(8,128)S(1)}, f32[2,8,1024]{2,1,0:T(8,128)S(1)}, u32[]{:S(2)}, u32[]{:S(2)}) collective-permute-start(f32[2,8,1024]{2,1,0:T(8,128)S(1)} %copy-done.55), channel_id=1, source_target_pairs={{2,0},{4,2},{6,4},{8,6},{10,8},{12,10},{14,12},{16,14},{18,16},{20... | collective-permute-start | bytes 196616 | tf_op jit(solution)/shard_map/ppermute | solution.py:35
  286.7 6.9 %copy-start.1 = (bf16[1,2048,512]{2,1,0:T(8,128)(2,1)S(1)}, bf16[1,2048,512]{2,1,0:T(8,128)(2,1)}, u32[]{:S(2)}) copy-start(bf16[1,2048,512]{2,1,0:T(8,128)(2,1)} %param.21) | copy-start | bytes 6291460
  (12 other events, 10.0 us)

commit v4 on v3

--- a/solution.py
+++ b/solution.py
@@ -331,6 +331,8 @@
     send_rows, late = lax.optimization_barrier((send_rows, late))
     gate_input, states, recur_input, cotangent_late, route_weight = late
     got_rows = lax.all_to_all(send_rows, "sp", split_axis=0, concat_axis=0, tiled=True)
+    own_weights = (gate_proj[0], up_proj[0], down_proj[0])
+    other_weights = tuple(swapped(weight, "tp", 1) for weight in own_weights)
     edge = jnp.concatenate([recur_input[-3:].astype(f32), states[-1:]], axis=0)
     edge = shifted(edge, "sp", 1)
     slot_weight = jnp.sum(jnp.where(hits, route_weight[None, :, :], 0.0), axis=(1, 2))
@@ -382,45 +384,48 @@
 
     rows_here = got_rows.reshape(own_slots, width)
     rows_there = swapped(rows_here, "tp", 1)
-    weight_gate = gate_proj[0]
-    weight_up = up_proj[0]
-    weight_down = down_proj[0]
-    pres = tuple(
-        (times(rows, weight_gate), times(rows, weight_up)) for rows in (rows_here, rows_there)
-    )
+    rows_here, rows_there = lax.optimization_barrier((rows_here, rows_there))
+
+    def first_half(gate_w, up_w):
+        gate_pre = times(rows_here, gate_w)
+        up_pre = times(rows_here, up_w)
+        sigmoid_gate = jax.nn.sigmoid(gate_pre)
+        silu_gate = gate_pre * sigmoid_gate
+        slope_gate = up_pre * sigmoid_gate * (1.0 + gate_pre * (1.0 - sigmoid_gate))
+        return (silu_gate * up_pre).astype(bf16), silu_gate.astype(bf16), slope_gate.astype(bf16)
+
+    pres = tuple(first_half(weights[0], weights[1]) for weights in (own_weights, other_weights))
     head_coef = jnp.stack([to_decay[:8], to_input[:8], direct[:8]])
     gates = (
         next_decay, decay_value[:1], head_coef,
         to_decay.astype(bf16), to_input.astype(bf16), direct.astype(bf16),
     )
-    got_grads, pres, rows_there, gates = lax.optimization_barrier((got_grads, pres, rows_there, gates))
+    got_grads, pres, gates = lax.optimization_barrier((got_grads, pres, gates))
     next_decay, first_decay, head_coef, to_decay, to_input, direct = gates
     for k in range(1, half):
         mixers[k ^ half] = swapped(mixers[half], "sp", k)
     grads_here = got_grads.reshape(own_slots, width)
-    grads_there = swapped(grads_here, "tp", 1)
-
-    def expert(pre, grads_in):
-        gate_pre, up_pre = pre
-        sigmoid_gate = jax.nn.sigmoid(gate_pre)
-        silu_gate = gate_pre * sigmoid_gate
-        hidden = (silu_gate * up_pre).astype(bf16)
-        hidden_grad = cols_of(grads_in, weight_down)
-        gate_pre_grad = (
-            hidden_grad * up_pre * sigmoid_gate * (1.0 + gate_pre * (1.0 - sigmoid_gate))
-        ).astype(bf16)
-        up_pre_grad = (hidden_grad * silu_gate).astype(bf16)
-        return hidden, gate_pre_grad, up_pre_grad
-
-    hidden_h, gate_h, up_h = expert(pres[0], grads_here)
-    grads_there, hidden_h, gate_h, up_h = lax.optimization_barrier((grads_there, hidden_h, gate_h, up_h))
-    hidden_t, gate_t, up_t = expert(pres[1], grads_there)
-    partial_t = cols_of(gate_t, weight_gate) + cols_of(up_t, weight_up)
-    from_there = swapped(partial_t.astype(bf16), "tp", 1)
-    partial_h = cols_of(gate_h, weight_gate) + cols_of(up_h, weight_up)
-    shared = (partial_h + from_there.astype(f32)).astype(bf16).reshape(experts, share, width)
+
+    def second_half(pre, down_w):
+        hidden_grad = cols_of(grads_here, down_w)
+        return (hidden_grad * pre[2].astype(f32)).astype(bf16), (hidden_grad * pre[1].astype(f32)).astype(bf16)
+
+    own_grads = second_half(pres[0], own_weights[2])
+    other_grads = second_half(pres[1], other_weights[2])
+    partial = (
+        cols_of(own_grads[0], own_weights[0])
+        + cols_of(own_grads[1], own_weights[1])
+        + cols_of(other_grads[0], other_weights[0])
+        + cols_of(other_grads[1], other_weights[1])
+    )
+    shared = partial.astype(bf16).reshape(experts, share, width)
     back = lax.all_to_all(shared, "sp", split_axis=0, concat_axis=0, tiled=True)
     head_coef = shifted(head_coef, "sp", -1)
+    hidden_h, gate_h, up_h = pres[0][0], own_grads[0], own_grads[1]
+    grads_there = swapped(grads_here, "tp", 1)
+    hidden_t = swapped(pres[1][0], "tp", 1)
+    gate_t = swapped(other_grads[0], "tp", 1)
+    up_t = swapped(other_grads[1], "tp", 1)
     down_grad = rows_of(hidden_h, grads_here) + rows_of(hidden_t, grads_there)
     gate_weight_grad = rows_of(rows_here, gate_h) + rows_of(rows_there, gate_t)
     up_weight_grad = rows_of(rows_here, up_h) + rows_of(rows_there, up_t)

time: 299 us -> 308 us (1.030)
  matrix products: 75.6 us -> 79.6 us
  waiting for transfers between devices: 109 us -> 113 us
  starting transfers between devices: 58 us -> 61.2 us
    dot_general x35, matrix products: 75.6 us -> 79.6 us  [dot(): lax.dot_general(left, right, (contract, ((), ())), preferred_element_type...]
    ppermute x12 -> x17, starting transfers between devices: 12.7 us -> 15.5 us  [swapped(): return lax.ppermute(value, axis, [(s, s ^ mask) for s in range(count)])]
    unnamed x113 -> x77, local copies, waits for them, and re-layouts: 12.6 us -> 10.8 us
    ppermute x12 -> x17, waiting for transfers between devices: 51.3 us -> 52.3 us  [swapped(): return lax.ppermute(value, axis, [(s, s ^ mask) for s in range(count)])]
  transfers between devices with their start and end apart: 20 -> 25, of which waited for: 11 -> 11; matrix products, arithmetic and copies ran while one was open for 21% -> 27% of each run, Pallas kernels for 5% -> 4%
where the time goes in v4:
time: 308 us; the launch traced here: 302 us
  waiting for transfers between devices  113 us (37%)
  matrix products  79.6 us (26%)
  starting transfers between devices  61.2 us (20%)
  other arithmetic  17.5 us (6%)
  Pallas kernels  15.4 us (5%)
  local copies, waits for them, and re-layouts  14.7 us (5%)
    dot_general x35, matrix products, dot(): lax.dot_general(left, right, (contract, ((), ())), preferred_element_type...  79.6 us
    ppermute x17, waiting for transfers between devices, swapped(): return lax.ppermute(value, axis, [(s, s ^ mask) for s in range(count)])  52.3 us
    all_to_all x1, waiting for transfers between devices, on_device(): lax.all_to_all(send_rows, 'sp', split_axis=0, concat_axis=0, tiled=True)  30.8 us
    all_to_all x1, waiting for transfers between devices, on_device(): lax.all_to_all(send_grads, 'sp', split_axis=0, concat_axis=0, tiled=True)  16.5 us
    ppermute x17, starting transfers between devices, swapped(): return lax.ppermute(value, axis, [(s, s ^ mask) for s in range(count)])  15.5 us
    all_to_all x1, starting transfers between devices, on_device(): back = lax.all_to_all(shared, 'sp', split_axis=0, concat_axis=0, tiled=True)  11 us
    unnamed x77, local copies, waits for them, and re-layouts  10.8 us
    all_to_all x1, starting transfers between devices, on_device(): lax.all_to_all(send_grads, 'sp', split_axis=0, concat_axis=0, tiled=True)  10.5 us
  transfers between devices with their start and end apart: 25, of which 11 were waited for; matrix products, arithmetic and copies ran while one was open for 27% of the time, Pallas kernels for 4%

profile of v4, /device:TPU:0, one launch (start us, length us, event | category | flops | bytes accessed | tf_op | source)
XLA Modules:
  0.0 302.5 jit_solution(10560288931700802911)
XLA Ops:
  1.9 1.2 reduce-window.6
  4.5 2.0 convolution_convert_fusion
  6.5 8.7 %all-to-all-start = ((bf16[16,32,2048]{2,1,0:T(8,128)(2,1)}), bf16[16,32,2048]{2,1,0:T(8,128)(2,1)}, u32[]{:S(2)}, u32[]{:S(2)}) async-start(bf16[16,32,2048]{2,1,0:T(8,128)(2,1)} %bitcast.135), calls=%async_computation | async-start | bytes 4194304 | tf_op jit(solution)/shard_map/all_to_all | solution.py:333
  15.3 3.8 %collective-permute-start = (f32[4,1024]{1,0:T(4,128)S(1)}, f32[4,1024]{1,0:T(4,128)S(1)}, u32[]{:S(2)}, u32[]{:S(2)}) collective-permute-start(f32[4,1024]{1,0:T(4,128)S(1)} %pad_maximum_fusion.2), channel_id=1, source_target_pairs={{0,2},{2,4},{4,6},{6,8},{8,10},{10,12},{12,14},{14,16},{16,18},{18... | collective-permute-start | bytes 49160 | tf_op jit(solution)/shard_map/ppermute | solution.py:35
  20.6 2.0 multiply_convert_fusion
  22.7 3.1 %multiply_convert_fusion.1 = (bf16[256,1024]{1,0:T(8,128)(2,1)S(1)}, f32[256,1024]{1,0:T(8,128)}, f32[256,1024]{1,0:T(8,128)}) fusion(f32[256,1024]{1,0:T(8,128)S(1)} %copy-done.15, bf16[256,1024]{1,0:T(8,128)(2,1)} %param.25), kind=kLoop, calls=%fused_computation.58 | loop fusion | flops 5767168 | bytes 4194304 | tf_op jit(solution)/shard_map/convert_element_type | solution.py:345
  26.4 1.1 convert_element_type.114
  27.5 30.8 %all-to-all-done = bf16[16,32,2048]{2,1,0:T(8,128)(2,1)} async-done(((bf16[16,32,2048]{2,1,0:T(8,128)(2,1)}), bf16[16,32,2048]{2,1,0:T(8,128)(2,1)}, u32[]{:S(2)}, u32[]{:S(2)}) %all-to-all-start) | async-done | bytes 2097184 | tf_op jit(solution)/shard_map/all_to_all | solution.py:333
  58.3 4.2 %fusion.106 = (bf16[256,1024]{1,0:T(8,128)(2,1)S(1)}, f32[256,1024]{1,0:T(8,128)}) fusion(f32[256,1024]{1,0:T(8,128)} %convert_element_type.114, f32[1024]{0:T(1024)} %bitcast.146, f32[3,1024]{1,0:T(4,128)} %bitcast.142, f32[1024]{0:T(1024)S(1)} %bitcast.145, f32[1024]{0:T(1024)S(1)} %bitcast.144, f32[1024]{0:T(1024)S(1)} %bitcast.143), kind=kLoop, calls=%fused_computation.174 | loop fusion | flops 2883584 | bytes 2650112 | tf_op jit(solution)/shard_map/convert_element_type | solution.py:362
  62.5 1.6 convolution_dynamic-update-slice_fusion.15
  64.1 1.6 convolution_dynamic-update-slice_fusion.14
  65.7 1.6 convolution_dynamic-update-slice_fusion.13
  67.2 1.6 convolution_dynamic-update-slice_fusion.12
  68.8 1.6 convolution_dynamic-update-slice_fusion.11
  70.3 1.6 convolution_dynamic-update-slice_fusion.10
  71.9 1.6 convolution_dynamic-update-slice_fusion.9
  73.4 1.6 convolution_dynamic-update-slice_fusion.8
  78.2 10.5 %all-to-all-start.1 = ((bf16[16,32,2048]{2,1,0:T(8,128)(2,1)}), bf16[16,32,2048]{2,1,0:T(8,128)(2,1)}, u32[]{:S(2)}, u32[]{:S(2)}) async-start(bf16[16,32,2048]{2,1,0:T(8,128)(2,1)} %bitcast.134), calls=%async_computation.1 | async-start | bytes 4194304 | tf_op jit(solution)/shard_map/all_to_all | solution.py:352
  92.6 5.2 %fusion.104 = (bf16[256,1024]{1,0:T(8,128)(2,1)}, f32[256,1024]{1,0:T(8,128)S(1)}, bf16[256,1024]{1,0:T(8,128)(2,1)}, f32[256,1024]{1,0:T(8,128)S(1)}, bf16[256,...) fusion(f32[256,1024]{1,0:T(8,128)} %get-tuple-element.110, ...), kind=kLoop, calls=%fused_computation.173 | loop fusion | flops 8126464 | bytes 11014400 | tf_op jit(solution)/shard_map/convert_element_type | solution.py:401
  98.5 1.1 concatenate.21.next_ref
  99.7 3.0 fusion.94
  102.7 4.1 %multiply_convert_fusion.8 = (bf16[512,512]{1,0:T(8,128)(2,1)S(1)}, bf16[512,512]{1,0:T(8,128)(2,1)}, bf16[512,512]{1,0:T(8,128)(2,1)S(1)}) fusion(f32[512,512]{1,0:T(8,128)S(1)} %fusion.94, bf16[512,2048]{1,0:T(8,128)(2,1)} %bitcast.3, bf16[1,2048,512]{2,1,0:T(8,128)(2,1)S(1)} %copy-done.20), kind=kOutput, calls=%fused_computation.72 | convolution fusion | flops 1077149696 | bytes 6815744 | tf_op jit(solution)/shard_map/dot_general | solution.py:17
  106.7 3.7 %fusion.109 = f32[512,512]{1,0:T(8,128)S(1)} fusion(bf16[512,2048]{1,0:T(8,128)(2,1)} %bitcast.3, bf16[2048,512]{1,0:T(8,128)(2,1)} %collective-permute-done.3), kind=kOutput, calls=%fused_computation.176 | convolution fusion | flops 1073741824 | bytes 5242880 | tf_op jit(solution)/shard_map/dot_general | solution.py:17
  110.4 4.8 %multiply_convert_fusion.6 = (bf16[512,512]{1,0:T(8,128)(2,1)S(1)}, bf16[512,512]{1,0:T(8,128)(2,1)}, bf16[512,512]{1,0:T(8,128)(2,1)}) fusion(f32[512,512]{1,0:T(8,128)S(1)} %fusion.109, bf16[512,2048]{1,0:T(8,128)(2,1)} %bitcast.3, bf16[2048,512]{1,0:T(8,128)(2,1)} %collective-permute-done.2), kind=kOutput, calls=%fused_computation.68 | convolution fusion | flops 1077149696 | bytes 6815744 | tf_op jit(solution)/shard_map/dot_general | solution.py:17
  115.2 16.5 %all-to-all-done.1 = bf16[16,32,2048]{2,1,0:T(8,128)(2,1)} async-done(((bf16[16,32,2048]{2,1,0:T(8,128)(2,1)}), bf16[16,32,2048]{2,1,0:T(8,128)(2,1)}, u32[]{:S(2)}, u32[]{:S(2)}) %all-to-all-start.1) | async-done | bytes 2097184 | tf_op jit(solution)/shard_map/all_to_all | solution.py:352
  131.7 3.6 %fusion.90 = f32[512,512]{1,0:T(8,128)S(1)} fusion(bf16[512,2048]{1,0:T(8,128)(2,1)} %bitcast.29, bf16[1,512,2048]{2,1,0:T(8,128)(2,1)} %param.22), kind=kOutput, calls=%fused_computation.160 | convolution fusion | flops 1073741824 | bytes 5242880 | tf_op jit(solution)/shard_map/dot_general | solution.py:17
  135.4 1.3 fusion.92
  137.4 1.3 fusion.96
  138.7 4.3 %multiply_convert_fusion.3 = (bf16[512,512]{1,0:T(8,128)(2,1)S(1)}, bf16[512,512]{1,0:T(8,128)(2,1)}) fusion(bf16[512,512]{1,0:T(8,128)(2,1)S(1)} %get-tuple-element.68, bf16[512,512]{1,0:T(8,128)(2,1)S(1)} %copy-done.37, bf16[512,2048]{1,0:T(8,128)(2,1)} %bitcast.29, bf16[512,2048]{1,0:T(8,128)(2,1)} %collective-permute-done.4), kind=kOutput, calls=%fused_computation.60 | convolution fusion | flops 1075314688 | bytes 6291456 | tf_op jit(solution)/shard_map/dot_general | solution.py:17
  143.1 3.1 %fusion.110 = f32[512,2048]{1,0:T(8,128)S(1)} fusion(bf16[512,512]{1,0:T(8,128)(2,1)S(1)} %get-tuple-element.122, bf16[2048,512]{1,0:T(8,128)(2,1)} %collective-permute-done.2), kind=kOutput, calls=%fused_computation.177 | convolution fusion | flops 1073741824 | bytes 6815744 | tf_op jit(solution)/shard_map/dot_general | solution.py:17
  146.1 4.8 %add_convert_fusion.3 = bf16[512,2048]{1,0:T(8,128)(2,1)} fusion(f32[512,2048]{1,0:T(8,128)S(1)} %fusion.110, f32[512,2048]{1,0:T(8,128)S(1)} %fusion.96, f32[512,2048]{1,0:T(8,128)S(1)} %fusion.92, bf16[512,512]{1,0:T(8,128)(2,1)} %get-tuple-element.123, bf16[2048,512]{1,0:T(8,128)(2,1)} %collective-permute-done.3), kind=kOutput, calls=%fused_computation.3 | convolution fusion | flops 1077936128 | bytes 17301504 | tf_op jit(solution)/shard_map/dot_general | solution.py:17
  150.9 11.0 %all-to-all-start.2 = ((bf16[16,32,2048]{2,1,0:T(8,128)(2,1)}), bf16[16,32,2048]{2,1,0:T(8,128)(2,1)}, u32[]{:S(2)}, u32[]{:S(2)}) async-start(bf16[16,32,2048]{2,1,0:T(8,128)(2,1)} %bitcast.133), calls=%async_computation.2 | async-start | bytes 4194304 | tf_op jit(solution)/shard_map/all_to_all | solution.py:422
  162.0 1.9 collective-permute-start.13
  163.9 1.5 collective-permute-start.10
  165.9 3.1 %fusion.113 = f32[512,2048]{1,0:T(8,128)S(1)} fusion(bf16[512,512]{1,0:T(8,128)(2,1)} %get-tuple-element.71, bf16[512,2048]{1,0:T(8,128)(2,1)} %bitcast.29), kind=kOutput, calls=%fused_computation.180 | convolution fusion | flops 1073741824 | bytes 6815744 | tf_op jit(solution)/shard_map/dot_general | solution.py:17
  169.0 1.5 collective-permute-start.11
  170.5 2.9 fusion.112
  173.5 3.0 fusion.111
  176.5 4.3 %add_convert_fusion.1 = bf16[2048,512]{1,0:T(8,128)(2,1)} fusion(f32[2048,512]{1,0:T(8,128)S(1)} %fusion.112, bf16[512,2048]{1,0:T(8,128)(2,1)} %bitcast.3, f32[512,512]{1,0:T(8,128)S(1)} %copy-done.14, bf16[512,512]{1,0:T(8,128)(2,1)S(1)} %copy-done.17), kind=kOutput, calls=%fused_computation.1 | convolution fusion | flops 1076625408 | bytes 9961472 | tf_op jit(solution)/shard_map/dot_general | solution.py:17
  180.9 27.7 %collective-permute-done.13.refs_4_ = bf16[256,1024]{1,0:T(8,128)(2,1)S(1)} collective-permute-done((bf16[256,1024]{1,0:T(8,128)(2,1)S(1)}, bf16[256,1024]{1,0:T(8,128)(2,1)S(1)}, u32[]{:S(2)}, u32[]{:S(2)}) %collective-permute-start.13) | collective-permute-done | bytes 524320 | tf_op jit(solution)/shard_map/ppermute | solution.py:40
  208.6 2.9 collective-permute-start.12
  211.6 1.1 collective-permute-start.14
  212.6 2.4 collective-permute-start.16
  215.1 4.3 %add_convert_fusion.2 = bf16[2048,512]{1,0:T(8,128)(2,1)} fusion(f32[2048,512]{1,0:T(8,128)S(1)} %fusion.111, bf16[512,2048]{1,0:T(8,128)(2,1)} %bitcast.3, f32[512,512]{1,0:T(8,128)S(1)} %copy-done.14, bf16[512,512]{1,0:T(8,128)(2,1)S(1)} %get-tuple-element.66), kind=kOutput, calls=%fused_computation.2 | convolution fusion | flops 1076625408 | bytes 9961472 | tf_op jit(solution)/shard_map/dot_general | solution.py:17
  219.4 1.3 collective-permute-start.9
  220.7 2.7 add_convert_fusion
  223.4 2.7 collective-permute-done.12.refs_3_
  226.8 10.4 %collective-permute-done.14.refs_5_ = bf16[256,1024]{1,0:T(8,128)(2,1)S(1)} collective-permute-done((bf16[256,1024]{1,0:T(8,128)(2,1)S(1)}, bf16[256,1024]{1,0:T(8,128)(2,1)S(1)}, u32[]{:S(2)}, u32[]{:S(2)}) %collective-permute-start.14) | collective-permute-done | bytes 524320 | tf_op jit(solution)/shard_map/ppermute | solution.py:40
  238.8 7.8 %collective-permute-done.16.refs_7_ = bf16[256,1024]{1,0:T(8,128)(2,1)S(1)} collective-permute-done((bf16[256,1024]{1,0:T(8,128)(2,1)S(1)}, bf16[256,1024]{1,0:T(8,128)(2,1)S(1)}, u32[]{:S(2)}, u32[]{:S(2)}) %collective-permute-start.16) | collective-permute-done | bytes 524320 | tf_op jit(solution)/shard_map/ppermute | solution.py:40
  248.1 2.4 convolution_convert_fusion.1.mine_ref
  250.6 2.6 collective-permute-done.17.other_ref
  253.3 2.0 combine.1
  255.3 4.0 %all-to-all-start.3 = ((bf16[8,256,256]{2,1,0:T(8,128)(2,1)}), bf16[8,256,256]{2,1,0:T(8,128)(2,1)S(1)}, u32[]{:S(2)}, u32[]{:S(2)}) async-start(bf16[8,256,256]{2,1,0:T(8,128)(2,1)} %get-tuple-element.78), calls=%async_computation.3 | async-start | bytes 2097152 | tf_op jit(solution)/shard_map/all_to_all | solution.py:444
  259.3 7.0 %mixer.1 = (bf16[256,1024]{1,0:T(8,128)(2,1)}, bf16[256,1024]{1,0:T(8,128)(2,1)}, bf16[256,1024]{1,0:T(8,128)(2,1)}, f32[16,2,1024]{2,1,0:T(2,128)}, f32[2,8,1024]{2,1,0:T(8,128)}) custom-call(bf16[256,2048]{1,0:T(8,128)(2,1)} %get-tuple-element.52.grad_ref, bf16[2048,1024]{1,0:T(8,128)(2,1)} %weight_ref.1, f32[256,1024]{1,0:T(8,128)} %get-tuple-element.90.gelu_ref, ...), custom_call_target="tpu_custom_call" | custom-call | flops 1073741824 | bytes 8388608 | tf_op jit(solution)/shard_map/mixer/pallas_call | solution.py:102
  266.4 7.8 %all-to-all-done.3.grads_ref = bf16[8,256,256]{2,1,0:T(8,128)(2,1)S(1)} async-done(((bf16[8,256,256]{2,1,0:T(8,128)(2,1)}), bf16[8,256,256]{2,1,0:T(8,128)(2,1)S(1)}, u32[]{:S(2)}, u32[]{:S(2)}) %all-to-all-start.3) | async-done | bytes 1048608 | tf_op jit(solution)/shard_map/all_to_all | solution.py:444
  274.2 5.2 %all-to-all-start.4 = ((f32[16,2,1024]{2,1,0:T(2,128)}), f32[16,2,1024]{2,1,0:T(2,128)S(1)}, u32[]{:S(2)}, u32[]{:S(2)}) async-start(f32[16,2,1024]{2,1,0:T(2,128)} %get-tuple-element.94), calls=%async_computation.4 | async-start | bytes 262144 | tf_op jit(solution)/shard_map/all_to_all | solution.py:451
  280.4 1.0 copy-done.6
  282.5 1.0 copy-done.10
  283.5 1.0 copy-done.12
  284.6 1.8 product.1
  286.4 2.9 collective-permute-start.18
  289.3 1.3 collective-permute-start.19
  290.5 4.9 %collective-permute-done.19.head_ref = f32[2,8,1024]{2,1,0:T(8,128)S(1)} collective-permute-done((f32[2,8,1024]{2,1,0:T(8,128)S(1)}, f32[2,8,1024]{2,1,0:T(8,128)S(1)}, u32[]{:S(2)}, u32[]{:S(2)}) %collective-permute-start.19) | collective-permute-done | bytes 65568 | tf_op jit(solution)/shard_map/ppermute | solution.py:35
  296.1 4.5 %tail.1 = bf16[256,1024]{1,0:T(8,128)(2,1)} custom-call(s32[1]{0:T(128)} %bitcast.35.where_ref, f32[16,2,1024]{2,1,0:T(2,128)} %copy-done.25, bf16[256,1024]{1,0:T(8,128)(2,1)} %get-tuple-element.95.local_ref, bf16[256,1024]{1,0:T(8,128)(2,1)} %get-tuple-element.96.cumul_ref, bf16[256,1024]{1,0:T(8,128)(2,1)} %get-tuple-element.97.to_decay_ref, ...), custom_call_target="tpu_custom_call" | custom-call | flops 268435456 | bytes 7340032 | tf_op jit(solution)/shard_map/tail/pallas_call | solution.py:183
  (134 shorter events, 22.6 us)
Async XLA Ops:
  0.6 3.8 %copy-start = (bf16[256,2048]{1,0:T(8,128)(2,1)S(1)}, bf16[256,2048]{1,0:T(8,128)(2,1)}, u32[]{:S(2)}) copy-start(bf16[256,2048]{1,0:T(8,128)(2,1)} %param.16) | copy-start | bytes 3145732
  6.5 8.7 %copy-start.15 = (f32[256,1024]{1,0:T(8,128)S(1)}, f32[256,1024]{1,0:T(8,128)}, u32[]{:S(2)}) copy-start(f32[256,1024]{1,0:T(8,128)} %param.26) | copy-start | bytes 3145732
  6.5 8.7 %copy-start.24 = (bf16[256,1024]{1,0:T(8,128)(2,1)S(1)}, bf16[256,1024]{1,0:T(8,128)(2,1)}, u32[]{:S(2)}) copy-start(bf16[256,1024]{1,0:T(8,128)(2,1)} %param.24) | copy-start | bytes 1572868
  6.5 13.2 %copy-start.33 = (f32[256,2]{0,1:T(2,128)S(1)}, f32[256,2]{0,1:T(2,128)}, u32[]{:S(2)}) copy-start(f32[256,2]{0,1:T(2,128)} %param.19) | copy-start | bytes 6148
  6.5 13.5 %copy-start.32 = (f32[1024]{0:T(1024)S(1)}, f32[1024]{0:T(1024)}, u32[]{:S(2)}) copy-start(f32[1024]{0:T(1024)} %param.30) | copy-start | bytes 12292
  6.5 13.5 %copy-start.27 = (bf16[4,1024]{1,0:T(4,128)(2,1)S(1)}, bf16[4,1024]{1,0:T(4,128)(2,1)}, u32[]{:S(2)}) copy-start(bf16[4,1024]{1,0:T(4,128)(2,1)} %taps_ref.1) | copy-start | bytes 24580
  6.5 14.1 %copy-start.2 = (bf16[256,2048]{1,0:T(8,128)(2,1)S(1)}, bf16[256,2048]{1,0:T(8,128)(2,1)}, u32[]{:S(2)}) copy-start(bf16[256,2048]{1,0:T(8,128)(2,1)} %cot_ref.1) | copy-start | bytes 3145732
  6.5 51.8 %all-to-all-start = ((bf16[16,32,2048]{2,1,0:T(8,128)(2,1)}), bf16[16,32,2048]{2,1,0:T(8,128)(2,1)}, u32[]{:S(2)}, u32[]{:S(2)}) async-start(bf16[16,32,2048]{2,1,0:T(8,128)(2,1)} %bitcast.135), calls=%async_computation | async-start | bytes 4194304 | tf_op jit(solution)/shard_map/all_to_all | solution.py:333
  15.3 12.2 %collective-permute-start = (f32[4,1024]{1,0:T(4,128)S(1)}, f32[4,1024]{1,0:T(4,128)S(1)}, u32[]{:S(2)}, u32[]{:S(2)}) collective-permute-start(f32[4,1024]{1,0:T(4,128)S(1)} %pad_maximum_fusion.2), channel_id=1, source_target_pairs={{0,2},{2,4},{4,6},{6,8},{8,10},{10,12},{12,14},{14,16},{16,18},{18... | collective-permute-start | bytes 49160 | tf_op jit(solution)/shard_map/ppermute | solution.py:35
  19.1 87.7 %collective-permute-start.3 = (bf16[2048,512]{1,0:T(8,128)(2,1)}, bf16[2048,512]{1,0:T(8,128)(2,1)}, u32[]{:S(2)}, u32[]{:S(2)}) collective-permute-start(bf16[2048,512]{1,0:T(8,128)(2,1)} %bitcast.140), channel_id=1, source_target_pairs={{0,1},{1,0},{2,3},{3,2},{4,5},{5,4},{6,7},{7,6},{8,9},{9,8},{10,11... | collective-permute-start | bytes 6291464 | tf_op jit(solution)/shard_map/ppermute | solution.py:40
  19.2 91.2 %collective-permute-start.2 = (bf16[2048,512]{1,0:T(8,128)(2,1)}, bf16[2048,512]{1,0:T(8,128)(2,1)}, u32[]{:S(2)}, u32[]{:S(2)}) collective-permute-start(bf16[2048,512]{1,0:T(8,128)(2,1)} %bitcast.141), channel_id=1, source_target_pairs={{0,1},{1,0},{2,3},{3,2},{4,5},{5,4},{6,7},{7,6},{8,9},{9,8},{10,11... | collective-permute-start | bytes 6291464 | tf_op jit(solution)/shard_map/ppermute | solution.py:40
  19.7 119.0 %collective-permute-start.4 = (bf16[512,2048]{1,0:T(8,128)(2,1)}, bf16[512,2048]{1,0:T(8,128)(2,1)}, u32[]{:S(2)}, u32[]{:S(2)}) collective-permute-start(bf16[512,2048]{1,0:T(8,128)(2,1)} %bitcast.147), channel_id=1, source_target_pairs={{0,1},{1,0},{2,3},{3,2},{4,5},{5,4},{6,7},{7,6},{8,9},{9,8},{10,11... | collective-permute-start | bytes 6291464 | tf_op jit(solution)/shard_map/ppermute | solution.py:40
  22.7 35.7 %copy-start.30 = (f32[1,1024]{1,0:T(1,128)S(1)}, f32[1,1024]{1,0:T(1,128)}, u32[]{:S(2)}) copy-start(f32[1,1024]{1,0:T(1,128)} %get-tuple-element.128) | copy-start | bytes 12292
  22.7 35.7 %copy-start.31 = (f32[1,1024]{1,0:T(1,128)S(1)}, f32[1,1024]{1,0:T(1,128)}, u32[]{:S(2)}) copy-start(f32[1,1024]{1,0:T(1,128)} %get-tuple-element.129) | copy-start | bytes 12292
  27.5 30.8 %copy-start.29 = (f32[4,1024]{1,0:T(4,128)}, f32[4,1024]{1,0:T(4,128)S(1)}, u32[]{:S(2)}) copy-start(f32[4,1024]{1,0:T(4,128)S(1)} %collective-permute-done) | copy-start | bytes 49156
  58.3 16.7 %copy-start.23 = (bf16[8,128,128]{2,1,0:T(8,128)(2,1)S(1)}, bf16[8,128,128]{2,1,0:T(8,128)(2,1)}, u32[]{:S(2)}) copy-start(bf16[8,128,128]{2,1,0:T(8,128)(2,1)} %input_w_ref.1) | copy-start | bytes 786436
  78.2 14.4 %copy-start.34 = (pred[256]{0:T(512)(128)(4,1)S(1)}, pred[256]{0:T(512)(128)(4,1)}, u32[]{:S(2)}) copy-start(pred[256]{0:T(512)(128)(4,1)} %add_compare_fusion) | copy-start | bytes 772
  78.2 21.4 %collective-permute-start.1 = (bf16[512,2048]{1,0:T(8,128)(2,1)}, bf16[512,2048]{1,0:T(8,128)(2,1)}, u32[]{:S(2)}, u32[]{:S(2)}) collective-permute-start(bf16[512,2048]{1,0:T(8,128)(2,1)} %bitcast.3), channel_id=1, source_target_pairs={{0,1},{1,0},{2,3},{3,2},{4,5},{5,4},{6,7},{7,6},{8,9},{9,8},{10,11... | collective-permute-start | bytes 6291464 | tf_op jit(solution)/shard_map/ppermute | solution.py:40
  78.2 53.5 %all-to-all-start.1 = ((bf16[16,32,2048]{2,1,0:T(8,128)(2,1)}), bf16[16,32,2048]{2,1,0:T(8,128)(2,1)}, u32[]{:S(2)}, u32[]{:S(2)}) async-start(bf16[16,32,2048]{2,1,0:T(8,128)(2,1)} %bitcast.134), calls=%async_computation.1 | async-start | bytes 4194304 | tf_op jit(solution)/shard_map/all_to_all | solution.py:352
  97.8 1.9 copy-start.18
  99.6 3.0 %copy-start.20 = (bf16[1,2048,512]{2,1,0:T(8,128)(2,1)S(1)}, bf16[1,2048,512]{2,1,0:T(8,128)(2,1)}, u32[]{:S(2)}) copy-start(bf16[1,2048,512]{2,1,0:T(8,128)(2,1)} %param.20) | copy-start | bytes 6291460
  106.7 28.7 %copy-start.16 = (bf16[512,512]{1,0:T(8,128)(2,1)}, bf16[512,512]{1,0:T(8,128)(2,1)S(1)}, u32[]{:S(2)}) copy-start(bf16[512,512]{1,0:T(8,128)(2,1)S(1)} %get-tuple-element.67) | copy-start | bytes 1572868
  131.7 3.7 %copy-start.19 = (bf16[1,2048,512]{2,1,0:T(8,128)(2,1)S(1)}, bf16[1,2048,512]{2,1,0:T(8,128)(2,1)}, u32[]{:S(2)}) copy-start(bf16[1,2048,512]{2,1,0:T(8,128)(2,1)} %param.21) | copy-start | bytes 6291460
  135.4 1.3 copy-start.13
  135.4 2.0 copy-start.21
  137.4 1.3 copy-start.37
  143.1 3.1 %copy-start.22 = (bf16[512,512]{1,0:T(8,128)(2,1)}, bf16[512,512]{1,0:T(8,128)(2,1)S(1)}, u32[]{:S(2)}) copy-start(bf16[512,512]{1,0:T(8,128)(2,1)S(1)} %get-tuple-element.122) | copy-start | bytes 1572868
  150.9 97.2 %all-to-all-start.2 = ((bf16[16,32,2048]{2,1,0:T(8,128)(2,1)}), bf16[16,32,2048]{2,1,0:T(8,128)(2,1)}, u32[]{:S(2)}, u32[]{:S(2)}) async-start(bf16[16,32,2048]{2,1,0:T(8,128)(2,1)} %bitcast.133), calls=%async_computation.2 | async-start | bytes 4194304 | tf_op jit(solution)/shard_map/all_to_all | solution.py:422
  162.0 7.0 %collective-permute-start.6 = (bf16[512,512]{1,0:T(8,128)(2,1)}, bf16[512,512]{1,0:T(8,128)(2,1)S(1)}, u32[]{:S(2)}, u32[]{:S(2)}) collective-permute-start(bf16[512,512]{1,0:T(8,128)(2,1)} %get-tuple-element.123), channel_id=1, source_target_pairs={{0,1},{1,0},{2,3},{3,2},{4,5},{5,4},{6,7},{7,6},{8,9},{9,8},{10,11... | collective-permute-start | bytes 1572872 | tf_op jit(solution)/shard_map/ppermute | solution.py:40
  162.0 46.6 %collective-permute-start.13 = (bf16[256,1024]{1,0:T(8,128)(2,1)S(1)}, bf16[256,1024]{1,0:T(8,128)(2,1)S(1)}, u32[]{:S(2)}, u32[]{:S(2)}) collective-permute-start(bf16[256,1024]{1,0:T(8,128)(2,1)S(1)} %get-tuple-element.79.refs_0_), channel_id=1, source_target_pairs={{0,8},{2,10},{4,12},{6,14},{8,0},{10,2},{12,4},{14,6},{16,24},{18,... | collective-permute-start | bytes 1572872 | tf_op jit(solution)/shard_map/ppermute | solution.py:40
  163.9 47.6 %collective-permute-start.10 = (bf16[256,1024]{1,0:T(8,128)(2,1)S(1)}, bf16[256,1024]{1,0:T(8,128)(2,1)S(1)}, u32[]{:S(2)}, u32[]{:S(2)}) collective-permute-start(bf16[256,1024]{1,0:T(8,128)(2,1)S(1)} %get-tuple-element.79.refs_0_), channel_id=1, source_target_pairs={{0,2},{2,0},{4,6},{6,4},{8,10},{10,8},{12,14},{14,12},{16,18},{18,... | collective-permute-start | bytes 1572872 | tf_op jit(solution)/shard_map/ppermute | solution.py:40
  165.4 54.0 %collective-permute-start.8 = (bf16[512,2048]{1,0:T(8,128)(2,1)}, bf16[512,2048]{1,0:T(8,128)(2,1)S(1)}, u32[]{:S(2)}, u32[]{:S(2)}) collective-permute-start(bf16[512,2048]{1,0:T(8,128)(2,1)} %bitcast.29), channel_id=1, source_target_pairs={{0,1},{1,0},{2,3},{3,2},{4,5},{5,4},{6,7},{7,6},{8,9},{9,8},{10,11... | collective-permute-start | bytes 6291464 | tf_op jit(solution)/shard_map/ppermute | solution.py:40
  165.4 8.0 %collective-permute-start.5 = (bf16[512,512]{1,0:T(8,128)(2,1)}, bf16[512,512]{1,0:T(8,128)(2,1)S(1)}, u32[]{:S(2)}, u32[]{:S(2)}) collective-permute-start(bf16[512,512]{1,0:T(8,128)(2,1)} %copy-done.22), channel_id=1, source_target_pairs={{0,1},{1,0},{2,3},{3,2},{4,5},{5,4},{6,7},{7,6},{8,9},{9,8},{10,11... | collective-permute-start | bytes 1572872 | tf_op jit(solution)/shard_map/ppermute | solution.py:40
  168.9 4.5 %copy-start.35 = (bf16[512,512]{1,0:T(8,128)(2,1)S(1)}, bf16[512,512]{1,0:T(8,128)(2,1)}, u32[]{:S(2)}) copy-start(bf16[512,512]{1,0:T(8,128)(2,1)} %get-tuple-element.72) | copy-start | bytes 1572868
  169.0 43.6 %collective-permute-start.11 = (bf16[256,1024]{1,0:T(8,128)(2,1)S(1)}, bf16[256,1024]{1,0:T(8,128)(2,1)S(1)}, u32[]{:S(2)}, u32[]{:S(2)}) collective-permute-start(bf16[256,1024]{1,0:T(8,128)(2,1)S(1)} %get-tuple-element.79.refs_0_), channel_id=1, source_target_pairs={{0,4},{2,6},{4,0},{6,2},{8,12},{10,14},{12,8},{14,10},{16,20},{18,... | collective-permute-start | bytes 1572872 | tf_op jit(solution)/shard_map/ppermute | solution.py:40
  173.4 3.1 %copy-start.14 = (f32[512,512]{1,0:T(8,128)S(1)}, f32[512,512]{1,0:T(8,128)}, u32[]{:S(2)}) copy-start(f32[512,512]{1,0:T(8,128)} %copy-done.13) | copy-start | bytes 3145732
  173.4 3.1 %copy-start.17 = (bf16[512,512]{1,0:T(8,128)(2,1)S(1)}, bf16[512,512]{1,0:T(8,128)(2,1)}, u32[]{:S(2)}) copy-start(bf16[512,512]{1,0:T(8,128)(2,1)} %copy-done.16) | copy-start | bytes 1572868
  173.4 39.2 %collective-permute-start.7 = (bf16[512,512]{1,0:T(8,128)(2,1)S(1)}, bf16[512,512]{1,0:T(8,128)(2,1)S(1)}, u32[]{:S(2)}, u32[]{:S(2)}) collective-permute-start(bf16[512,512]{1,0:T(8,128)(2,1)S(1)} %copy-done.35), channel_id=1, source_target_pairs={{0,1},{1,0},{2,3},{3,2},{4,5},{5,4},{6,7},{7,6},{8,9},{9,8},{10,11... | collective-permute-start | bytes 1572872 | tf_op jit(solution)/shard_map/ppermute | solution.py:40
  208.6 17.4 %collective-permute-start.12 = (bf16[256,1024]{1,0:T(8,128)(2,1)S(1)}, bf16[256,1024]{1,0:T(8,128)(2,1)S(1)}, u32[]{:S(2)}, u32[]{:S(2)}) collective-permute-start(bf16[256,1024]{1,0:T(8,128)(2,1)S(1)} %get-tuple-element.79.refs_0_), channel_id=1, source_target_pairs={{0,6},{2,4},{4,2},{6,0},{8,14},{10,12},{12,10},{14,8},{16,22},{18,... | collective-permute-start | bytes 1572872 | tf_op jit(solution)/shard_map/ppermute | solution.py:40
  211.6 25.7 %collective-permute-start.14 = (bf16[256,1024]{1,0:T(8,128)(2,1)S(1)}, bf16[256,1024]{1,0:T(8,128)(2,1)S(1)}, u32[]{:S(2)}, u32[]{:S(2)}) collective-permute-start(bf16[256,1024]{1,0:T(8,128)(2,1)S(1)} %collective-permute-done.13.refs_4_), channel_id=1, source_target_pairs={{0,2},{2,0},{4,6},{6,4},{8,10},{10,8},{12,14},{14,12},{16,18},{18,... | collective-permute-start | bytes 1572872 | tf_op jit(solution)/shard_map/ppermute | solution.py:40
  212.6 6.8 %copy-start.3 = (bf16[256,1024]{1,0:T(8,128)(2,1)}, bf16[256,1024]{1,0:T(8,128)(2,1)S(1)}, u32[]{:S(2)}) copy-start(bf16[256,1024]{1,0:T(8,128)(2,1)S(1)} %collective-permute-done.11.refs_2_) | copy-start | bytes 1572868
  212.6 25.4 %collective-permute-start.15 = (bf16[256,1024]{1,0:T(8,128)(2,1)S(1)}, bf16[256,1024]{1,0:T(8,128)(2,1)S(1)}, u32[]{:S(2)}, u32[]{:S(2)}) collective-permute-start(bf16[256,1024]{1,0:T(8,128)(2,1)S(1)} %collective-permute-done.13.refs_4_), channel_id=1, source_target_pairs={{0,4},{2,6},{4,0},{6,2},{8,12},{10,14},{12,8},{14,10},{16,20},{18,... | collective-permute-start | bytes 1572872 | tf_op jit(solution)/shard_map/ppermute | solution.py:40
  212.6 34.0 %collective-permute-start.16 = (bf16[256,1024]{1,0:T(8,128)(2,1)S(1)}, bf16[256,1024]{1,0:T(8,128)(2,1)S(1)}, u32[]{:S(2)}, u32[]{:S(2)}) collective-permute-start(bf16[256,1024]{1,0:T(8,128)(2,1)S(1)} %collective-permute-done.13.refs_4_), channel_id=1, source_target_pairs={{0,6},{2,4},{4,2},{6,0},{8,14},{10,12},{12,10},{14,8},{16,22},{18,... | collective-permute-start | bytes 1572872 | tf_op jit(solution)/shard_map/ppermute | solution.py:40
  219.4 28.8 %collective-permute-start.9 = (f32[3,8,1024]{2,1,0:T(8,128)S(1)}, f32[3,8,1024]{2,1,0:T(8,128)S(1)}, u32[]{:S(2)}, u32[]{:S(2)}) collective-permute-start(f32[3,8,1024]{2,1,0:T(8,128)S(1)} %pad_maximum_fusion.1), channel_id=1, source_target_pairs={{2,0},{4,2},{6,4},{8,6},{10,8},{12,10},{14,12},{16,14},{18,16},{20... | collective-permute-start | bytes 294920 | tf_op jit(solution)/shard_map/ppermute | solution.py:35
  226.0 0.8 copy-start.5
  237.2 0.8 copy-start.7
  238.0 0.8 copy-start.9
  246.6 0.9 copy-start.11
  248.1 7.2 %copy-start.26 = (f32[3,8,1024]{2,1,0:T(8,128)}, f32[3,8,1024]{2,1,0:T(8,128)S(1)}, u32[]{:S(2)}) copy-start(f32[3,8,1024]{2,1,0:T(8,128)S(1)} %collective-permute-done.9.head_coef_ref) | copy-start | bytes 294916
  250.5 2.7 collective-permute-start.17
  255.3 18.9 %all-to-all-start.3 = ((bf16[8,256,256]{2,1,0:T(8,128)(2,1)}), bf16[8,256,256]{2,1,0:T(8,128)(2,1)S(1)}, u32[]{:S(2)}, u32[]{:S(2)}) async-start(bf16[8,256,256]{2,1,0:T(8,128)(2,1)} %get-tuple-element.78), calls=%async_computation.3 | async-start | bytes 2097152 | tf_op jit(solution)/shard_map/all_to_all | solution.py:444
  274.2 21.2 %all-to-all-start.4 = ((f32[16,2,1024]{2,1,0:T(2,128)}), f32[16,2,1024]{2,1,0:T(2,128)S(1)}, u32[]{:S(2)}, u32[]{:S(2)}) async-start(f32[16,2,1024]{2,1,0:T(2,128)} %get-tuple-element.94), calls=%async_computation.4 | async-start | bytes 262144 | tf_op jit(solution)/shard_map/all_to_all | solution.py:451
  279.4 1.0 copy-start.4
  280.4 1.0 copy-start.6
  281.5 1.0 copy-start.8
  282.5 1.0 copy-start.10
  283.5 1.0 copy-start.12
  284.6 4.7 %copy-start.36 = (f32[2,8,1024]{2,1,0:T(8,128)S(1)}, f32[2,8,1024]{2,1,0:T(8,128)}, u32[]{:S(2)}) copy-start(f32[2,8,1024]{2,1,0:T(8,128)} %get-tuple-element.100) | copy-start | bytes 196612
  286.4 15.3 %collective-permute-start.18 = (bf16[128,1024]{1,0:T(8,128)(2,1)S(1)}, bf16[128,1024]{1,0:T(8,128)(2,1)S(1)}, u32[]{:S(2)}, u32[]{:S(2)}) collective-permute-start(bf16[128,1024]{1,0:T(8,128)(2,1)S(1)} %get-tuple-element.88), channel_id=1, source_target_pairs={{0,16},{2,18},{4,20},{6,22},{8,24},{10,26},{12,28},{14,30},{16,0},... | collective-permute-start | bytes 786440 | tf_op jit(solution)/shard_map/ppermute | solution.py:40
  289.3 6.1 %collective-permute-start.19 = (f32[2,8,1024]{2,1,0:T(8,128)S(1)}, f32[2,8,1024]{2,1,0:T(8,128)S(1)}, u32[]{:S(2)}, u32[]{:S(2)}) collective-permute-start(f32[2,8,1024]{2,1,0:T(8,128)S(1)} %copy-done.36), channel_id=1, source_target_pairs={{2,0},{4,2},{6,4},{8,6},{10,8},{12,10},{14,12},{16,14},{18,16},{20... | collective-permute-start | bytes 196616 | tf_op jit(solution)/shard_map/ppermute | solution.py:35
  295.4 0.6 copy-start.28
  295.4 0.7 copy-start.25
  295.4 7.1 %copy-start.1 = (bf16[256,2048]{1,0:T(8,128)(2,1)S(1)}, bf16[256,2048]{1,0:T(8,128)(2,1)}, u32[]{:S(2)}) copy-start(bf16[256,2048]{1,0:T(8,128)(2,1)} %param.16) | copy-start | bytes 3145732

commit v5 on v4

--- a/solution.py
+++ b/solution.py
@@ -89,12 +89,10 @@
     head_ref[0] = values[0]
     head_ref[1] = decays[0]
     first = first_ref[...]
-    both = jnp.concatenate([first * decays[0][:1], first * values[0][:1]], axis=0)
-    for peer in range(ends_ref.shape[0]):
-        ends_ref[peer] = both
-
-
-def mixer_call(input_grad, out_weight, gelu, slope, next_decay, first, peers):
+    ends_ref[...] = jnp.concatenate([first * decays[0][:1], first * values[0][:1]], axis=0)
+
+
+def mixer_call(input_grad, out_weight, gelu, slope, next_decay, first):
     rows, width = input_grad.shape
     channels = out_weight.shape[1]
     block = 256
@@ -110,14 +108,14 @@
         ],
         out_specs=[
             wide, wide, wide,
-            pl.BlockSpec((peers, 2, block), lambda i: (0, 0, i)),
+            pl.BlockSpec((2, block), lambda i: (0, i)),
             pl.BlockSpec((2, 8, block), lambda i: (0, 0, i)),
         ],
         out_shape=[
             jax.ShapeDtypeStruct((rows, channels), bf16),
             jax.ShapeDtypeStruct((rows, channels), bf16),
             jax.ShapeDtypeStruct((rows, channels), bf16),
-            jax.ShapeDtypeStruct((peers, 2, channels), f32),
+            jax.ShapeDtypeStruct((2, channels), f32),
             jax.ShapeDtypeStruct((2, 8, channels), f32),
         ],
         cost_estimate=pl.CostEstimate(
@@ -127,21 +125,64 @@
     )(input_grad, out_weight, gelu, slope, next_decay, first)
 
 
-def tail_kernel(where_ref, ends_ref, local_ref, cumul_ref, to_decay_ref, to_input_ref, direct_ref,
-                head_ref, head_coef_ref, taps_ref, decay_w_ref, input_w_ref, out_ref):
-    mine = where_ref[0]
-    count = ends_ref.shape[0]
+def joined(near, far_a, far_b):
+    return near[0:1] * far_a, near[1:2] + near[0:1] * far_b
+
+
+def chosen(refs, wanted):
+    value = refs[0][...]
+    for k in range(1, len(refs)):
+        value = jnp.where(wanted == k, refs[k][...], value)
+    return value
+
+
+def near_kernel(where_ref, *refs):
+    later_ref, total_ref = refs[-2:]
+    ends = refs[:-2]
+    count = len(ends)
+    mine = lax.rem(where_ref[0], count)
+    whole = (jnp.ones_like(ends[0][:1]), jnp.zeros_like(ends[0][:1]))
+    later = whole
+    for spot in reversed(range(count)):
+        whole = joined(chosen(ends, mine ^ spot), *whole)
+        later = tuple(jnp.where(spot > mine, new, old) for new, old in zip(whole, later))
+    later_ref[...] = jnp.concatenate(later, axis=0)
+    total_ref[...] = jnp.concatenate(whole, axis=0)
+
+
+def near_call(where, ends):
+    shape = jax.ShapeDtypeStruct(ends[0].shape, f32)
+    return pl.pallas_call(
+        near_kernel,
+        in_specs=[pl.BlockSpec(memory_space=pltpu.SMEM)] + held(len(ends)),
+        out_specs=held(2),
+        out_shape=[shape, shape],
+        compiler_params=params(4),
+        cost_estimate=pl.CostEstimate(flops=1 << 20, bytes_accessed=1 << 16, transcendentals=0),
+        name="near",
+    )(where, *ends)
+
+
+def tail_kernel(count, where_ref, later_ref, next_ref, *refs):
+    far = refs[:count]
+    (local_ref, cumul_ref, to_decay_ref, to_input_ref, direct_ref,
+     head_ref, head_coef_ref, taps_ref, decay_w_ref, input_w_ref, out_ref) = refs[count:]
+    near = where_ref[1]
+    mine = where_ref[0] // near
+    after = (where_ref[0] + 1) // near
     block = decay_w_ref.shape[1]
     rows = local_ref.shape[0]
     taps = taps_ref[...].astype(f32)
 
-    carry = jnp.zeros_like(local_ref[:1])
+    carry = jnp.zeros_like(later_ref[:1])
     head_carry = carry
-    for place in reversed(range(1, count)):
-        ends = ends_ref[place]
-        longer = ends[1:2] + ends[0:1] * carry
-        head_carry = jnp.where(place > mine + 1, longer, head_carry)
-        carry = jnp.where(place > mine, longer, carry)
+    for spot in reversed(range(1, count)):
+        total = chosen(far, mine ^ spot)
+        longer = total[1:2] + total[0:1] * carry
+        head_carry = jnp.where(spot > after, longer, head_carry)
+        carry = jnp.where(spot > mine, longer, carry)
+    carry = later_ref[1:2] + later_ref[0:1] * carry
+    head_carry = next_ref[1:2] + next_ref[0:1] * head_carry
 
     for index in range(decay_w_ref.shape[0]):
         cols = slice(index * block, (index + 1) * block)
@@ -173,20 +214,20 @@
         out_ref[:, cols] = total[:rows].astype(bf16)
 
 
-def tail_call(where, *arrays):
-    ends, local, decay_w = arrays[0], arrays[1], arrays[-1]
+def tail_call(where, later, later_next, far, *arrays):
+    local, decay_w = arrays[0], arrays[-1]
     rows, channels = local.shape
     width = decay_w.shape[1]
     block = 2 * width
     wide = pl.BlockSpec((rows, block), lambda i, s: (0, i))
     gate = pl.BlockSpec((2, width, width), lambda i, s: (i, 0, 0))
+    pair = pl.BlockSpec((2, block), lambda i, s: (0, i))
     return pl.pallas_call(
-        tail_kernel,
+        functools.partial(tail_kernel, len(far)),
         grid_spec=pltpu.PrefetchScalarGridSpec(
             num_scalar_prefetch=1,
             grid=(channels // block,),
-            in_specs=[
-                pl.BlockSpec((ends.shape[0], 2, block), lambda i, s: (0, 0, i)),
+            in_specs=[pair] * (2 + len(far)) + [
                 wide, wide, wide, wide, wide,
                 pl.BlockSpec((2, 8, block), lambda i, s: (0, 0, i)),
                 pl.BlockSpec((3, 8, block), lambda i, s: (0, 0, i)),
@@ -200,7 +241,7 @@
             flops=8 * rows * width * channels, bytes_accessed=7 << 20, transcendentals=0
         ),
         name="tail",
-    )(where, *arrays)
+    )(where, later, later_next, *far, *arrays)
 
 
 def combine_kernel(lanes, mine_ref, other_ref, cot_ref, grad_ref, piece_ref):
@@ -229,6 +270,90 @@
         cost_estimate=pl.CostEstimate(flops=1 << 28, bytes_accessed=5 << 20, transcendentals=0),
         name="combine",
     )(mine, other, cotangent)
+
+
+def expert_kernel(span, grads_ref, *refs):
+    silus, slopes, downs, gates, ups = (refs[2 * n : 2 * n + 2] for n in range(5))
+    out_ref, gate_outs, up_outs = refs[10], refs[11:13], refs[13:15]
+    grads_v, pre_v, down_v, wide_v, out_v, sems = refs[15:]
+    hidden, width = downs[0].shape
+    used = []
+
+    def fetch(source, target):
+        copy = pltpu.make_async_copy(source, target, sems.at[len(used)])
+        copy.start()
+        used.append(copy)
+        return copy
+
+    chunks = [(side, start) for side in range(2) for start in range(0, hidden, span)]
+    grads_copy = fetch(grads_ref, grads_v)
+    chunk_copies = {}
+    for side, start in chunks:
+        rows = pl.ds(start, span)
+        chunk_copies[side, start] = [fetch(downs[side].at[rows], down_v.at[side, rows])]
+        if start == 0:
+            chunk_copies[side, start] += [
+                fetch(silus[side], pre_v.at[side]), fetch(slopes[side], pre_v.at[2 + side])
+            ]
+    blocks = range(0, width, span)
+    wide_copies = {
+        start: [
+            fetch(source.at[pl.ds(start, span)], wide_v.at[n, pl.ds(start, span)])
+            for n, source in enumerate((*gates, *ups))
+        ]
+        for start in blocks
+    }
+    grads_copy.wait()
+    for side, start in chunks:
+        for copy in chunk_copies[side, start]:
+            copy.wait()
+        cols = slice(start, start + span)
+        hidden_grad = cols_of(grads_v[...], down_v[side, cols, :])
+        gate_outs[side][:, cols] = (hidden_grad * pre_v[2 + side, :, cols].astype(f32)).astype(bf16)
+        up_outs[side][:, cols] = (hidden_grad * pre_v[side, :, cols].astype(f32)).astype(bf16)
+    results = []
+    for start in blocks:
+        for copy in wide_copies[start]:
+            copy.wait()
+        cols = slice(start, start + span)
+        total = None
+        for n, part_ref in enumerate((*gate_outs, *up_outs)):
+            part = cols_of(part_ref[...], wide_v[n, cols, :])
+            total = part if total is None else total + part
+        out_v[:, cols] = total.astype(bf16)
+        results.append(fetch(out_v.at[:, pl.ds(start, span)], out_ref.at[:, pl.ds(start, span)]))
+    for copy in results:
+        copy.wait()
+
+
+def expert_call(grads, pres, weights):
+    slots, width = grads.shape
+    hidden = weights[0][2].shape[0]
+    span = min(256, hidden)
+    arrays = [pre[1] for pre in pres] + [pre[2] for pre in pres]
+    for n in (2, 0, 1):
+        arrays += [weight[n] for weight in weights]
+    part = jax.ShapeDtypeStruct((slots, hidden), bf16)
+    count = 1 + 2 * (hidden // span) + 4 + 5 * (width // span)
+    return pl.pallas_call(
+        functools.partial(expert_kernel, span),
+        in_specs=[pl.BlockSpec(memory_space=pl.ANY)] * (1 + len(arrays)),
+        out_specs=[pl.BlockSpec(memory_space=pl.ANY)] + held(4),
+        out_shape=[jax.ShapeDtypeStruct((slots, width), bf16)] + [part] * 4,
+        scratch_shapes=[
+            pltpu.VMEM((slots, width), bf16),
+            pltpu.VMEM((4, slots, hidden), bf16),
+            pltpu.VMEM((2, hidden, width), bf16),
+            pltpu.VMEM((4, width, hidden), bf16),
+            pltpu.VMEM((slots, width), bf16),
+            pltpu.SemaphoreType.DMA((count,)),
+        ],
+        compiler_params=params(36),
+        cost_estimate=pl.CostEstimate(
+            flops=12 * slots * width * hidden, bytes_accessed=18 << 20, transcendentals=0
+        ),
+        name="expert",
+    )(grads, *arrays)
 
 
 def product_kernel(where_ref, grads_ref, *refs):
@@ -406,19 +531,9 @@
         mixers[k ^ half] = swapped(mixers[half], "sp", k)
     grads_here = got_grads.reshape(own_slots, width)
 
-    def second_half(pre, down_w):
-        hidden_grad = cols_of(grads_here, down_w)
-        return (hidden_grad * pre[2].astype(f32)).astype(bf16), (hidden_grad * pre[1].astype(f32)).astype(bf16)
-
-    own_grads = second_half(pres[0], own_weights[2])
-    other_grads = second_half(pres[1], other_weights[2])
-    partial = (
-        cols_of(own_grads[0], own_weights[0])
-        + cols_of(own_grads[1], own_weights[1])
-        + cols_of(other_grads[0], other_weights[0])
-        + cols_of(other_grads[1], other_weights[1])
-    )
-    shared = partial.astype(bf16).reshape(experts, share, width)
+    partial, gate_h, gate_o, up_h, up_o = expert_call(grads_here, pres, (own_weights, other_weights))
+    own_grads, other_grads = (gate_h, up_h), (gate_o, up_o)
+    shared = partial.reshape(experts, share, width)
     back = lax.all_to_all(shared, "sp", split_axis=0, concat_axis=0, tiled=True)
     head_coef = shifted(head_coef, "sp", -1)
     hidden_h, gate_h, up_h = pres[0][0], own_grads[0], own_grads[1]
@@ -445,10 +560,15 @@
         pieces, "sp", split_axis=0, concat_axis=0, tiled=True, axis_index_groups=groups
     )
     gate_grad, local, cumul, ends, head = mixer_call(
-        input_grad, out_weight, gelu_value, slope, next_decay, first_decay, experts
+        input_grad, out_weight, gelu_value, slope, next_decay, first_decay
     )
     head = shifted(head, "sp", -1)
-    ends = lax.all_to_all(ends, "sp", split_axis=0, concat_axis=0, tiled=True)
+    near = 4 if experts % 4 == 0 else experts
+    ends = [ends] + [swapped(ends, "sp", k) for k in range(1, near)]
+    grads, ends, head = lax.optimization_barrier((grads, ends, head))
+    later, total = near_call(where, ends)
+    later_next = shifted(later, "sp", -1)
+    far = [total] + [swapped(total, "sp", k * near) for k in range(1, experts // near)]
     mixers = [mixers[k] for k in range(group)]
     received = []
     if outer == 2 and out_rows % 128 == 0:
@@ -469,8 +589,9 @@
     for part in received:
         out_weight_grad = out_weight_grad + part.astype(f32)
 
+    where = jnp.concatenate([where, jnp.full((1,), near, jnp.int32)])
     recur_grad = tail_call(
-        where, ends, local, cumul, to_decay, to_input, direct,
+        where, later, later_next, far, local, cumul, to_decay, to_input, direct,
         head, head_coef, conv_taps, decay_gate_w, input_gate_w,
     )
     return (

time: 308 us -> 282 us (0.916); the launches traced: 302 us -> 280 us
  matrix products: 79.6 us -> 34.9 us
  Pallas kernels: 15.4 us -> 33.8 us
  waiting for transfers between devices: 113 us -> 95.3 us
  starting transfers between devices: 61.2 us -> 76.8 us
  local copies, waits for them, and re-layouts: 14.7 us -> 24.5 us
  other arithmetic: 17.5 us -> 13.7 us
    dot_general x35 -> x29, matrix products: 79.6 us -> 34.9 us  [dot(): lax.dot_general(left, right, (contract, ((), ())), preferred_element_type...]
    ppermute x17 -> x23, starting transfers between devices: 15.5 us -> 34.8 us  [swapped(): return lax.ppermute(value, axis, [(s, s ^ mask) for s in range(count)])]
    pallas_call x1 -> x3, Pallas kernels: 4.53 us -> 22.9 us  [the longest x1 17.7 us: expert_call(): pl.pallas_call(functools.partial(expert_kernel, span), in_specs=[pl.Block...]
    ppermute x17 -> x23, waiting for transfers between devices: 52.3 us -> 41.8 us  [swapped(): return lax.ppermute(value, axis, [(s, s ^ mask) for s in range(count)])]
    unnamed x77 -> x113, local copies, waits for them, and re-layouts: 10.8 us -> 21.2 us
    all_to_all x1, waiting for transfers between devices: 7.82 us -> 0.01 us  [on_device(): lax.all_to_all(pieces, 'sp', split_axis=0, concat_axis=0, tiled=True, axi...]
    all_to_all x1 -> x0, starting transfers between devices: 5.18 us -> none  [on_device(): ends = lax.all_to_all(ends, 'sp', split_axis=0, concat_axis=0, tiled=True)]
    ppermute x3 -> x4, starting transfers between devices: 6.34 us -> 7.95 us  [shifted(): return lax.ppermute(value, axis, pairs)]
  transfers between devices with their start and end apart: 25 -> 31, of which waited for: 11 -> 12; matrix products, arithmetic and copies ran while one was open for 27% -> 16% of each run, Pallas kernels for 4% -> 4%
where the time goes in v5:
time: 282 us; the launch traced here: 280 us
  waiting for transfers between devices  95.3 us (34%)
  starting transfers between devices  76.8 us (27%)
  matrix products  34.9 us (12%)
  Pallas kernels  33.8 us (12%)
  local copies, waits for them, and re-layouts  24.5 us (9%)
  other arithmetic  13.7 us (5%)
    ppermute x23, waiting for transfers between devices, swapped(): return lax.ppermute(value, axis, [(s, s ^ mask) for s in range(count)])  41.8 us
    dot_general x29, matrix products, dot(): lax.dot_general(left, right, (contract, ((), ())), preferred_element_type...  34.9 us
    ppermute x23, starting transfers between devices, swapped(): return lax.ppermute(value, axis, [(s, s ^ mask) for s in range(count)])  34.8 us
    all_to_all x1, waiting for transfers between devices, on_device(): lax.all_to_all(send_rows, 'sp', split_axis=0, concat_axis=0, tiled=True)  31.5 us
    unnamed x113, local copies, waits for them, and re-layouts  21.2 us
    all_to_all x1, waiting for transfers between devices, on_device(): lax.all_to_all(send_grads, 'sp', split_axis=0, concat_axis=0, tiled=True)  18.3 us
    pallas_call x1, Pallas kernels, expert_call(): pl.pallas_call(functools.partial(expert_kernel, span), in_specs=[pl.Block...  17.7 us
    all_to_all x1, starting transfers between devices, on_device(): lax.all_to_all(send_grads, 'sp', split_axis=0, concat_axis=0, tiled=True)  10 us
  transfers between devices with their start and end apart: 31, of which 12 were waited for; matrix products, arithmetic and copies ran while one was open for 16% of the time, Pallas kernels for 4%

profile of v5, /device:TPU:0, one launch (start us, length us, event | category | flops | bytes accessed | tf_op | source)
XLA Modules:
  0.0 280.4 jit_solution(9026100575571696929)
XLA Ops:
  1.9 1.2 reduce-window.6
  4.5 2.0 convolution_convert_fusion
  6.5 8.5 %all-to-all-start = ((bf16[16,32,2048]{2,1,0:T(8,128)(2,1)}), bf16[16,32,2048]{2,1,0:T(8,128)(2,1)S(1)}, u32[]{:S(2)}, u32[]{:S(2)}) async-start(bf16[16,32,2048]{2,1,0:T(8,128)(2,1)} %bitcast.134), calls=%async_computation | async-start | bytes 4194304 | tf_op jit(solution)/shard_map/all_to_all | solution.py:458
  16.5 3.8 %collective-permute-start = (f32[4,1024]{1,0:T(4,128)S(1)}, f32[4,1024]{1,0:T(4,128)S(1)}, u32[]{:S(2)}, u32[]{:S(2)}) collective-permute-start(f32[4,1024]{1,0:T(4,128)S(1)} %pad_maximum_fusion.2), channel_id=1, source_target_pairs={{0,2},{2,4},{4,6},{6,8},{8,10},{10,12},{12,14},{14,16},{16,18},{18... | collective-permute-start | bytes 49160 | tf_op jit(solution)/shard_map/ppermute | solution.py:35
  21.3 2.0 multiply_convert_fusion
  23.4 2.1 multiply_convert_fusion.1
  25.5 1.1 convert_element_type.87
  26.5 31.5 %all-to-all-done = bf16[16,32,2048]{2,1,0:T(8,128)(2,1)S(1)} async-done(((bf16[16,32,2048]{2,1,0:T(8,128)(2,1)}), bf16[16,32,2048]{2,1,0:T(8,128)(2,1)S(1)}, u32[]{:S(2)}, u32[]{:S(2)}) %all-to-all-start) | async-done | bytes 2097184 | tf_op jit(solution)/shard_map/all_to_all | solution.py:458
  58.1 1.3 copy-done.33
  59.4 10.0 %all-to-all-start.1 = ((bf16[16,32,2048]{2,1,0:T(8,128)(2,1)}), bf16[16,32,2048]{2,1,0:T(8,128)(2,1)S(1)}, u32[]{:S(2)}, u32[]{:S(2)}) async-start(bf16[16,32,2048]{2,1,0:T(8,128)(2,1)} %bitcast.133), calls=%async_computation.1 | async-start | bytes 4194304 | tf_op jit(solution)/shard_map/all_to_all | solution.py:477
  69.5 3.0 %fusion.100 = (bf16[256,1024]{1,0:T(8,128)(2,1)S(1)}, f32[256,1024]{1,0:T(8,128)S(1)}) fusion(f32[256,1024]{1,0:T(8,128)} %convert_element_type.87, f32[1024]{0:T(1024)S(1)} %bitcast.143, f32[3,1024]{1,0:T(4,128)S(1)} %bitcast.139, f32[1024]{0:T(1024)S(1)} %bitcast.142, f32[1024]{0:T(1024)S(1)} %bitcast.141, f32[1024]{0:T(1024)S(1)} %bitcast.140), kind=kLoop, calls=%fused_computation.164 | loop fusion | flops 2883584 | bytes 2650112 | tf_op jit(solution)/shard_map/convert_element_type | solution.py:487
  74.9 3.0 %fusion.98 = (bf16[256,1024]{1,0:T(8,128)(2,1)}, f32[256,1024]{1,0:T(8,128)S(1)}, bf16[256,1024]{1,0:T(8,128)(2,1)}, f32[256,1024]{1,0:T(8,128)S(1)}, bf16[256,1...) fusion(f32[256,1024]{1,0:T(8,128)S(1)} %get-tuple-element.136, ...), kind=kLoop, calls=%fused_computation.163 | loop fusion | flops 8126464 | bytes 11014400 | tf_op jit(solution)/shard_map/convert_element_type | solution.py:526
  78.7 1.1 concatenate.24.next_ref
  80.6 1.3 fusion.90
  81.9 2.8 %fusion.103 = f32[512,512]{1,0:T(8,128)S(1)} fusion(bf16[512,2048]{1,0:T(8,128)(2,1)S(1)} %bitcast.128, bf16[2048,512]{1,0:T(8,128)(2,1)} %collective-permute-done.3.refs_9_), kind=kOutput, calls=%fused_computation.166 | convolution fusion | flops 1073741824 | bytes 5242880 | tf_op jit(solution)/shard_map/dot_general | solution.py:17
  84.8 4.4 %multiply_convert_fusion.4 = (bf16[512,512]{1,0:T(8,128)(2,1)}, bf16[512,512]{1,0:T(8,128)(2,1)}, bf16[512,512]{1,0:T(8,128)(2,1)}) fusion(f32[512,512]{1,0:T(8,128)S(1)} %fusion.90, bf16[512,2048]{1,0:T(8,128)(2,1)S(1)} %bitcast.129, bf16[1,2048,512]{2,1,0:T(8,128)(2,1)} %param.20), kind=kOutput, calls=%fused_computation.67 | convolution fusion | flops 1077149696 | bytes 6815744 | tf_op jit(solution)/shard_map/dot_general | solution.py:17
  89.2 4.4 %multiply_convert_fusion.2 = (bf16[512,512]{1,0:T(8,128)(2,1)}, bf16[512,512]{1,0:T(8,128)(2,1)}, bf16[512,512]{1,0:T(8,128)(2,1)}) fusion(f32[512,512]{1,0:T(8,128)S(1)} %fusion.103, bf16[512,2048]{1,0:T(8,128)(2,1)S(1)} %bitcast.130, bf16[2048,512]{1,0:T(8,128)(2,1)} %collective-permute-done.2.refs_7_), kind=kOutput, calls=%fused_computation.63 | convolution fusion | flops 1077149696 | bytes 6815744 | tf_op jit(solution)/shard_map/dot_general | solution.py:17
  93.6 18.3 %all-to-all-done.1 = bf16[16,32,2048]{2,1,0:T(8,128)(2,1)S(1)} async-done(((bf16[16,32,2048]{2,1,0:T(8,128)(2,1)}), bf16[16,32,2048]{2,1,0:T(8,128)(2,1)S(1)}, u32[]{:S(2)}, u32[]{:S(2)}) %all-to-all-start.1) | async-done | bytes 2097184 | tf_op jit(solution)/shard_map/all_to_all | solution.py:477
  111.9 1.0 copy-done.29
  112.9 1.0 copy-done.30
  114.0 1.0 copy-done.31
  115.0 1.0 copy-done.32
  116.1 17.7 %expert.1 = (bf16[512,2048]{1,0:T(8,128)(2,1)S(1)}, bf16[512,512]{1,0:T(8,128)(2,1)S(1)}, bf16[512,512]{1,0:T(8,128)(2,1)S(1)}, bf16[512,512]{1,0:T(8,128)(2,1)S(1)}, bf16[512,512]{1,0:T(8,128)(2,1)S(1)}) custom-call(bf16[512,2048]{1,0:T(8,128)(2,1)S(1)} %bitcast.122, bf16[512,512]{1,0:T(8,128)(2,1)S(1)} %copy-done.30, bf16[512,512]{1,0:T(8,128)(2,1)S(1)} %copy-done.32, ...), custom_call_target="tpu_custom_call" | custom-call | flops 6442450944 | bytes 18874368 | tf_op jit(solution)/shard_map/expert/pallas_call | solution.py:338
  133.8 1.3 copy-done.3
  138.3 9.9 %all-to-all-start.2 = ((bf16[16,32,2048]{2,1,0:T(8,128)(2,1)}), bf16[16,32,2048]{2,1,0:T(8,128)(2,1)}, u32[]{:S(2)}, u32[]{:S(2)}) async-start(bf16[16,32,2048]{2,1,0:T(8,128)(2,1)} %bitcast.125), calls=%async_computation.2 | async-start | bytes 4194304 | tf_op jit(solution)/shard_map/all_to_all | solution.py:537
  148.2 1.9 collective-permute-start.10
  150.1 1.5 collective-permute-start.11
  152.1 2.6 fusion.106
  154.7 1.5 collective-permute-start.13
  156.2 1.3 fusion.104
  157.7 1.3 fusion.105
  159.3 2.7 add_convert_fusion.2
  162.0 6.1 %collective-permute-done.10.refs_1_ = bf16[256,1024]{1,0:T(8,128)(2,1)S(1)} collective-permute-done((bf16[256,1024]{1,0:T(8,128)(2,1)}, bf16[256,1024]{1,0:T(8,128)(2,1)S(1)}, u32[]{:S(2)}, u32[]{:S(2)}) %collective-permute-start.10) | collective-permute-done | bytes 524320 | tf_op jit(solution)/shard_map/ppermute | solution.py:40
  168.1 12.5 %collective-permute-start.12 = (bf16[256,1024]{1,0:T(8,128)(2,1)S(1)}, bf16[256,1024]{1,0:T(8,128)(2,1)S(1)}, u32[]{:S(2)}, u32[]{:S(2)}) collective-permute-start(bf16[256,1024]{1,0:T(8,128)(2,1)S(1)} %copy-done.4), channel_id=1, source_target_pairs={{0,6},{2,4},{4,2},{6,0},{8,14},{10,12},{12,10},{14,8},{16,22},{18,... | collective-permute-start | bytes 1572872 | tf_op jit(solution)/shard_map/ppermute | solution.py:40
  180.6 14.0 %collective-permute-done.13.refs_4_ = bf16[256,1024]{1,0:T(8,128)(2,1)S(1)} collective-permute-done((bf16[256,1024]{1,0:T(8,128)(2,1)S(1)}, bf16[256,1024]{1,0:T(8,128)(2,1)S(1)}, u32[]{:S(2)}, u32[]{:S(2)}) %collective-permute-start.13) | collective-permute-done | bytes 524320 | tf_op jit(solution)/shard_map/ppermute | solution.py:40
  194.6 1.5 collective-permute-start.14
  196.1 2.1 collective-permute-start.15
  198.7 2.7 add_convert_fusion.1
  201.4 1.6 collective-permute-start.9
  202.9 2.7 add_convert_fusion
  206.4 4.0 %collective-permute-done.14.refs_5_ = bf16[256,1024]{1,0:T(8,128)(2,1)S(1)} collective-permute-done((bf16[256,1024]{1,0:T(8,128)(2,1)S(1)}, bf16[256,1024]{1,0:T(8,128)(2,1)S(1)}, u32[]{:S(2)}, u32[]{:S(2)}) %collective-permute-start.14) | collective-permute-done | bytes 524320 | tf_op jit(solution)/shard_map/ppermute | solution.py:40
  211.3 8.3 %collective-permute-done.15.refs_6_ = bf16[256,1024]{1,0:T(8,128)(2,1)S(1)} collective-permute-done((bf16[256,1024]{1,0:T(8,128)(2,1)S(1)}, bf16[256,1024]{1,0:T(8,128)(2,1)S(1)}, u32[]{:S(2)}, u32[]{:S(2)}) %collective-permute-start.15) | collective-permute-done | bytes 524320 | tf_op jit(solution)/shard_map/ppermute | solution.py:40
  220.4 1.4 collective-permute-done.16.refs_7_
  222.7 2.4 convolution_convert_fusion.1.mine_ref
  225.1 2.6 collective-permute-done.17.other_ref
  227.8 2.0 combine.1
  229.8 5.7 %all-to-all-start.3 = ((bf16[8,256,256]{2,1,0:T(8,128)(2,1)}), bf16[8,256,256]{2,1,0:T(8,128)(2,1)S(1)}, u32[]{:S(2)}, u32[]{:S(2)}) async-start(bf16[8,256,256]{2,1,0:T(8,128)(2,1)} %get-tuple-element.96), calls=%async_computation.3 | async-start | bytes 2097152 | tf_op jit(solution)/shard_map/all_to_all | solution.py:559
  235.5 7.1 %mixer.1 = (bf16[256,1024]{1,0:T(8,128)(2,1)}, bf16[256,1024]{1,0:T(8,128)(2,1)}, bf16[256,1024]{1,0:T(8,128)(2,1)}, f32[2,1024]{1,0:T(2,128)}, f32[2,8,1024]{2,1,0:T(8,128)}) custom-call(bf16[256,2048]{1,0:T(8,128)(2,1)} %get-tuple-element.65.grad_ref, bf16[2048,1024]{1,0:T(8,128)(2,1)} %weight_ref.1, f32[256,1024]{1,0:T(8,128)} %get-tuple-element.98.gelu_ref, ...), custom_call_target="tpu_custom_call" | custom-call | flops 1073741824 | bytes 8388608 | tf_op jit(solution)/shard_map/mixer/pallas_call | solution.py:100
  242.6 1.3 collective-permute-start.21
  243.9 2.7 collective-permute-start.18
  246.6 2.0 collective-permute-start.19
  249.6 1.5 collective-permute-done.18.refs_1_
  251.1 2.4 collective-permute-done.20.refs_3_
  256.6 1.0 copy-done.21
  257.6 1.0 copy-done.23
  258.7 1.8 product.1
  260.5 1.9 collective-permute-start.22
  262.4 1.2 collective-permute-start.24
  263.6 1.4 collective-permute-start.25
  265.0 1.8 collective-permute-start.26
  266.9 1.3 collective-permute-start.23
  268.7 3.7 %collective-permute-done.23.next_ref = f32[2,1024]{1,0:T(2,128)S(1)} collective-permute-done((f32[2,1024]{1,0:T(2,128)S(1)}, f32[2,1024]{1,0:T(2,128)S(1)}, u32[]{:S(2)}, u32[]{:S(2)}) %collective-permute-start.23) | collective-permute-done | bytes 8224 | tf_op jit(solution)/shard_map/ppermute | solution.py:35
  272.4 1.3 collective-permute-done.25.refs_2_
  274.4 5.1 %tail.1 = bf16[256,1024]{1,0:T(8,128)(2,1)} custom-call(s32[2]{0:T(128)} %pad_add_fusion.where_ref, f32[2,1024]{1,0:T(2,128)} %copy-done.24, f32[2,1024]{1,0:T(2,128)} %copy-done.51, f32[2,1024]{1,0:T(2,128)} %copy-done.25, f32[2,1024]{1,0:T(2,128)} %copy-done.48, f32[2,1024]{1,0:T(2,128)} %copy-done.49, f32[2,1024]{1,0:T(2,128)} %copy-done.50, ...), custom_call_target="tpu_custom_call" | custom-call | flops 268435456 | bytes 7340032 | tf_op jit(solution)/shard_map/tail/pallas_call | solution.py:225
  (179 shorter events, 23.2 us)
Async XLA Ops:
  0.6 3.8 %copy-start = (bf16[256,2048]{1,0:T(8,128)(2,1)S(1)}, bf16[256,2048]{1,0:T(8,128)(2,1)}, u32[]{:S(2)}) copy-start(bf16[256,2048]{1,0:T(8,128)(2,1)} %param.16) | copy-start | bytes 3145732
  6.5 14.5 %copy-start.53 = (f32[256,2]{0,1:T(2,128)S(1)}, f32[256,2]{0,1:T(2,128)}, u32[]{:S(2)}) copy-start(f32[256,2]{0,1:T(2,128)} %param.19) | copy-start | bytes 6148
  6.5 14.8 %copy-start.52 = (f32[1024]{0:T(1024)S(1)}, f32[1024]{0:T(1024)}, u32[]{:S(2)}) copy-start(f32[1024]{0:T(1024)} %param.30) | copy-start | bytes 12292
  6.5 14.8 %copy-start.46 = (bf16[4,1024]{1,0:T(4,128)(2,1)S(1)}, bf16[4,1024]{1,0:T(4,128)(2,1)}, u32[]{:S(2)}) copy-start(bf16[4,1024]{1,0:T(4,128)(2,1)} %refs_11_.1) | copy-start | bytes 24580
  6.5 14.8 %copy-start.2 = (bf16[256,2048]{1,0:T(8,128)(2,1)S(1)}, bf16[256,2048]{1,0:T(8,128)(2,1)}, u32[]{:S(2)}) copy-start(bf16[256,2048]{1,0:T(8,128)(2,1)} %cot_ref.1) | copy-start | bytes 3145732
  6.5 51.5 %all-to-all-start = ((bf16[16,32,2048]{2,1,0:T(8,128)(2,1)}), bf16[16,32,2048]{2,1,0:T(8,128)(2,1)S(1)}, u32[]{:S(2)}, u32[]{:S(2)}) async-start(bf16[16,32,2048]{2,1,0:T(8,128)(2,1)} %bitcast.134), calls=%async_computation | async-start | bytes 4194304 | tf_op jit(solution)/shard_map/all_to_all | solution.py:458
  16.5 10.0 %collective-permute-start = (f32[4,1024]{1,0:T(4,128)S(1)}, f32[4,1024]{1,0:T(4,128)S(1)}, u32[]{:S(2)}, u32[]{:S(2)}) collective-permute-start(f32[4,1024]{1,0:T(4,128)S(1)} %pad_maximum_fusion.2), channel_id=1, source_target_pairs={{0,2},{2,4},{4,6},{6,8},{8,10},{10,12},{12,14},{14,16},{16,18},{18... | collective-permute-start | bytes 49160 | tf_op jit(solution)/shard_map/ppermute | solution.py:35
  20.4 61.6 %collective-permute-start.3 = (bf16[2048,512]{1,0:T(8,128)(2,1)}, bf16[2048,512]{1,0:T(8,128)(2,1)}, u32[]{:S(2)}, u32[]{:S(2)}) collective-permute-start(bf16[2048,512]{1,0:T(8,128)(2,1)} %bitcast.144), channel_id=1, source_target_pairs={{0,1},{1,0},{2,3},{3,2},{4,5},{5,4},{6,7},{7,6},{8,9},{9,8},{10,11... | collective-permute-start | bytes 6291464 | tf_op jit(solution)/shard_map/ppermute | solution.py:40
  20.4 68.7 %collective-permute-start.2 = (bf16[2048,512]{1,0:T(8,128)(2,1)}, bf16[2048,512]{1,0:T(8,128)(2,1)}, u32[]{:S(2)}, u32[]{:S(2)}) collective-permute-start(bf16[2048,512]{1,0:T(8,128)(2,1)} %bitcast.4.refs_6_), channel_id=1, source_target_pairs={{0,1},{1,0},{2,3},{3,2},{4,5},{5,4},{6,7},{7,6},{8,9},{9,8},{10,11... | collective-permute-start | bytes 6291464 | tf_op jit(solution)/shard_map/ppermute | solution.py:40
  20.9 91.0 %collective-permute-start.4 = (bf16[512,2048]{1,0:T(8,128)(2,1)}, bf16[512,2048]{1,0:T(8,128)(2,1)}, u32[]{:S(2)}, u32[]{:S(2)}) collective-permute-start(bf16[512,2048]{1,0:T(8,128)(2,1)} %bitcast.30.refs_4_), channel_id=1, source_target_pairs={{0,1},{1,0},{2,3},{3,2},{4,5},{5,4},{6,7},{7,6},{8,9},{9,8},{10,11... | collective-permute-start | bytes 6291464 | tf_op jit(solution)/shard_map/ppermute | solution.py:40
  21.0 2.4 copy-start.38
  21.0 2.4 copy-start.44
  23.4 2.1 copy-start.43
  59.4 52.5 %all-to-all-start.1 = ((bf16[16,32,2048]{2,1,0:T(8,128)(2,1)}), bf16[16,32,2048]{2,1,0:T(8,128)(2,1)S(1)}, u32[]{:S(2)}, u32[]{:S(2)}) async-start(bf16[16,32,2048]{2,1,0:T(8,128)(2,1)} %bitcast.133), calls=%async_computation.1 | async-start | bytes 4194304 | tf_op jit(solution)/shard_map/all_to_all | solution.py:477
  69.4 3.1 %copy-start.41 = (bf16[8,128,128]{2,1,0:T(8,128)(2,1)S(1)}, bf16[8,128,128]{2,1,0:T(8,128)(2,1)}, u32[]{:S(2)}) copy-start(bf16[8,128,128]{2,1,0:T(8,128)(2,1)} %refs_13_.1) | copy-start | bytes 786436
  69.4 10.4 %collective-permute-start.1 = (bf16[512,2048]{1,0:T(8,128)(2,1)}, bf16[512,2048]{1,0:T(8,128)(2,1)S(1)}, u32[]{:S(2)}, u32[]{:S(2)}) collective-permute-start(bf16[512,2048]{1,0:T(8,128)(2,1)} %bitcast.126), channel_id=1, source_target_pairs={{0,1},{1,0},{2,3},{3,2},{4,5},{5,4},{6,7},{7,6},{8,9},{9,8},{10,11... | collective-permute-start | bytes 6291464 | tf_op jit(solution)/shard_map/ppermute | solution.py:40
  69.5 4.2 %copy-start.42 = (bf16[8,128,128]{2,1,0:T(8,128)(2,1)S(1)}, bf16[8,128,128]{2,1,0:T(8,128)(2,1)}, u32[]{:S(2)}) copy-start(bf16[8,128,128]{2,1,0:T(8,128)(2,1)} %refs_12_.1) | copy-start | bytes 786436
  72.5 2.5 copy-start.39
  72.5 2.5 copy-start.40
  78.0 1.8 copy-start.34
  78.0 2.6 copy-start.54
  138.3 84.4 %all-to-all-start.2 = ((bf16[16,32,2048]{2,1,0:T(8,128)(2,1)}), bf16[16,32,2048]{2,1,0:T(8,128)(2,1)}, u32[]{:S(2)}, u32[]{:S(2)}) async-start(bf16[16,32,2048]{2,1,0:T(8,128)(2,1)} %bitcast.125), calls=%async_computation.2 | async-start | bytes 4194304 | tf_op jit(solution)/shard_map/all_to_all | solution.py:537
  148.2 6.5 %collective-permute-start.5 = (bf16[512,512]{1,0:T(8,128)(2,1)}, bf16[512,512]{1,0:T(8,128)(2,1)S(1)}, u32[]{:S(2)}, u32[]{:S(2)}) collective-permute-start(bf16[512,512]{1,0:T(8,128)(2,1)} %copy-done.28), channel_id=1, source_target_pairs={{0,1},{1,0},{2,3},{3,2},{4,5},{5,4},{6,7},{7,6},{8,9},{9,8},{10,11... | collective-permute-start | bytes 1572872 | tf_op jit(solution)/shard_map/ppermute | solution.py:40
  148.2 19.9 %collective-permute-start.10 = (bf16[256,1024]{1,0:T(8,128)(2,1)}, bf16[256,1024]{1,0:T(8,128)(2,1)S(1)}, u32[]{:S(2)}, u32[]{:S(2)}) collective-permute-start(bf16[256,1024]{1,0:T(8,128)(2,1)} %get-tuple-element.105.refs_0_), channel_id=1, source_target_pairs={{0,2},{2,0},{4,6},{6,4},{8,10},{10,8},{12,14},{14,12},{16,18},{18,... | collective-permute-start | bytes 1572872 | tf_op jit(solution)/shard_map/ppermute | solution.py:40
  150.1 45.9 %collective-permute-start.11 = (bf16[256,1024]{1,0:T(8,128)(2,1)}, bf16[256,1024]{1,0:T(8,128)(2,1)S(1)}, u32[]{:S(2)}, u32[]{:S(2)}) collective-permute-start(bf16[256,1024]{1,0:T(8,128)(2,1)} %get-tuple-element.105.refs_0_), channel_id=1, source_target_pairs={{0,4},{2,6},{4,0},{6,2},{8,12},{10,14},{12,8},{14,10},{16,20},{18,... | collective-permute-start | bytes 1572872 | tf_op jit(solution)/shard_map/ppermute | solution.py:40
  151.6 49.8 %collective-permute-start.8 = (bf16[512,2048]{1,0:T(8,128)(2,1)S(1)}, bf16[512,2048]{1,0:T(8,128)(2,1)S(1)}, u32[]{:S(2)}, u32[]{:S(2)}) collective-permute-start(bf16[512,2048]{1,0:T(8,128)(2,1)S(1)} %bitcast.123), channel_id=1, source_target_pairs={{0,1},{1,0},{2,3},{3,2},{4,5},{5,4},{6,7},{7,6},{8,9},{9,8},{10,11... | collective-permute-start | bytes 6291464 | tf_op jit(solution)/shard_map/ppermute | solution.py:40
  151.6 3.1 %copy-start.4 = (bf16[256,1024]{1,0:T(8,128)(2,1)S(1)}, bf16[256,1024]{1,0:T(8,128)(2,1)}, u32[]{:S(2)}) copy-start(bf16[256,1024]{1,0:T(8,128)(2,1)} %get-tuple-element.105.refs_0_) | copy-start | bytes 1572868
  151.6 4.7 %copy-start.37 = (bf16[512,2048]{1,0:T(8,128)(2,1)S(1)}, bf16[512,2048]{1,0:T(8,128)(2,1)}, u32[]{:S(2)}) copy-start(bf16[512,2048]{1,0:T(8,128)(2,1)} %copy-done.36) | copy-start | bytes 6291460
  151.6 6.0 %collective-permute-start.6 = (bf16[512,512]{1,0:T(8,128)(2,1)}, bf16[512,512]{1,0:T(8,128)(2,1)S(1)}, u32[]{:S(2)}, u32[]{:S(2)}) collective-permute-start(bf16[512,512]{1,0:T(8,128)(2,1)} %copy-done.27), channel_id=1, source_target_pairs={{0,1},{1,0},{2,3},{3,2},{4,5},{5,4},{6,7},{7,6},{8,9},{9,8},{10,11... | collective-permute-start | bytes 1572872 | tf_op jit(solution)/shard_map/ppermute | solution.py:40
  154.7 2.9 %copy-start.55 = (bf16[512,512]{1,0:T(8,128)(2,1)S(1)}, bf16[512,512]{1,0:T(8,128)(2,1)}, u32[]{:S(2)}) copy-start(bf16[512,512]{1,0:T(8,128)(2,1)} %get-tuple-element.90) | copy-start | bytes 1572868
  154.7 39.9 %collective-permute-start.13 = (bf16[256,1024]{1,0:T(8,128)(2,1)S(1)}, bf16[256,1024]{1,0:T(8,128)(2,1)S(1)}, u32[]{:S(2)}, u32[]{:S(2)}) collective-permute-start(bf16[256,1024]{1,0:T(8,128)(2,1)S(1)} %copy-done.4), channel_id=1, source_target_pairs={{0,8},{2,10},{4,12},{6,14},{8,0},{10,2},{12,4},{14,6},{16,24},{18,... | collective-permute-start | bytes 1572872 | tf_op jit(solution)/shard_map/ppermute | solution.py:40
  157.5 1.4 copy-start.9
  157.5 1.8 copy-start.35
  157.6 40.5 %collective-permute-start.7 = (bf16[512,512]{1,0:T(8,128)(2,1)S(1)}, bf16[512,512]{1,0:T(8,128)(2,1)S(1)}, u32[]{:S(2)}, u32[]{:S(2)}) collective-permute-start(bf16[512,512]{1,0:T(8,128)(2,1)S(1)} %copy-done.55), channel_id=1, source_target_pairs={{0,1},{1,0},{2,3},{3,2},{4,5},{5,4},{6,7},{7,6},{8,9},{9,8},{10,11... | collective-permute-start | bytes 1572872 | tf_op jit(solution)/shard_map/ppermute | solution.py:40
  159.3 39.3 %copy-start.7 = (bf16[512,512]{1,0:T(8,128)(2,1)S(1)}, bf16[512,512]{1,0:T(8,128)(2,1)}, u32[]{:S(2)}) copy-start(bf16[512,512]{1,0:T(8,128)(2,1)} %copy-done.6) | copy-start | bytes 1572868
  168.1 33.3 %copy-start.10 = (bf16[256,1024]{1,0:T(8,128)(2,1)}, bf16[256,1024]{1,0:T(8,128)(2,1)S(1)}, u32[]{:S(2)}) copy-start(bf16[256,1024]{1,0:T(8,128)(2,1)S(1)} %collective-permute-done.10.refs_1_) | copy-start | bytes 1572868
  168.1 37.5 %collective-permute-start.12 = (bf16[256,1024]{1,0:T(8,128)(2,1)S(1)}, bf16[256,1024]{1,0:T(8,128)(2,1)S(1)}, u32[]{:S(2)}, u32[]{:S(2)}) collective-permute-start(bf16[256,1024]{1,0:T(8,128)(2,1)S(1)} %copy-done.4), channel_id=1, source_target_pairs={{0,6},{2,4},{4,2},{6,0},{8,14},{10,12},{12,10},{14,8},{16,22},{18,... | collective-permute-start | bytes 1572872 | tf_op jit(solution)/shard_map/ppermute | solution.py:40
  194.6 6.8 %copy-start.14 = (bf16[256,1024]{1,0:T(8,128)(2,1)}, bf16[256,1024]{1,0:T(8,128)(2,1)S(1)}, u32[]{:S(2)}) copy-start(bf16[256,1024]{1,0:T(8,128)(2,1)S(1)} %collective-permute-done.13.refs_4_) | copy-start | bytes 1572868
  194.6 15.9 %collective-permute-start.14 = (bf16[256,1024]{1,0:T(8,128)(2,1)S(1)}, bf16[256,1024]{1,0:T(8,128)(2,1)S(1)}, u32[]{:S(2)}, u32[]{:S(2)}) collective-permute-start(bf16[256,1024]{1,0:T(8,128)(2,1)S(1)} %collective-permute-done.13.refs_4_), channel_id=1, source_target_pairs={{0,2},{2,0},{4,6},{6,4},{8,10},{10,8},{12,14},{14,12},{16,18},{18,... | collective-permute-start | bytes 1572872 | tf_op jit(solution)/shard_map/ppermute | solution.py:40
  196.1 5.3 %copy-start.12 = (bf16[256,1024]{1,0:T(8,128)(2,1)}, bf16[256,1024]{1,0:T(8,128)(2,1)S(1)}, u32[]{:S(2)}) copy-start(bf16[256,1024]{1,0:T(8,128)(2,1)S(1)} %collective-permute-done.11.refs_2_) | copy-start | bytes 1572868
  196.1 23.5 %collective-permute-start.15 = (bf16[256,1024]{1,0:T(8,128)(2,1)S(1)}, bf16[256,1024]{1,0:T(8,128)(2,1)S(1)}, u32[]{:S(2)}, u32[]{:S(2)}) collective-permute-start(bf16[256,1024]{1,0:T(8,128)(2,1)S(1)} %collective-permute-done.13.refs_4_), channel_id=1, source_target_pairs={{0,4},{2,6},{4,0},{6,2},{8,12},{10,14},{12,8},{14,10},{16,20},{18,... | collective-permute-start | bytes 1572872 | tf_op jit(solution)/shard_map/ppermute | solution.py:40
  198.1 23.7 %collective-permute-start.16 = (bf16[256,1024]{1,0:T(8,128)(2,1)S(1)}, bf16[256,1024]{1,0:T(8,128)(2,1)S(1)}, u32[]{:S(2)}, u32[]{:S(2)}) collective-permute-start(bf16[256,1024]{1,0:T(8,128)(2,1)S(1)} %collective-permute-done.13.refs_4_), channel_id=1, source_target_pairs={{0,6},{2,4},{4,2},{6,0},{8,14},{10,12},{12,10},{14,8},{16,22},{18,... | collective-permute-start | bytes 1572872 | tf_op jit(solution)/shard_map/ppermute | solution.py:40
  201.4 21.3 %collective-permute-start.9 = (f32[3,8,1024]{2,1,0:T(8,128)S(1)}, f32[3,8,1024]{2,1,0:T(8,128)S(1)}, u32[]{:S(2)}, u32[]{:S(2)}) collective-permute-start(f32[3,8,1024]{2,1,0:T(8,128)S(1)} %pad_maximum_fusion.1), channel_id=1, source_target_pairs={{2,0},{4,2},{6,4},{8,6},{10,8},{12,10},{14,12},{16,14},{18,16},{20... | collective-permute-start | bytes 294920 | tf_op jit(solution)/shard_map/ppermute | solution.py:35
  222.7 7.1 %copy-start.45 = (f32[3,8,1024]{2,1,0:T(8,128)}, f32[3,8,1024]{2,1,0:T(8,128)S(1)}, u32[]{:S(2)}) copy-start(f32[3,8,1024]{2,1,0:T(8,128)S(1)} %collective-permute-done.9.refs_10_) | copy-start | bytes 294916
  225.1 2.7 collective-permute-start.17
  229.8 23.6 %all-to-all-start.3 = ((bf16[8,256,256]{2,1,0:T(8,128)(2,1)}), bf16[8,256,256]{2,1,0:T(8,128)(2,1)S(1)}, u32[]{:S(2)}, u32[]{:S(2)}) async-start(bf16[8,256,256]{2,1,0:T(8,128)(2,1)} %get-tuple-element.96), calls=%async_computation.3 | async-start | bytes 2097152 | tf_op jit(solution)/shard_map/all_to_all | solution.py:559
  235.5 17.9 %copy-start.5 = (bf16[256,1024]{1,0:T(8,128)(2,1)S(1)}, bf16[256,1024]{1,0:T(8,128)(2,1)}, u32[]{:S(2)}) copy-start(bf16[256,1024]{1,0:T(8,128)(2,1)} %get-tuple-element.105.refs_0_) | copy-start | bytes 1572868
  235.5 17.9 %copy-start.11 = (bf16[256,1024]{1,0:T(8,128)(2,1)S(1)}, bf16[256,1024]{1,0:T(8,128)(2,1)}, u32[]{:S(2)}) copy-start(bf16[256,1024]{1,0:T(8,128)(2,1)} %copy-done.10) | copy-start | bytes 1572868
  235.5 17.9 %copy-start.13 = (bf16[256,1024]{1,0:T(8,128)(2,1)S(1)}, bf16[256,1024]{1,0:T(8,128)(2,1)}, u32[]{:S(2)}) copy-start(bf16[256,1024]{1,0:T(8,128)(2,1)} %copy-done.12) | copy-start | bytes 1572868
  242.6 10.8 %collective-permute-start.21 = (f32[2,8,1024]{2,1,0:T(8,128)}, f32[2,8,1024]{2,1,0:T(8,128)S(1)}, u32[]{:S(2)}, u32[]{:S(2)}) collective-permute-start(f32[2,8,1024]{2,1,0:T(8,128)} %get-tuple-element.103), channel_id=1, source_target_pairs={{2,0},{4,2},{6,4},{8,6},{10,8},{12,10},{14,12},{16,14},{18,16},{20... | collective-permute-start | bytes 196616 | tf_op jit(solution)/shard_map/ppermute | solution.py:35
  243.9 7.1 %collective-permute-start.18 = (f32[2,1024]{1,0:T(2,128)}, f32[2,1024]{1,0:T(2,128)S(1)}, u32[]{:S(2)}, u32[]{:S(2)}) collective-permute-start(f32[2,1024]{1,0:T(2,128)} %get-tuple-element.115.refs_0_), channel_id=1, source_target_pairs={{0,2},{2,0},{4,6},{6,4},{8,10},{10,8},{12,14},{14,12},{16,18},{18,... | collective-permute-start | bytes 24584 | tf_op jit(solution)/shard_map/ppermute | solution.py:40
  246.6 4.4 %collective-permute-start.19 = (f32[2,1024]{1,0:T(2,128)}, f32[2,1024]{1,0:T(2,128)S(1)}, u32[]{:S(2)}, u32[]{:S(2)}) collective-permute-start(f32[2,1024]{1,0:T(2,128)} %get-tuple-element.115.refs_0_), channel_id=1, source_target_pairs={{0,4},{2,6},{4,0},{6,2},{8,12},{10,14},{12,8},{14,10},{16,20},{18,... | collective-permute-start | bytes 24584 | tf_op jit(solution)/shard_map/ppermute | solution.py:40
  248.7 4.8 %collective-permute-start.20 = (f32[2,1024]{1,0:T(2,128)}, f32[2,1024]{1,0:T(2,128)S(1)}, u32[]{:S(2)}, u32[]{:S(2)}) collective-permute-start(f32[2,1024]{1,0:T(2,128)} %get-tuple-element.115.refs_0_), channel_id=1, source_target_pairs={{0,6},{2,4},{4,2},{6,0},{8,14},{10,12},{12,10},{14,8},{16,22},{18,... | collective-permute-start | bytes 24584 | tf_op jit(solution)/shard_map/ppermute | solution.py:40
  253.4 7.0 %copy-start.47 = (f32[2,8,1024]{2,1,0:T(8,128)}, f32[2,8,1024]{2,1,0:T(8,128)S(1)}, u32[]{:S(2)}) copy-start(f32[2,8,1024]{2,1,0:T(8,128)S(1)} %collective-permute-done.21.refs_9_) | copy-start | bytes 196612
  258.7 3.7 %copy-start.26 = (f32[2,1024]{1,0:T(2,128)S(1)}, f32[2,1024]{1,0:T(2,128)}, u32[]{:S(2)}) copy-start(f32[2,1024]{1,0:T(2,128)} %get-tuple-element.115.refs_0_) | copy-start | bytes 24580
  260.5 19.1 %collective-permute-start.22 = (bf16[128,1024]{1,0:T(8,128)(2,1)S(1)}, bf16[128,1024]{1,0:T(8,128)(2,1)S(1)}, u32[]{:S(2)}, u32[]{:S(2)}) collective-permute-start(bf16[128,1024]{1,0:T(8,128)(2,1)S(1)} %get-tuple-element.114), channel_id=1, source_target_pairs={{0,16},{2,18},{4,20},{6,22},{8,24},{10,26},{12,28},{14,30},{16,0},... | collective-permute-start | bytes 786440 | tf_op jit(solution)/shard_map/ppermute | solution.py:40
  262.4 11.4 %copy-start.24 = (f32[2,1024]{1,0:T(2,128)}, f32[2,1024]{1,0:T(2,128)S(1)}, u32[]{:S(2)}) copy-start(f32[2,1024]{1,0:T(2,128)S(1)} %get-tuple-element.119.later_ref) | copy-start | bytes 24580
  262.4 11.4 %copy-start.25 = (f32[2,1024]{1,0:T(2,128)}, f32[2,1024]{1,0:T(2,128)S(1)}, u32[]{:S(2)}) copy-start(f32[2,1024]{1,0:T(2,128)S(1)} %get-tuple-element.120.refs_0_) | copy-start | bytes 24580
  262.4 10.0 %collective-permute-start.24 = (f32[2,1024]{1,0:T(2,128)S(1)}, f32[2,1024]{1,0:T(2,128)S(1)}, u32[]{:S(2)}, u32[]{:S(2)}) collective-permute-start(f32[2,1024]{1,0:T(2,128)S(1)} %get-tuple-element.120.refs_0_), channel_id=1, source_target_pairs={{0,8},{2,10},{4,12},{6,14},{8,0},{10,2},{12,4},{14,6},{16,24},{18,... | collective-permute-start | bytes 24584 | tf_op jit(solution)/shard_map/ppermute | solution.py:40
  263.6 10.1 %collective-permute-start.25 = (f32[2,1024]{1,0:T(2,128)S(1)}, f32[2,1024]{1,0:T(2,128)S(1)}, u32[]{:S(2)}, u32[]{:S(2)}) collective-permute-start(f32[2,1024]{1,0:T(2,128)S(1)} %get-tuple-element.120.refs_0_), channel_id=1, source_target_pairs={{0,16},{2,18},{4,20},{6,22},{8,24},{10,26},{12,28},{14,30},{16,0},... | collective-permute-start | bytes 24584 | tf_op jit(solution)/shard_map/ppermute | solution.py:40
  265.0 8.7 %collective-permute-start.26 = (f32[2,1024]{1,0:T(2,128)S(1)}, f32[2,1024]{1,0:T(2,128)S(1)}, u32[]{:S(2)}, u32[]{:S(2)}) collective-permute-start(f32[2,1024]{1,0:T(2,128)S(1)} %get-tuple-element.120.refs_0_), channel_id=1, source_target_pairs={{0,24},{2,26},{4,28},{6,30},{8,16},{10,18},{12,20},{14,22},{16,8},... | collective-permute-start | bytes 24584 | tf_op jit(solution)/shard_map/ppermute | solution.py:40
  266.9 5.5 %collective-permute-start.23 = (f32[2,1024]{1,0:T(2,128)S(1)}, f32[2,1024]{1,0:T(2,128)S(1)}, u32[]{:S(2)}, u32[]{:S(2)}) collective-permute-start(f32[2,1024]{1,0:T(2,128)S(1)} %get-tuple-element.119.later_ref), channel_id=1, source_target_pairs={{2,0},{4,2},{6,4},{8,6},{10,8},{12,10},{14,12},{16,14},{18,16},{20... | collective-permute-start | bytes 24584 | tf_op jit(solution)/shard_map/ppermute | solution.py:35
  272.4 1.4 copy-start.48
  273.8 6.6 %copy-start.1 = (bf16[256,2048]{1,0:T(8,128)(2,1)S(1)}, bf16[256,2048]{1,0:T(8,128)(2,1)}, u32[]{:S(2)}) copy-start(bf16[256,2048]{1,0:T(8,128)(2,1)} %param.16) | copy-start | bytes 3145732
  (23 other events, 22.3 us)

commit v6 on v4

--- a/solution.py
+++ b/solution.py
@@ -346,8 +346,12 @@
     half = group // 2
     mixers = {0: mixer_out}
     mixers[half] = swapped(mixer_out, "sp", half)
-    send_grads, gelu_value, slope, edge, got_rows = lax.optimization_barrier(
-        (send_grads, gelu_value, slope, edge, got_rows)
+    weights = tuple(
+        jnp.concatenate([own, other], axis=axis)
+        for own, other, axis in zip(own_weights, other_weights, (1, 1, 0))
+    )
+    send_grads, gelu_value, slope, edge, got_rows, weights = lax.optimization_barrier(
+        (send_grads, gelu_value, slope, edge, got_rows, weights)
     )
     got_grads = lax.all_to_all(send_grads, "sp", split_axis=0, concat_axis=0, tiled=True)
     for k in range(1, half):
@@ -394,7 +398,7 @@
         slope_gate = up_pre * sigmoid_gate * (1.0 + gate_pre * (1.0 - sigmoid_gate))
         return (silu_gate * up_pre).astype(bf16), silu_gate.astype(bf16), slope_gate.astype(bf16)
 
-    pres = tuple(first_half(weights[0], weights[1]) for weights in (own_weights, other_weights))
+    pres = first_half(weights[0], weights[1])
     head_coef = jnp.stack([to_decay[:8], to_input[:8], direct[:8]])
     gates = (
         next_decay, decay_value[:1], head_coef,
@@ -410,22 +414,19 @@
         hidden_grad = cols_of(grads_here, down_w)
         return (hidden_grad * pre[2].astype(f32)).astype(bf16), (hidden_grad * pre[1].astype(f32)).astype(bf16)
 
-    own_grads = second_half(pres[0], own_weights[2])
-    other_grads = second_half(pres[1], other_weights[2])
-    partial = (
-        cols_of(own_grads[0], own_weights[0])
-        + cols_of(own_grads[1], own_weights[1])
-        + cols_of(other_grads[0], other_weights[0])
-        + cols_of(other_grads[1], other_weights[1])
-    )
+    gate_grads, up_grads = second_half(pres, weights[2])
+    partial = cols_of(gate_grads, weights[0]) + cols_of(up_grads, weights[1])
     shared = partial.astype(bf16).reshape(experts, share, width)
     back = lax.all_to_all(shared, "sp", split_axis=0, concat_axis=0, tiled=True)
     head_coef = shifted(head_coef, "sp", -1)
-    hidden_h, gate_h, up_h = pres[0][0], own_grads[0], own_grads[1]
+    units = own_weights[0].shape[1]
+    (hidden_h, hidden_o), (gate_h, gate_o), (up_h, up_o) = (
+        (value[:, :units], value[:, units:]) for value in (pres[0], gate_grads, up_grads)
+    )
     grads_there = swapped(grads_here, "tp", 1)
-    hidden_t = swapped(pres[1][0], "tp", 1)
-    gate_t = swapped(other_grads[0], "tp", 1)
-    up_t = swapped(other_grads[1], "tp", 1)
+    hidden_t = swapped(hidden_o, "tp", 1)
+    gate_t = swapped(gate_o, "tp", 1)
+    up_t = swapped(up_o, "tp", 1)
     down_grad = rows_of(hidden_h, grads_here) + rows_of(hidden_t, grads_there)
     gate_weight_grad = rows_of(rows_here, gate_h) + rows_of(rows_there, gate_t)
     up_weight_grad = rows_of(rows_here, up_h) + rows_of(rows_there, up_t)

time: 308 us -> 268 us (0.87)
  matrix products: 79.6 us -> 49.4 us
  waiting for transfers between devices: 113 us -> 85.2 us
  starting transfers between devices: 61.2 us -> 71.7 us
  other arithmetic: 17.5 us -> 25.6 us
    dot_general x35 -> x30, matrix products: 79.6 us -> 49.4 us  [dot(): lax.dot_general(left, right, (contract, ((), ())), preferred_element_type...]
    ppermute x17, waiting for transfers between devices: 52.3 us -> 32.9 us  [swapped(): return lax.ppermute(value, axis, [(s, s ^ mask) for s in range(count)])]
    concatenate x0 -> x3, other arithmetic: none -> 12.8 us  [on_device(): jnp.concatenate([own, other], axis=axis)]
    all_to_all x1, waiting for transfers between devices: 30.8 us -> 20 us  [on_device(): lax.all_to_all(send_rows, 'sp', split_axis=0, concat_axis=0, tiled=True)]
    ppermute x17, starting transfers between devices: 15.5 us -> 25.7 us  [swapped(): return lax.ppermute(value, axis, [(s, s ^ mask) for s in range(count)])]
    unnamed x77 -> x79, local copies, waits for them, and re-layouts: 10.8 us -> 11.3 us
  transfers between devices with their start and end apart: 25 -> 25, of which waited for: 11 -> 11; matrix products, arithmetic and copies ran while one was open for 27% -> 22% of each run, Pallas kernels for 4% -> 5%
where the time goes in v6:
time: 268 us; the launch traced here: 264 us
  waiting for transfers between devices  85.2 us (32%)
  starting transfers between devices  71.7 us (27%)
  matrix products  49.4 us (18%)
  other arithmetic  25.6 us (10%)
  Pallas kernels  15.4 us (6%)
  local copies, waits for them, and re-layouts  15 us (6%)
    dot_general x30, matrix products, dot(): lax.dot_general(left, right, (contract, ((), ())), preferred_element_type...  49.4 us
    ppermute x17, waiting for transfers between devices, swapped(): return lax.ppermute(value, axis, [(s, s ^ mask) for s in range(count)])  32.9 us
    ppermute x17, starting transfers between devices, swapped(): return lax.ppermute(value, axis, [(s, s ^ mask) for s in range(count)])  25.7 us
    all_to_all x1, waiting for transfers between devices, on_device(): lax.all_to_all(send_rows, 'sp', split_axis=0, concat_axis=0, tiled=True)  20 us
    all_to_all x1, waiting for transfers between devices, on_device(): lax.all_to_all(send_grads, 'sp', split_axis=0, concat_axis=0, tiled=True)  19.5 us
    concatenate x3, other arithmetic, on_device(): jnp.concatenate([own, other], axis=axis)  12.8 us
    unnamed x79, local copies, waits for them, and re-layouts  11.3 us
    all_to_all x1, starting transfers between devices, on_device(): lax.all_to_all(send_grads, 'sp', split_axis=0, concat_axis=0, tiled=True)  10.2 us
  transfers between devices with their start and end apart: 25, of which 11 were waited for; matrix products, arithmetic and copies ran while one was open for 22% of the time, Pallas kernels for 5%

profile of v6, /device:TPU:0, one launch (start us, length us, event | category | flops | bytes accessed | tf_op | source)
XLA Modules:
  0.0 263.7 jit_solution(4266015199213929436)
XLA Ops:
  0.6 0.9 copy.85
  1.9 1.2 reduce-window.6
  4.5 2.0 convolution_convert_fusion
  6.5 8.7 %all-to-all-start = ((bf16[16,32,2048]{2,1,0:T(8,128)(2,1)}), bf16[16,32,2048]{2,1,0:T(8,128)(2,1)}, u32[]{:S(2)}, u32[]{:S(2)}) async-start(bf16[16,32,2048]{2,1,0:T(8,128)(2,1)} %bitcast.118), calls=%async_computation | async-start | bytes 4194304 | tf_op jit(solution)/shard_map/all_to_all | solution.py:333
  15.9 3.8 %collective-permute-start = (f32[4,1024]{1,0:T(4,128)S(1)}, f32[4,1024]{1,0:T(4,128)S(1)}, u32[]{:S(2)}, u32[]{:S(2)}) collective-permute-start(f32[4,1024]{1,0:T(4,128)S(1)} %pad_maximum_fusion.5), channel_id=1, source_target_pairs={{0,2},{2,4},{4,6},{6,8},{8,10},{10,12},{12,14},{14,16},{16,18},{18... | collective-permute-start | bytes 49160 | tf_op jit(solution)/shard_map/ppermute | solution.py:35
  19.8 1.1 convert_element_type.90
  21.2 2.0 multiply_convert_fusion
  23.2 2.1 multiply_convert_fusion.5
  25.4 4.3 %pad_maximum_fusion = bf16[2048,1024]{1,0:T(8,128)(2,1)} fusion(bf16[2048,512]{1,0:T(8,128)(2,1)} %collective-permute-done.1, bf16[2048,512]{1,0:T(8,128)(2,1)S(1)} %bitcast.125), kind=kLoop, calls=%fused_computation | loop fusion | flops 8388608 | bytes 8388608 | tf_op jit(solution)/shard_map/concatenate | solution.py:350
  29.7 4.3 %pad_maximum_fusion.1 = bf16[2048,1024]{1,0:T(8,128)(2,1)} fusion(bf16[2048,512]{1,0:T(8,128)(2,1)} %collective-permute-done.2, bf16[2048,512]{1,0:T(8,128)(2,1)S(1)} %bitcast.127), kind=kLoop, calls=%fused_computation.1 | loop fusion | flops 8388608 | bytes 8388608 | tf_op jit(solution)/shard_map/concatenate | solution.py:350
  34.0 4.2 %pad_maximum_fusion.2 = bf16[1024,2048]{1,0:T(8,128)(2,1)} fusion(bf16[512,2048]{1,0:T(8,128)(2,1)} %collective-permute-done.3, bf16[512,2048]{1,0:T(8,128)(2,1)S(1)} %bitcast.129), kind=kLoop, calls=%fused_computation.2 | loop fusion | flops 8388608 | bytes 8388608 | tf_op jit(solution)/shard_map/concatenate | solution.py:350
  38.3 20.0 %all-to-all-done = bf16[16,32,2048]{2,1,0:T(8,128)(2,1)} async-done(((bf16[16,32,2048]{2,1,0:T(8,128)(2,1)}), bf16[16,32,2048]{2,1,0:T(8,128)(2,1)}, u32[]{:S(2)}, u32[]{:S(2)}) %all-to-all-start) | async-done | bytes 2097184 | tf_op jit(solution)/shard_map/all_to_all | solution.py:333
  58.3 10.2 %all-to-all-start.1 = ((bf16[16,32,2048]{2,1,0:T(8,128)(2,1)}), bf16[16,32,2048]{2,1,0:T(8,128)(2,1)}, u32[]{:S(2)}, u32[]{:S(2)}) async-start(bf16[16,32,2048]{2,1,0:T(8,128)(2,1)} %bitcast.117), calls=%async_computation.1 | async-start | bytes 4194304 | tf_op jit(solution)/shard_map/all_to_all | solution.py:356
  68.7 3.2 %fusion.98 = (bf16[256,1024]{1,0:T(8,128)(2,1)S(1)}, f32[256,1024]{1,0:T(8,128)S(1)}) fusion(f32[256,1024]{1,0:T(8,128)} %convert_element_type.90, f32[1024]{0:T(1024)S(1)} %bitcast.134, f32[3,1024]{1,0:T(4,128)S(1)} %bitcast.130, f32[1024]{0:T(1024)S(1)} %bitcast.133, f32[1024]{0:T(1024)S(1)} %bitcast.132, f32[1024]{0:T(1024)S(1)} %bitcast.131), kind=kLoop, calls=%fused_computation.164 | loop fusion | flops 2883584 | bytes 2650112 | tf_op jit(solution)/shard_map/convert_element_type | solution.py:366
  74.4 3.0 %fusion.96 = (bf16[256,1024]{1,0:T(8,128)(2,1)}, f32[256,1024]{1,0:T(8,128)S(1)}, bf16[256,1024]{1,0:T(8,128)(2,1)}, f32[256,1024]{1,0:T(8,128)S(1)}, bf16[256,1...) fusion(f32[256,1024]{1,0:T(8,128)S(1)} %get-tuple-element.110, ...), kind=kLoop, calls=%fused_computation.163 | loop fusion | flops 8126464 | bytes 11014400 | tf_op jit(solution)/shard_map/convert_element_type | solution.py:405
  78.1 1.1 concatenate.33.next_ref
  80.0 5.0 %fusion.101 = f32[512,1024]{1,0:T(8,128)S(1)} fusion(bf16[512,2048]{1,0:T(8,128)(2,1)} %bitcast.6, bf16[2048,1024]{1,0:T(8,128)(2,1)S(1)} %copy-done.18), kind=kOutput, calls=%fused_computation.166 | convolution fusion | flops 2147483648 | bytes 8388608 | tf_op jit(solution)/shard_map/dot_general | solution.py:17
  85.0 6.4 %multiply_convert_fusion.3 = (bf16[512,1024]{1,0:T(8,128)(2,1)}, bf16[512,1024]{1,0:T(8,128)(2,1)}, bf16[512,1024]{1,0:T(8,128)(2,1)}) fusion(f32[512,1024]{1,0:T(8,128)S(1)} %fusion.101, bf16[512,2048]{1,0:T(8,128)(2,1)} %bitcast.6, bf16[2048,1024]{1,0:T(8,128)(2,1)S(1)} %copy-done.16), kind=kOutput, calls=%fused_computation.12 | convolution fusion | flops 2154299392 | bytes 11534336 | tf_op jit(solution)/shard_map/dot_general | solution.py:17
  91.4 19.5 %all-to-all-done.1 = bf16[16,32,2048]{2,1,0:T(8,128)(2,1)} async-done(((bf16[16,32,2048]{2,1,0:T(8,128)(2,1)}), bf16[16,32,2048]{2,1,0:T(8,128)(2,1)}, u32[]{:S(2)}, u32[]{:S(2)}) %all-to-all-start.1) | async-done | bytes 2097184 | tf_op jit(solution)/shard_map/all_to_all | solution.py:356
  110.9 6.0 %multiply_convert_fusion.2 = (bf16[512,1024]{1,0:T(8,128)(2,1)S(1)}, bf16[512,1024]{1,0:T(8,128)(2,1)S(1)}) fusion(bf16[512,1024]{1,0:T(8,128)(2,1)} %get-tuple-element.69, bf16[512,1024]{1,0:T(8,128)(2,1)} %get-tuple-element.70, bf16[512,2048]{1,0:T(8,128)(2,1)} %bitcast.30, bf16[1024,2048]{1,0:T(8,128)(2,1)} %pad_maximum_fusion.2), kind=kOutput, calls=%fused_computation.11 | convolution fusion | flops 2150629376 | bytes 10485760 | tf_op jit(solution)/shard_map/dot_general | solution.py:17
  117.0 2.4 fusion.102
  119.9 4.0 %add_convert_fusion.3 = bf16[512,2048]{1,0:T(8,128)(2,1)} fusion(f32[512,2048]{1,0:T(8,128)S(1)} %fusion.102, bf16[512,1024]{1,0:T(8,128)(2,1)S(1)} %get-tuple-element.118, bf16[2048,1024]{1,0:T(8,128)(2,1)S(1)} %copy-done.17), kind=kOutput, calls=%fused_computation.6 | convolution fusion | flops 2149580800 | bytes 11534336 | tf_op jit(solution)/shard_map/dot_general | solution.py:17
  123.9 9.9 %all-to-all-start.2 = ((bf16[16,32,2048]{2,1,0:T(8,128)(2,1)}), bf16[16,32,2048]{2,1,0:T(8,128)(2,1)}, u32[]{:S(2)}, u32[]{:S(2)}) async-start(bf16[16,32,2048]{2,1,0:T(8,128)(2,1)} %bitcast.123), calls=%async_computation.2 | async-start | bytes 4194304 | tf_op jit(solution)/shard_map/all_to_all | solution.py:420
  133.9 1.9 collective-permute-start.10
  135.8 1.5 collective-permute-start.11
  137.3 1.1 slice.229
  139.0 2.9 %fusion.26 = f32[512,2048]{1,0:T(8,128)S(1)} fusion(bf16[512,2048]{1,0:T(8,128)(2,1)} %bitcast.30, bf16[512,1024]{1,0:T(8,128)(2,1)S(1)} %copy-done.30), kind=kOutput, calls=%fused_computation.76 | convolution fusion | flops 1073741824 | bytes 6815744 | tf_op jit(solution)/shard_map/dot_general | solution.py:17
  142.0 1.5 collective-permute-start.13
  143.5 1.3 fusion.103
  144.9 1.3 fusion.104
  146.2 4.4 %add_convert_fusion.2 = bf16[2048,512]{1,0:T(8,128)(2,1)} fusion(f32[2048,512]{1,0:T(8,128)S(1)} %fusion.103, bf16[512,2048]{1,0:T(8,128)(2,1)} %bitcast.6, bf16[512,1024]{1,0:T(8,128)(2,1)S(1)} %copy-done.29), kind=kOutput, calls=%fused_computation.5 | convolution fusion | flops 1075838976 | bytes 8912896 | tf_op jit(solution)/shard_map/dot_general | solution.py:17
  150.6 3.1 %collective-permute-done.10.refs_1_ = bf16[256,1024]{1,0:T(8,128)(2,1)S(1)} collective-permute-done((bf16[256,1024]{1,0:T(8,128)(2,1)S(1)}, bf16[256,1024]{1,0:T(8,128)(2,1)S(1)}, u32[]{:S(2)}, u32[]{:S(2)}) %collective-permute-start.10) | collective-permute-done | bytes 524320 | tf_op jit(solution)/shard_map/ppermute | solution.py:40
  153.7 12.3 %collective-permute-start.12 = (bf16[256,1024]{1,0:T(8,128)(2,1)S(1)}, bf16[256,1024]{1,0:T(8,128)(2,1)S(1)}, u32[]{:S(2)}, u32[]{:S(2)}) collective-permute-start(bf16[256,1024]{1,0:T(8,128)(2,1)S(1)} %get-tuple-element.79.refs_0_), channel_id=1, source_target_pairs={{0,6},{2,4},{4,2},{6,0},{8,14},{10,12},{12,10},{14,8},{16,22},{18,... | collective-permute-start | bytes 1572872 | tf_op jit(solution)/shard_map/ppermute | solution.py:40
  166.1 14.1 %collective-permute-done.13.refs_4_ = bf16[256,1024]{1,0:T(8,128)(2,1)S(1)} collective-permute-done((bf16[256,1024]{1,0:T(8,128)(2,1)S(1)}, bf16[256,1024]{1,0:T(8,128)(2,1)S(1)}, u32[]{:S(2)}, u32[]{:S(2)}) %collective-permute-start.13) | collective-permute-done | bytes 524320 | tf_op jit(solution)/shard_map/ppermute | solution.py:40
  180.2 1.5 collective-permute-start.14
  181.7 2.1 collective-permute-start.15
  184.2 4.3 %add_convert_fusion.1 = bf16[2048,512]{1,0:T(8,128)(2,1)} fusion(f32[2048,512]{1,0:T(8,128)S(1)} %fusion.104, bf16[512,2048]{1,0:T(8,128)(2,1)} %bitcast.6, bf16[512,1024]{1,0:T(8,128)(2,1)S(1)} %copy-done.27), kind=kOutput, calls=%fused_computation.4 | convolution fusion | flops 1075838976 | bytes 8912896 | tf_op jit(solution)/shard_map/dot_general | solution.py:17
  188.5 1.3 collective-permute-start.9
  189.8 2.7 %add_convert_fusion = bf16[512,2048]{1,0:T(8,128)(2,1)} fusion(f32[512,2048]{1,0:T(8,128)S(1)} %fusion.26, bf16[512,512]{1,0:T(8,128)(2,1)S(1)} %collective-permute-done.7, bf16[512,2048]{1,0:T(8,128)(2,1)S(1)} %collective-permute-done.8), kind=kOutput, calls=%fused_computation.3 | convolution fusion | flops 1075838976 | bytes 8912896 | tf_op jit(solution)/shard_map/dot_general | solution.py:17
  192.5 0.8 copy-done.5
  193.3 1.7 collective-permute-done.14.refs_5_
  195.0 0.8 copy-done.7
  195.9 9.3 %collective-permute-done.15.refs_6_ = bf16[256,1024]{1,0:T(8,128)(2,1)S(1)} collective-permute-done((bf16[256,1024]{1,0:T(8,128)(2,1)S(1)}, bf16[256,1024]{1,0:T(8,128)(2,1)S(1)}, u32[]{:S(2)}, u32[]{:S(2)}) %collective-permute-start.15) | collective-permute-done | bytes 524320 | tf_op jit(solution)/shard_map/ppermute | solution.py:40
  205.2 0.8 copy-done.9
  206.0 1.4 collective-permute-done.16.refs_7_
  207.4 0.8 copy-done.11
  208.2 2.3 convolution_convert_fusion.1.mine_ref
  210.6 2.6 %collective-permute-done.17.other_ref = bf16[256,2048]{1,0:T(8,128)(2,1)S(1)} collective-permute-done((bf16[256,2048]{1,0:T(8,128)(2,1)S(1)}, bf16[256,2048]{1,0:T(8,128)(2,1)S(1)}, u32[]{:S(2)}, u32[]{:S(2)}) %collective-permute-start.17) | collective-permute-done | bytes 1048608 | tf_op jit(solution)/shard_map/ppermute | solution.py:40
  213.3 2.0 combine.1
  215.3 5.7 %all-to-all-start.3 = ((bf16[8,256,256]{2,1,0:T(8,128)(2,1)}), bf16[8,256,256]{2,1,0:T(8,128)(2,1)S(1)}, u32[]{:S(2)}, u32[]{:S(2)}) async-start(bf16[8,256,256]{2,1,0:T(8,128)(2,1)} %get-tuple-element.78), calls=%async_computation.3 | async-start | bytes 2097152 | tf_op jit(solution)/shard_map/all_to_all | solution.py:445
  221.0 7.1 %mixer.1 = (bf16[256,1024]{1,0:T(8,128)(2,1)}, bf16[256,1024]{1,0:T(8,128)(2,1)}, bf16[256,1024]{1,0:T(8,128)(2,1)}, f32[16,2,1024]{2,1,0:T(2,128)}, f32[2,8,1024]{2,1,0:T(8,128)}) custom-call(bf16[256,2048]{1,0:T(8,128)(2,1)} %get-tuple-element.52.grad_ref, bf16[2048,1024]{1,0:T(8,128)(2,1)} %weight_ref.1, f32[256,1024]{1,0:T(8,128)} %get-tuple-element.90.gelu_ref, ...), custom_call_target="tpu_custom_call" | custom-call | flops 1073741824 | bytes 8388608 | tf_op jit(solution)/shard_map/mixer/pallas_call | solution.py:102
  228.1 7.8 %all-to-all-done.3.grads_ref = bf16[8,256,256]{2,1,0:T(8,128)(2,1)S(1)} async-done(((bf16[8,256,256]{2,1,0:T(8,128)(2,1)}), bf16[8,256,256]{2,1,0:T(8,128)(2,1)S(1)}, u32[]{:S(2)}, u32[]{:S(2)}) %all-to-all-start.3) | async-done | bytes 1048608 | tf_op jit(solution)/shard_map/all_to_all | solution.py:445
  235.9 5.1 %all-to-all-start.4 = ((f32[16,2,1024]{2,1,0:T(2,128)}), f32[16,2,1024]{2,1,0:T(2,128)S(1)}, u32[]{:S(2)}, u32[]{:S(2)}) async-start(f32[16,2,1024]{2,1,0:T(2,128)} %get-tuple-element.94), calls=%async_computation.4 | async-start | bytes 262144 | tf_op jit(solution)/shard_map/all_to_all | solution.py:452
  241.0 1.0 copy-done.4
  242.1 1.0 copy-done.6
  243.1 1.0 copy-done.8
  244.2 1.0 copy-done.10
  245.2 1.0 copy-done.12
  246.2 1.7 product.1
  248.0 2.9 %collective-permute-start.18 = (bf16[128,1024]{1,0:T(8,128)(2,1)S(1)}, bf16[128,1024]{1,0:T(8,128)(2,1)S(1)}, u32[]{:S(2)}, u32[]{:S(2)}) collective-permute-start(bf16[128,1024]{1,0:T(8,128)(2,1)S(1)} %get-tuple-element.88), channel_id=1, source_target_pairs={{0,16},{2,18},{4,20},{6,22},{8,24},{10,26},{12,28},{14,30},{16,0},... | collective-permute-start | bytes 786440 | tf_op jit(solution)/shard_map/ppermute | solution.py:40
  250.9 1.3 collective-permute-start.19
  252.2 4.9 %collective-permute-done.19.head_ref = f32[2,8,1024]{2,1,0:T(8,128)S(1)} collective-permute-done((f32[2,8,1024]{2,1,0:T(8,128)S(1)}, f32[2,8,1024]{2,1,0:T(8,128)S(1)}, u32[]{:S(2)}, u32[]{:S(2)}) %collective-permute-start.19) | collective-permute-done | bytes 65568 | tf_op jit(solution)/shard_map/ppermute | solution.py:35
  257.7 4.5 %tail.1 = bf16[256,1024]{1,0:T(8,128)(2,1)} custom-call(s32[1]{0:T(128)} %bitcast.35.where_ref, f32[16,2,1024]{2,1,0:T(2,128)} %copy-done.32, bf16[256,1024]{1,0:T(8,128)(2,1)} %get-tuple-element.95.local_ref, bf16[256,1024]{1,0:T(8,128)(2,1)} %get-tuple-element.96.cumul_ref, bf16[256,1024]{1,0:T(8,128)(2,1)} %get-tuple-element.97.to_decay_ref, ...), custom_call_target="tpu_custom_call" | custom-call | flops 268435456 | bytes 7340032 | tf_op jit(solution)/shard_map/tail/pallas_call | solution.py:183
  262.8 0.8 convert_add_fusion.1
  (137 shorter events, 9.8 us)
Async XLA Ops:
  0.6 3.8 %copy-start = (bf16[256,2048]{1,0:T(8,128)(2,1)S(1)}, bf16[256,2048]{1,0:T(8,128)(2,1)}, u32[]{:S(2)}) copy-start(bf16[256,2048]{1,0:T(8,128)(2,1)} %param.16) | copy-start | bytes 3145732
  6.5 9.4 %copy-start.15 = (f32[256,1024]{1,0:T(8,128)S(1)}, f32[256,1024]{1,0:T(8,128)}, u32[]{:S(2)}) copy-start(f32[256,1024]{1,0:T(8,128)} %param.26) | copy-start | bytes 3145732
  6.5 9.4 %copy-start.31 = (bf16[256,1024]{1,0:T(8,128)(2,1)S(1)}, bf16[256,1024]{1,0:T(8,128)(2,1)}, u32[]{:S(2)}) copy-start(bf16[256,1024]{1,0:T(8,128)(2,1)} %param.24) | copy-start | bytes 1572868
  6.5 14.4 %copy-start.37 = (f32[256,2]{0,1:T(2,128)S(1)}, f32[256,2]{0,1:T(2,128)}, u32[]{:S(2)}) copy-start(f32[256,2]{0,1:T(2,128)} %param.19) | copy-start | bytes 6148
  6.5 14.6 %copy-start.36 = (f32[1024]{0:T(1024)S(1)}, f32[1024]{0:T(1024)}, u32[]{:S(2)}) copy-start(f32[1024]{0:T(1024)} %param.30) | copy-start | bytes 12292
  6.5 14.6 %copy-start.34 = (bf16[4,1024]{1,0:T(4,128)(2,1)S(1)}, bf16[4,1024]{1,0:T(4,128)(2,1)}, u32[]{:S(2)}) copy-start(bf16[4,1024]{1,0:T(4,128)(2,1)} %taps_ref.1) | copy-start | bytes 24580
  6.5 14.7 %copy-start.2 = (bf16[256,2048]{1,0:T(8,128)(2,1)S(1)}, bf16[256,2048]{1,0:T(8,128)(2,1)}, u32[]{:S(2)}) copy-start(bf16[256,2048]{1,0:T(8,128)(2,1)} %cot_ref.1) | copy-start | bytes 3145732
  6.5 51.8 %all-to-all-start = ((bf16[16,32,2048]{2,1,0:T(8,128)(2,1)}), bf16[16,32,2048]{2,1,0:T(8,128)(2,1)}, u32[]{:S(2)}, u32[]{:S(2)}) async-start(bf16[16,32,2048]{2,1,0:T(8,128)(2,1)} %bitcast.118), calls=%async_computation | async-start | bytes 4194304 | tf_op jit(solution)/shard_map/all_to_all | solution.py:333
  15.2 10.2 %collective-permute-start.1 = (bf16[2048,512]{1,0:T(8,128)(2,1)}, bf16[2048,512]{1,0:T(8,128)(2,1)}, u32[]{:S(2)}, u32[]{:S(2)}) collective-permute-start(bf16[2048,512]{1,0:T(8,128)(2,1)} %bitcast.124), channel_id=1, source_target_pairs={{0,1},{1,0},{2,3},{3,2},{4,5},{5,4},{6,7},{7,6},{8,9},{9,8},{10,11... | collective-permute-start | bytes 6291464 | tf_op jit(solution)/shard_map/ppermute | solution.py:40
  15.3 14.4 %collective-permute-start.2 = (bf16[2048,512]{1,0:T(8,128)(2,1)}, bf16[2048,512]{1,0:T(8,128)(2,1)}, u32[]{:S(2)}, u32[]{:S(2)}) collective-permute-start(bf16[2048,512]{1,0:T(8,128)(2,1)} %bitcast.126), channel_id=1, source_target_pairs={{0,1},{1,0},{2,3},{3,2},{4,5},{5,4},{6,7},{7,6},{8,9},{9,8},{10,11... | collective-permute-start | bytes 6291464 | tf_op jit(solution)/shard_map/ppermute | solution.py:40
  15.8 18.2 %collective-permute-start.3 = (bf16[512,2048]{1,0:T(8,128)(2,1)}, bf16[512,2048]{1,0:T(8,128)(2,1)}, u32[]{:S(2)}, u32[]{:S(2)}) collective-permute-start(bf16[512,2048]{1,0:T(8,128)(2,1)} %bitcast.128), channel_id=1, source_target_pairs={{0,1},{1,0},{2,3},{3,2},{4,5},{5,4},{6,7},{7,6},{8,9},{9,8},{10,11... | collective-permute-start | bytes 6291464 | tf_op jit(solution)/shard_map/ppermute | solution.py:40
  15.9 7.3 %copy-start.33 = (bf16[256,1024]{1,0:T(8,128)(2,1)S(1)}, bf16[256,1024]{1,0:T(8,128)(2,1)}, u32[]{:S(2)}) copy-start(bf16[256,1024]{1,0:T(8,128)(2,1)} %param.25) | copy-start | bytes 1572868
  15.9 22.3 %collective-permute-start = (f32[4,1024]{1,0:T(4,128)S(1)}, f32[4,1024]{1,0:T(4,128)S(1)}, u32[]{:S(2)}, u32[]{:S(2)}) collective-permute-start(f32[4,1024]{1,0:T(4,128)S(1)} %pad_maximum_fusion.5), channel_id=1, source_target_pairs={{0,2},{2,4},{4,6},{6,8},{8,10},{10,12},{12,14},{14,16},{16,18},{18... | collective-permute-start | bytes 49160 | tf_op jit(solution)/shard_map/ppermute | solution.py:35
  23.2 2.1 copy-start.20
  25.4 4.3 %copy-start.21 = (bf16[1,2048,512]{2,1,0:T(8,128)(2,1)S(1)}, bf16[1,2048,512]{2,1,0:T(8,128)(2,1)}, u32[]{:S(2)}) copy-start(bf16[1,2048,512]{2,1,0:T(8,128)(2,1)} %param.21) | copy-start | bytes 6291460
  29.7 4.3 %copy-start.22 = (bf16[1,512,2048]{2,1,0:T(8,128)(2,1)S(1)}, bf16[1,512,2048]{2,1,0:T(8,128)(2,1)}, u32[]{:S(2)}) copy-start(bf16[1,512,2048]{2,1,0:T(8,128)(2,1)} %param.22) | copy-start | bytes 6291460
  58.3 52.6 %all-to-all-start.1 = ((bf16[16,32,2048]{2,1,0:T(8,128)(2,1)}), bf16[16,32,2048]{2,1,0:T(8,128)(2,1)}, u32[]{:S(2)}, u32[]{:S(2)}) async-start(bf16[16,32,2048]{2,1,0:T(8,128)(2,1)} %bitcast.117), calls=%async_computation.1 | async-start | bytes 4194304 | tf_op jit(solution)/shard_map/all_to_all | solution.py:356
  68.6 3.4 %copy-start.24 = (bf16[8,128,128]{2,1,0:T(8,128)(2,1)S(1)}, bf16[8,128,128]{2,1,0:T(8,128)(2,1)}, u32[]{:S(2)}) copy-start(bf16[8,128,128]{2,1,0:T(8,128)(2,1)} %input_w_ref.1) | copy-start | bytes 786436
  68.6 10.7 %collective-permute-start.4 = (bf16[512,2048]{1,0:T(8,128)(2,1)}, bf16[512,2048]{1,0:T(8,128)(2,1)S(1)}, u32[]{:S(2)}, u32[]{:S(2)}) collective-permute-start(bf16[512,2048]{1,0:T(8,128)(2,1)} %bitcast.6), channel_id=1, source_target_pairs={{0,1},{1,0},{2,3},{3,2},{4,5},{5,4},{6,7},{7,6},{8,9},{9,8},{10,11... | collective-permute-start | bytes 6291464 | tf_op jit(solution)/shard_map/ppermute | solution.py:40
  68.7 4.5 %copy-start.25 = (bf16[8,128,128]{2,1,0:T(8,128)(2,1)S(1)}, bf16[8,128,128]{2,1,0:T(8,128)(2,1)}, u32[]{:S(2)}) copy-start(bf16[8,128,128]{2,1,0:T(8,128)(2,1)} %decay_w_ref.1) | copy-start | bytes 786436
  71.9 2.4 copy-start.23
  77.4 2.6 copy-start.18
  79.2 5.8 %copy-start.16 = (bf16[2048,1024]{1,0:T(8,128)(2,1)S(1)}, bf16[2048,1024]{1,0:T(8,128)(2,1)}, u32[]{:S(2)}) copy-start(bf16[2048,1024]{1,0:T(8,128)(2,1)} %pad_maximum_fusion) | copy-start | bytes 12582916
  80.0 5.0 %copy-start.13 = (bf16[512,2048]{1,0:T(8,128)(2,1)}, bf16[512,2048]{1,0:T(8,128)(2,1)S(1)}, u32[]{:S(2)}) copy-start(bf16[512,2048]{1,0:T(8,128)(2,1)S(1)} %collective-permute-done.4) | copy-start | bytes 6291460
  110.9 6.0 %copy-start.19 = (bf16[2048,1024]{1,0:T(8,128)(2,1)S(1)}, bf16[2048,1024]{1,0:T(8,128)(2,1)}, u32[]{:S(2)}) copy-start(bf16[2048,1024]{1,0:T(8,128)(2,1)} %pad_maximum_fusion.1) | copy-start | bytes 12582916
  116.9 2.4 copy-start.26
  116.9 16.8 %copy-start.28 = (bf16[512,1024]{1,0:T(8,128)(2,1)}, bf16[512,1024]{1,0:T(8,128)(2,1)S(1)}, u32[]{:S(2)}) copy-start(bf16[512,1024]{1,0:T(8,128)(2,1)S(1)} %get-tuple-element.118) | copy-start | bytes 3145732
  117.0 2.9 %copy-start.17 = (bf16[2048,1024]{1,0:T(8,128)(2,1)S(1)}, bf16[2048,1024]{1,0:T(8,128)(2,1)}, u32[]{:S(2)}) copy-start(bf16[2048,1024]{1,0:T(8,128)(2,1)} %pad_maximum_fusion) | copy-start | bytes 12582916
  123.9 84.3 %all-to-all-start.2 = ((bf16[16,32,2048]{2,1,0:T(8,128)(2,1)}), bf16[16,32,2048]{2,1,0:T(8,128)(2,1)}, u32[]{:S(2)}, u32[]{:S(2)}) async-start(bf16[16,32,2048]{2,1,0:T(8,128)(2,1)} %bitcast.123), calls=%async_computation.2 | async-start | bytes 4194304 | tf_op jit(solution)/shard_map/all_to_all | solution.py:420
  133.8 5.2 %copy-start.30 = (bf16[512,1024]{1,0:T(8,128)(2,1)S(1)}, bf16[512,1024]{1,0:T(8,128)(2,1)}, u32[]{:S(2)}) copy-start(bf16[512,1024]{1,0:T(8,128)(2,1)} %get-tuple-element.72) | copy-start | bytes 3145732
  133.8 8.1 %collective-permute-start.5 = (bf16[512,512]{1,0:T(8,128)(2,1)S(1)}, bf16[512,512]{1,0:T(8,128)(2,1)S(1)}, u32[]{:S(2)}, u32[]{:S(2)}) collective-permute-start(bf16[512,512]{1,0:T(8,128)(2,1)S(1)} %slice.227), channel_id=1, source_target_pairs={{0,1},{1,0},{2,3},{3,2},{4,5},{5,4},{6,7},{7,6},{8,9},{9,8},{10,11... | collective-permute-start | bytes 1572872 | tf_op jit(solution)/shard_map/ppermute | solution.py:40
  133.9 19.8 %collective-permute-start.10 = (bf16[256,1024]{1,0:T(8,128)(2,1)S(1)}, bf16[256,1024]{1,0:T(8,128)(2,1)S(1)}, u32[]{:S(2)}, u32[]{:S(2)}) collective-permute-start(bf16[256,1024]{1,0:T(8,128)(2,1)S(1)} %get-tuple-element.79.refs_0_), channel_id=1, source_target_pairs={{0,2},{2,0},{4,6},{6,4},{8,10},{10,8},{12,14},{14,12},{16,18},{18,... | collective-permute-start | bytes 1572872 | tf_op jit(solution)/shard_map/ppermute | solution.py:40
  135.8 45.8 %collective-permute-start.11 = (bf16[256,1024]{1,0:T(8,128)(2,1)S(1)}, bf16[256,1024]{1,0:T(8,128)(2,1)S(1)}, u32[]{:S(2)}, u32[]{:S(2)}) collective-permute-start(bf16[256,1024]{1,0:T(8,128)(2,1)S(1)} %get-tuple-element.79.refs_0_), channel_id=1, source_target_pairs={{0,4},{2,6},{4,0},{6,2},{8,12},{10,14},{12,8},{14,10},{16,20},{18,... | collective-permute-start | bytes 1572872 | tf_op jit(solution)/shard_map/ppermute | solution.py:40
  138.4 5.1 %copy-start.14 = (bf16[512,2048]{1,0:T(8,128)(2,1)S(1)}, bf16[512,2048]{1,0:T(8,128)(2,1)}, u32[]{:S(2)}) copy-start(bf16[512,2048]{1,0:T(8,128)(2,1)} %copy-done.13) | copy-start | bytes 6291460
  138.4 50.1 %collective-permute-start.8 = (bf16[512,2048]{1,0:T(8,128)(2,1)}, bf16[512,2048]{1,0:T(8,128)(2,1)S(1)}, u32[]{:S(2)}, u32[]{:S(2)}) collective-permute-start(bf16[512,2048]{1,0:T(8,128)(2,1)} %bitcast.30), channel_id=1, source_target_pairs={{0,1},{1,0},{2,3},{3,2},{4,5},{5,4},{6,7},{7,6},{8,9},{9,8},{10,11... | collective-permute-start | bytes 6291464 | tf_op jit(solution)/shard_map/ppermute | solution.py:40
  138.5 6.3 %collective-permute-start.6 = (bf16[512,512]{1,0:T(8,128)(2,1)S(1)}, bf16[512,512]{1,0:T(8,128)(2,1)S(1)}, u32[]{:S(2)}, u32[]{:S(2)}) collective-permute-start(bf16[512,512]{1,0:T(8,128)(2,1)S(1)} %slice.229), channel_id=1, source_target_pairs={{0,1},{1,0},{2,3},{3,2},{4,5},{5,4},{6,7},{7,6},{8,9},{9,8},{10,11... | collective-permute-start | bytes 1572872 | tf_op jit(solution)/shard_map/ppermute | solution.py:40
  142.0 38.2 %collective-permute-start.13 = (bf16[256,1024]{1,0:T(8,128)(2,1)S(1)}, bf16[256,1024]{1,0:T(8,128)(2,1)S(1)}, u32[]{:S(2)}, u32[]{:S(2)}) collective-permute-start(bf16[256,1024]{1,0:T(8,128)(2,1)S(1)} %get-tuple-element.79.refs_0_), channel_id=1, source_target_pairs={{0,8},{2,10},{4,12},{6,14},{8,0},{10,2},{12,4},{14,6},{16,24},{18,... | collective-permute-start | bytes 1572872 | tf_op jit(solution)/shard_map/ppermute | solution.py:40
  144.8 1.4 copy-start.29
  144.8 38.9 %collective-permute-start.7 = (bf16[512,512]{1,0:T(8,128)(2,1)S(1)}, bf16[512,512]{1,0:T(8,128)(2,1)S(1)}, u32[]{:S(2)}, u32[]{:S(2)}) collective-permute-start(bf16[512,512]{1,0:T(8,128)(2,1)S(1)} %slice.203), channel_id=1, source_target_pairs={{0,1},{1,0},{2,3},{3,2},{4,5},{5,4},{6,7},{7,6},{8,9},{9,8},{10,11... | collective-permute-start | bytes 1572872 | tf_op jit(solution)/shard_map/ppermute | solution.py:40
  146.2 38.0 %copy-start.27 = (bf16[512,1024]{1,0:T(8,128)(2,1)S(1)}, bf16[512,1024]{1,0:T(8,128)(2,1)}, u32[]{:S(2)}) copy-start(bf16[512,1024]{1,0:T(8,128)(2,1)} %copy-done.26) | copy-start | bytes 3145732
  153.7 38.8 %collective-permute-start.12 = (bf16[256,1024]{1,0:T(8,128)(2,1)S(1)}, bf16[256,1024]{1,0:T(8,128)(2,1)S(1)}, u32[]{:S(2)}, u32[]{:S(2)}) collective-permute-start(bf16[256,1024]{1,0:T(8,128)(2,1)S(1)} %get-tuple-element.79.refs_0_), channel_id=1, source_target_pairs={{0,6},{2,4},{4,2},{6,0},{8,14},{10,12},{12,10},{14,8},{16,22},{18,... | collective-permute-start | bytes 1572872 | tf_op jit(solution)/shard_map/ppermute | solution.py:40
  180.2 8.3 %copy-start.3 = (bf16[256,1024]{1,0:T(8,128)(2,1)}, bf16[256,1024]{1,0:T(8,128)(2,1)S(1)}, u32[]{:S(2)}) copy-start(bf16[256,1024]{1,0:T(8,128)(2,1)S(1)} %collective-permute-done.13.refs_4_) | copy-start | bytes 1572868
  180.2 14.9 %collective-permute-start.14 = (bf16[256,1024]{1,0:T(8,128)(2,1)S(1)}, bf16[256,1024]{1,0:T(8,128)(2,1)S(1)}, u32[]{:S(2)}, u32[]{:S(2)}) collective-permute-start(bf16[256,1024]{1,0:T(8,128)(2,1)S(1)} %collective-permute-done.13.refs_4_), channel_id=1, source_target_pairs={{0,2},{2,0},{4,6},{6,4},{8,10},{10,8},{12,14},{14,12},{16,18},{18,... | collective-permute-start | bytes 1572872 | tf_op jit(solution)/shard_map/ppermute | solution.py:40
  181.7 23.5 %collective-permute-start.15 = (bf16[256,1024]{1,0:T(8,128)(2,1)S(1)}, bf16[256,1024]{1,0:T(8,128)(2,1)S(1)}, u32[]{:S(2)}, u32[]{:S(2)}) collective-permute-start(bf16[256,1024]{1,0:T(8,128)(2,1)S(1)} %collective-permute-done.13.refs_4_), channel_id=1, source_target_pairs={{0,4},{2,6},{4,0},{6,2},{8,12},{10,14},{12,8},{14,10},{16,20},{18,... | collective-permute-start | bytes 1572872 | tf_op jit(solution)/shard_map/ppermute | solution.py:40
  183.7 23.7 %collective-permute-start.16 = (bf16[256,1024]{1,0:T(8,128)(2,1)S(1)}, bf16[256,1024]{1,0:T(8,128)(2,1)S(1)}, u32[]{:S(2)}, u32[]{:S(2)}) collective-permute-start(bf16[256,1024]{1,0:T(8,128)(2,1)S(1)} %collective-permute-done.13.refs_4_), channel_id=1, source_target_pairs={{0,6},{2,4},{4,2},{6,0},{8,14},{10,12},{12,10},{14,8},{16,22},{18,... | collective-permute-start | bytes 1572872 | tf_op jit(solution)/shard_map/ppermute | solution.py:40
  188.5 19.7 %collective-permute-start.9 = (f32[3,8,1024]{2,1,0:T(8,128)S(1)}, f32[3,8,1024]{2,1,0:T(8,128)}, u32[]{:S(2)}, u32[]{:S(2)}) collective-permute-start(f32[3,8,1024]{2,1,0:T(8,128)S(1)} %pad_maximum_fusion.4), channel_id=1, source_target_pairs={{2,0},{4,2},{6,4},{8,6},{10,8},{12,10},{14,12},{16,14},{18,16},{20... | collective-permute-start | bytes 294920 | tf_op jit(solution)/shard_map/ppermute | solution.py:35
  192.5 0.8 copy-start.5
  195.0 0.8 copy-start.7
  205.2 0.8 copy-start.9
  207.4 0.8 copy-start.11
  210.6 2.7 %collective-permute-start.17 = (bf16[256,2048]{1,0:T(8,128)(2,1)S(1)}, bf16[256,2048]{1,0:T(8,128)(2,1)S(1)}, u32[]{:S(2)}, u32[]{:S(2)}) collective-permute-start(bf16[256,2048]{1,0:T(8,128)(2,1)S(1)} %convolution_convert_fusion.1.mine_ref), channel_id=1, source_target_pairs={{0,1},{1,0},{2,3},{3,2},{4,5},{5,4},{6,7},{7,6},{8,9},{9,8},{10,11... | collective-permute-start | bytes 3145736 | tf_op jit(solution)/shard_map/ppermute | solution.py:40
  215.3 20.6 %all-to-all-start.3 = ((bf16[8,256,256]{2,1,0:T(8,128)(2,1)}), bf16[8,256,256]{2,1,0:T(8,128)(2,1)S(1)}, u32[]{:S(2)}, u32[]{:S(2)}) async-start(bf16[8,256,256]{2,1,0:T(8,128)(2,1)} %get-tuple-element.78), calls=%async_computation.3 | async-start | bytes 2097152 | tf_op jit(solution)/shard_map/all_to_all | solution.py:445
  235.9 21.2 %all-to-all-start.4 = ((f32[16,2,1024]{2,1,0:T(2,128)}), f32[16,2,1024]{2,1,0:T(2,128)S(1)}, u32[]{:S(2)}, u32[]{:S(2)}) async-start(f32[16,2,1024]{2,1,0:T(2,128)} %get-tuple-element.94), calls=%async_computation.4 | async-start | bytes 262144 | tf_op jit(solution)/shard_map/all_to_all | solution.py:452
  241.0 1.0 copy-start.4
  242.1 1.0 copy-start.6
  243.1 1.0 copy-start.8
  244.2 1.0 copy-start.10
  245.2 1.0 copy-start.12
  246.2 4.7 %copy-start.38 = (f32[2,8,1024]{2,1,0:T(8,128)S(1)}, f32[2,8,1024]{2,1,0:T(8,128)}, u32[]{:S(2)}) copy-start(f32[2,8,1024]{2,1,0:T(8,128)} %get-tuple-element.100) | copy-start | bytes 196612
  248.0 14.8 %collective-permute-start.18 = (bf16[128,1024]{1,0:T(8,128)(2,1)S(1)}, bf16[128,1024]{1,0:T(8,128)(2,1)S(1)}, u32[]{:S(2)}, u32[]{:S(2)}) collective-permute-start(bf16[128,1024]{1,0:T(8,128)(2,1)S(1)} %get-tuple-element.88), channel_id=1, source_target_pairs={{0,16},{2,18},{4,20},{6,22},{8,24},{10,26},{12,28},{14,30},{16,0},... | collective-permute-start | bytes 786440 | tf_op jit(solution)/shard_map/ppermute | solution.py:40
  250.9 6.1 %collective-permute-start.19 = (f32[2,8,1024]{2,1,0:T(8,128)S(1)}, f32[2,8,1024]{2,1,0:T(8,128)S(1)}, u32[]{:S(2)}, u32[]{:S(2)}) collective-permute-start(f32[2,8,1024]{2,1,0:T(8,128)S(1)} %copy-done.38), channel_id=1, source_target_pairs={{2,0},{4,2},{6,4},{8,6},{10,8},{12,10},{14,12},{16,14},{18,16},{20... | collective-permute-start | bytes 196616 | tf_op jit(solution)/shard_map/ppermute | solution.py:35
  257.1 0.6 copy-start.35
  257.1 0.7 copy-start.32
  257.1 6.6 %copy-start.1 = (bf16[256,2048]{1,0:T(8,128)(2,1)S(1)}, bf16[256,2048]{1,0:T(8,128)(2,1)}, u32[]{:S(2)}) copy-start(bf16[256,2048]{1,0:T(8,128)(2,1)} %param.16) | copy-start | bytes 3145732
